TPU v7x, 256 devices: a whole 4x4x8 slice. The times are simulated.
256 devices in a mesh: ep: 32 (over z, x), tp: 8 (over y, core).
Axes of the slice: x: 4, y: 4, z: 8, core: 2. Of those that a mesh axis runs over, the one named last changes fastest.
Arguments:
- tokens: bfloat16 [2048, 2048], P('ep', 'tp')
- norm_gain: float32 [2048], P('tp'), may hold values from 0.1 to 1.9
- expert_ids: int32 [2048, 4], P('ep'), may hold values from 0 to 31, all different within a row; in each aligned block of 64 rows (0 to 63, 64 to 127, ...) at most 16 rows name the same one
- route_weights: float32 [2048, 4], P('ep'), may hold values from 0.1 to 1
- gate_proj: bfloat16 [32, 2048, 2048], P('ep', None, 'tp'), may hold values from -0.5 to 0.5
- up_proj: bfloat16 [32, 2048, 2048], P('ep', None, 'tp'), may hold values from -0.5 to 0.5
- down_proj: bfloat16 [32, 2048, 2048], P('ep', 'tp')
- final_gain: float32 [2048], P('tp'), may hold values from 0.1 to 1.9
Outputs:
- layer_output: bfloat16 [2048, 2048], P('ep', 'tp')
Inputs may be any that keep to these rules, and one draw needn't show every extreme that they name: `expert_ids`: each row names 4 different experts. Within the 64 rows of one device no expert is named by more than 16 rows, a bound that some block reaches.
All inputs are finite; a program needn't handle non-finite values.
Results may differ from a plain program's by a relative error of at most 0.017.
Values may be sent and summed in bfloat16 or wider, within the bound.
No kernel may reach another device: no remote copies, remote signals or barrier semaphores. Data moves between devices by JAX's collectives and lax.ppermute only.
A program may use at most 64 MiB of HBM per device.

v0:
```python
import functools

import jax
import jax.numpy as jnp
from jax import lax
from jax.experimental import pallas as pl
from jax.experimental.pallas import tpu as pltpu
from jax.sharding import PartitionSpec as P


EPSILON = 1e-05
CLAMP_LIMIT = 7.0
SIGMOID_SLOPE = 1.702
CORES = 2
TAIL = 16
VMEM = pl.BlockSpec(memory_space=pltpu.VMEM)
HBM = pl.BlockSpec(memory_space=pltpu.HBM)


def split3(v):
    hi = v.astype(jnp.bfloat16)
    rest = v - hi.astype(jnp.float32)
    mid = rest.astype(jnp.bfloat16)
    lo = (rest - mid.astype(jnp.float32)).astype(jnp.bfloat16)
    return hi, mid, lo


def dot_t(a, b):
    return lax.dot_general(a, b, (((1,), (1,)), ((), ())), preferred_element_type=jnp.float32)


def dot_0(a, b):
    return lax.dot_general(a, b, (((0,), (0,)), ((), ())), preferred_element_type=jnp.float32)


def slot_matrix(ids, experts, capacity):
    choices, tokens = ids.shape
    expert = lax.broadcasted_iota(jnp.int32, (experts, tokens), 0)
    named = [(ids[k : k + 1, :] == expert).astype(jnp.float32) for k in range(choices)]
    match = functools.reduce(jnp.add, named)
    before = lax.broadcasted_iota(jnp.int32, (tokens, tokens), 0)
    after = lax.broadcasted_iota(jnp.int32, (tokens, tokens), 1)
    earlier = (before < after).astype(jnp.bfloat16)
    place = jnp.dot(match.astype(jnp.bfloat16), earlier, preferred_element_type=jnp.float32)
    place = jnp.where(match > 0.0, place, -1.0)

    def spread(rows):
        wide = jnp.broadcast_to(rows[:, None, :], (experts, capacity, tokens))
        return wide.reshape(experts * capacity, tokens)

    slot = lax.broadcasted_iota(jnp.int32, (experts, capacity, tokens), 1)
    slot = slot.reshape(experts * capacity, tokens).astype(jnp.float32)
    holds = spread(place) == slot
    return holds, named, spread


def pick_kernel(experts, capacity, ids_hbm, tokens_hbm, gain_hbm, rows_ref, gain_ref, ids_ref, tokens_ref, sems):
    copies = [
        pltpu.make_async_copy(ids_hbm, ids_ref, sems.at[0]),
        pltpu.make_async_copy(tokens_hbm, tokens_ref, sems.at[1]),
        pltpu.make_async_copy(gain_hbm, gain_ref, sems.at[2]),
    ]
    for copy in copies:
        copy.start()
    copies[0].wait()
    holds, _, _ = slot_matrix(ids_ref[...], experts, capacity)
    holds = holds.astype(jnp.bfloat16)
    copies[1].wait()
    picked = jnp.dot(holds, tokens_ref[...], preferred_element_type=jnp.float32)
    rows_ref[...] = picked.astype(jnp.bfloat16)
    copies[2].wait()


def load_kernel(experts, capacity, *refs):
    ids_hbm, weights_hbm, *sources = refs[:6]
    share_ref, *targets = refs[6:11]
    ids_ref, weights_ref, sems = refs[11:]
    pairs = [(ids_hbm, ids_ref), (weights_hbm, weights_ref), *zip(sources, targets)]
    copies = [pltpu.make_async_copy(*pair, sems.at[i]) for i, pair in enumerate(pairs)]
    for copy in copies:
        copy.start()
    copies[0].wait()
    holds, named, spread = slot_matrix(ids_ref[...], experts, capacity)
    copies[1].wait()
    weights = weights_ref[...]
    share = functools.reduce(
        jnp.add, [weights[k : k + 1, :] * named[k] for k in range(len(named))]
    )
    share = jnp.where(holds, spread(share), 0.0).T
    tokens = share.shape[0]
    for i, part in enumerate(split3(share)):
        share_ref[i * tokens : (i + 1) * tokens, :] = part
    for copy in copies[2:]:
        copy.wait()


def mid_kernel(rows_ref, gain_ref, out_ref):
    rows, width = rows_ref.shape
    x = rows_ref[...].astype(jnp.float32)
    out_ref[0:rows, :] = (x * gain_ref[...]).astype(jnp.bfloat16)
    hi, mid, _ = split3(x * x)
    ones = jnp.ones((8, width), jnp.bfloat16)
    sums = dot_t(ones, hi) + dot_t(ones, mid)
    row = lax.broadcasted_iota(jnp.int32, (8, width), 0)
    tail = []
    for part in range(rows // width):
        pieces = [v.astype(jnp.float32) for v in split3(sums[:, part * width : (part + 1) * width])]
        tail.append(
            jnp.where(
                row == 0,
                pieces[0],
                jnp.where(row == 1, pieces[1], jnp.where(row == 2, pieces[2], 0.0)),
            )
        )
    out_ref[rows : rows + TAIL, :] = jnp.concatenate(tail, axis=0).astype(jnp.bfloat16)


def ahead(step, other, chips):
    me = lax.axis_index("tp")
    core = me % CORES
    return (me // CORES + step * (1 - 2 * core) + chips) % chips * CORES + (core + other) % CORES


def products(part, width, places, pieces, gate_ref, up_ref, gate, up, squares):
    rows = pieces[0].shape[0] - TAIL
    at = part * width
    row = lax.broadcasted_iota(jnp.int32, (TAIL, 128), 0)
    ones = jnp.where(row // 8 == part, 1.0, 0.0).astype(jnp.bfloat16)
    for where, piece in zip(places, pieces):
        from_row = pl.ds(pl.multiple_of(ahead(*where) * width, width), width)
        x = piece[at : at + width, :]
        gate += jnp.dot(x, gate_ref[from_row, :], preferred_element_type=jnp.float32)
        up += jnp.dot(x, up_ref[from_row, :], preferred_element_type=jnp.float32)
        squares += dot_0(piece[rows : rows + TAIL, :], ones)
    return gate, up, squares


def first_kernel(places, *refs):
    count = len(places)
    gate_ref, up_ref, gate_out, up_out, squares_out = refs[count:]
    width = gate_ref.shape[1]
    for part in range(gate_out.shape[0] // width):
        at = slice(part * width, (part + 1) * width)
        zero = jnp.zeros((width, width), jnp.float32)
        gate, up, squares = products(
            part, width, places, refs[:count], gate_ref, up_ref, zero, zero, zero[:, :128]
        )
        gate_out[at, :] = gate
        up_out[at, :] = up
        squares_out[at, :] = squares


def last_kernel(places, *refs):
    count = len(places)
    gate_ref, up_ref, gate_in, up_in, squares_in, act_ref = refs[count:]
    model_width, width = gate_ref.shape
    for part in range(gate_in.shape[0] // width):
        at = slice(part * width, (part + 1) * width)
        gate, up, squares = products(
            part, width, places, refs[:count], gate_ref, up_ref,
            gate_in[at, :], up_in[at, :], squares_in[at, :],
        )
        scale = lax.rsqrt(squares / model_width + EPSILON)
        scale = jnp.concatenate([scale] * (width // 128), axis=1)
        gate = jnp.minimum(gate * scale, CLAMP_LIMIT)
        up = jnp.clip(up * scale, -CLAMP_LIMIT, CLAMP_LIMIT)
        act = (up + 1.0) * gate * jax.nn.sigmoid(SIGMOID_SLOPE * gate)
        act_ref[at, :] = act.astype(jnp.bfloat16)


def down_kernel(places, own_ref, other_ref, down_ref, down_other_ref, *outs):
    width = own_ref.shape[1]
    for where, out in zip(places, outs):
        columns = pl.ds(pl.multiple_of(ahead(*where) * width, width), width)
        total = jnp.dot(own_ref[...], down_ref[:, columns], preferred_element_type=jnp.float32)
        total += jnp.dot(
            other_ref[...], down_other_ref[:, columns], preferred_element_type=jnp.float32
        )
        out[...] = total.astype(jnp.bfloat16)


def combine_kernel(share_ref, rows_ref, mix_ref, squares_ref):
    tokens = mix_ref.shape[0]
    parts = jnp.dot(share_ref[...], rows_ref[...], preferred_element_type=jnp.float32)
    mix = parts[:tokens] + parts[tokens : 2 * tokens] + parts[2 * tokens :]
    mix_ref[...] = mix
    ones = jnp.ones((8, mix.shape[1]), jnp.bfloat16)
    sums = functools.reduce(jnp.add, [dot_t(ones, part) for part in split3(mix * mix)])
    sums = jnp.concatenate([sums, jnp.zeros_like(sums)], axis=1)
    for i in range(squares_ref.shape[0]):
        squares_ref[i] = sums


def final_kernel(model_width, mix_ref, squares_ref, gain_ref, out_ref):
    total = squares_ref[0]
    for i in range(1, squares_ref.shape[0]):
        total += squares_ref[i]
    mix = mix_ref[...]
    tokens = mix.shape[0]
    wide = jnp.concatenate([total] * (tokens // 8), axis=0)
    row = lax.broadcasted_iota(jnp.int32, wide.shape, 0)
    lane = lax.broadcasted_iota(jnp.int32, wide.shape, 1)
    column = jnp.sum(jnp.where(row == lane, wide, 0.0), axis=1, keepdims=True)
    scale = lax.rsqrt(column / model_width + EPSILON)
    out_ref[...] = (mix * scale * gain_ref[...]).astype(jnp.bfloat16)


def call(kernel, outs, *args, limit=8, flops=0, space=VMEM, scratch=()):
    single = not isinstance(outs, (list, tuple))
    if space is HBM:
        args = [pltpu.with_memory_space_constraint(arg, pltpu.HBM) for arg in args]
    return pl.pallas_call(
        kernel,
        out_shape=outs,
        in_specs=[space] * len(args),
        out_specs=VMEM if single else [VMEM] * len(outs),
        scratch_shapes=scratch,
        cost_estimate=pl.CostEstimate(flops=flops, bytes_accessed=0, transcendentals=0),
        compiler_params=pltpu.CompilerParams(vmem_limit_bytes=limit << 20),
    )(*args)


def shape_of(dims, dtype):
    return jax.ShapeDtypeStruct(dims, dtype)


def local(tokens, norm_gain, expert_ids, route_weights, gate_proj, up_proj, down_proj, final_gain):
    tok_rows, width = tokens.shape
    peers = lax.axis_size("tp")
    experts = lax.axis_size("ep")
    chips = peers // CORES
    capacity = min(tok_rows, 2 * tok_rows * expert_ids.shape[1] // experts)
    rows = experts * capacity
    model_width = width * peers

    def onward(value):
        pairs = [
            (y * CORES + c, ((y + 1 - 2 * c) % chips) * CORES + c)
            for y in range(chips)
            for c in range(CORES)
        ]
        return lax.ppermute(value, "tp", pairs)

    def swap(value):
        pairs = [(y * CORES + c, y * CORES + 1 - c) for y in range(chips) for c in range(CORES)]
        return lax.ppermute(value, "tp", pairs)

    narrow = shape_of((rows, width), jnp.bfloat16)
    ids = expert_ids.T
    outbound, gain = call(
        functools.partial(pick_kernel, experts, capacity),
        [narrow, shape_of((1, width), jnp.float32)],
        ids,
        tokens,
        norm_gain[None, :],
        space=HBM,
        scratch=(
            pltpu.VMEM(ids.shape, jnp.int32),
            pltpu.VMEM(tokens.shape, jnp.bfloat16),
            pltpu.SemaphoreType.DMA((3,)),
        ),
    )
    received = lax.all_to_all(
        outbound.reshape(experts, capacity, width), "ep", split_axis=0, concat_axis=0, tiled=True
    ).reshape(rows, width)
    own = call(mid_kernel, shape_of((rows + TAIL, width), jnp.bfloat16), received, gain)

    first = onward(own)
    own_other = swap(own)
    sources = (ids, route_weights.T, final_gain[None, :], gate_proj[0], up_proj[0], down_proj[0])
    share, final_gain, gate, up, down = call(
        functools.partial(load_kernel, experts, capacity),
        [shape_of((3 * tok_rows, rows), jnp.bfloat16)]
        + [shape_of(source.shape, source.dtype) for source in sources[2:]],
        *sources,
        space=HBM,
        scratch=(
            pltpu.VMEM(ids.shape, jnp.int32),
            pltpu.VMEM(ids.shape, jnp.float32),
            pltpu.SemaphoreType.DMA((len(sources),)),
        ),
    )
    down_other = swap(down)
    second = onward(own_other)
    third = onward(first)
    first_other = swap(first)
    second_other = swap(second)
    third_other = swap(third)
    held = [
        (own, (0, 0)),
        (own_other, (0, 1)),
        (first, (-1, 0)),
        (first_other, (1, 1)),
        (second, (-1, 1)),
        (second_other, (1, 0)),
        (third, (-2, 0)),
        (third_other, (2, 1)),
    ]
    places = [where + (chips,) for _, where in held]
    early = 6
    wide = shape_of((rows, width), jnp.float32)
    flops = 4 * rows * width * width
    sums = call(
        functools.partial(first_kernel, places[:early]),
        [wide, wide, shape_of((rows, 128), jnp.float32)],
        *[piece for piece, _ in held[:early]],
        gate,
        up,
        limit=16,
        flops=early * flops,
    )
    act = call(
        functools.partial(last_kernel, places[early:]),
        narrow,
        *[piece for piece, _ in held[early:]],
        gate,
        up,
        *sums,
        limit=16,
        flops=(len(held) - early) * flops,
    )
    act_other = swap(act)
    wanted = [(2, 0, chips), (1, 1, chips), (1, 0, chips), (0, 0, chips)]
    far, near_other, near, kept = call(
        functools.partial(down_kernel, wanted),
        [narrow] * len(wanted),
        act,
        act_other,
        down,
        down_other,
        limit=16,
        flops=len(wanted) * flops,
    )
    far = onward(far)
    near_other = swap(onward(near_other))
    near = (near.astype(jnp.float32) + far.astype(jnp.float32)).astype(jnp.bfloat16)
    near = onward(near)
    total = functools.reduce(
        jnp.add, [part.astype(jnp.float32) for part in (kept, near_other, near)]
    )
    expert_out = total.astype(jnp.bfloat16).reshape(experts, capacity, width)
    returned = lax.all_to_all(expert_out, "ep", split_axis=0, concat_axis=0, tiled=True)
    mixture, squares = call(
        combine_kernel,
        [shape_of((tok_rows, width), jnp.float32), shape_of((peers, 8, 128), jnp.float32)],
        share,
        returned.reshape(rows, width),
    )
    squares = lax.all_to_all(squares, "tp", split_axis=0, concat_axis=0, tiled=True)
    return call(
        functools.partial(final_kernel, model_width),
        shape_of((tok_rows, width), jnp.bfloat16),
        mixture,
        squares,
        final_gain,
    )


def solution(mesh):
    placed = (
        P("ep", "tp"),
        P("tp"),
        P("ep", None),
        P("ep", None),
        P("ep", None, "tp"),
        P("ep", None, "tp"),
        P("ep", "tp", None),
        P("tp"),
    )

    return jax.shard_map(
        local, mesh=mesh, in_specs=placed, out_specs=P("ep", "tp"), check_vma=False
    )
```

profile of v0, /device:TPU:1, one launch (start us, length us, event | category | flops | bytes accessed | tf_op | source)
XLA Modules:
  0.0 86.3 jit_solution(13450706367814224321)
XLA Ops:
  0.0 1.1 %shard_map.83 = (bf16[512,256]{1,0:T(8,128)(2,1)S(1)}, f32[1,256]{1,0:T(1,128)S(1)}) custom-call(s32[4,64]{1,0:T(4,128)} %bitcast.18, bf16[64,256]{1,0:T(8,128)(2,1)} %tokens_hbm.1, f32[1,256]{1,0:T(1,128)} %bitcast.22), custom_call_target="tpu_custom_call" | custom-call | tf_op jit(solution)/shard_map/pallas_call | solution.py:212
  1.1 23.0 %all_to_all.15 = bf16[32,16,256]{2,1,0:T(8,128)(2,1)S(1)} all-to-all(bf16[32,16,256]{2,1,0:T(8,128)(2,1)S(1)} %bitcast.13), channel_id=1, replica_groups=mesh['ep'=32,'tp'=8] {'ep'}, dimensions={0} | all-to-all | bytes 524288 | tf_op jit(solution)/shard_map/all_to_all | solution.py:263
  24.0 0.3 shard_map.84.refs_0_
  24.3 2.5 %collective-permute-start.3 = (bf16[528,256]{1,0:T(8,128)(2,1)S(1)}, bf16[528,256]{1,0:T(8,128)(2,1)S(1)}, u32[]{:S(2)}, u32[]{:S(2)}) collective-permute-start(bf16[528,256]{1,0:T(8,128)(2,1)S(1)} %shard_map.84.refs_0_), channel_id=1, source_target_pairs={{0,1},{1,0},{2,3},{3,2},{4,5},{5,4},{6,7},{7,6},{8,9},{9,8},{10,11... | collective-permute-start | bytes 811016 | tf_op jit(solution)/shard_map/ppermute | solution.py:246
  26.9 2.7 %collective-permute-start = (bf16[528,256]{1,0:T(8,128)(2,1)S(1)}, bf16[528,256]{1,0:T(8,128)(2,1)S(1)}, u32[]{:S(2)}, u32[]{:S(2)}) collective-permute-start(bf16[528,256]{1,0:T(8,128)(2,1)S(1)} %shard_map.84.refs_0_), channel_id=1, source_target_pairs={{0,2},{1,7},{2,4},{3,1},{4,6},{5,3},{6,0},{7,5},{8,10},{9,15},{10,... | collective-permute-start | bytes 811016 | tf_op jit(solution)/shard_map/ppermute | solution.py:242
  29.6 2.0 %shard_map.82 = (bf16[192,512]{1,0:T(8,128)(2,1)S(1)}, f32[1,256]{1,0:T(1,128)S(1)}, bf16[2048,256]{1,0:T(8,128)(2,1)S(1)}, bf16[2048,256]{1,0:T(8,128)(2,1)S(1)}, bf16[256,2048]{1,0:T(8,128)(2,1)S(1)}) custom-call(s32[4,64]{1,0:T(4,128)} %bitcast.19, f32[4,64]{1,0:T(4,128)} %bitcast.20, f32[1,256]{1,0:T(1,128)} %bitcast.21, bf16[2048,256]{1,0:T(8,128)(2,1)} %bitcast.14, ...), custom_call_target="tpu_custom_call" | custom-call | tf_op jit(solution)/shard_map/pallas_call | solution.py:212
  31.6 0.1 collective-permute-start.8
  31.7 0.5 collective-permute-start.5
  32.2 0.8 collective-permute-done.refs_2_
  33.0 3.1 %collective-permute-start.1 = (bf16[528,256]{1,0:T(8,128)(2,1)S(1)}, bf16[528,256]{1,0:T(8,128)(2,1)S(1)}, u32[]{:S(2)}, u32[]{:S(2)}) collective-permute-start(bf16[528,256]{1,0:T(8,128)(2,1)S(1)} %collective-permute-done.refs_2_), channel_id=1, source_target_pairs={{0,2},{1,7},{2,4},{3,1},{4,6},{5,3},{6,0},{7,5},{8,10},{9,15},{10,... | collective-permute-start | bytes 811016 | tf_op jit(solution)/shard_map/ppermute | solution.py:242
  36.2 1.2 %collective-permute-done.5.refs_4_ = bf16[528,256]{1,0:T(8,128)(2,1)S(1)} collective-permute-done((bf16[528,256]{1,0:T(8,128)(2,1)S(1)}, bf16[528,256]{1,0:T(8,128)(2,1)S(1)}, u32[]{:S(2)}, u32[]{:S(2)}) %collective-permute-start.5) | collective-permute-done | bytes 270368 | tf_op jit(solution)/shard_map/ppermute | solution.py:242
  37.4 2.5 %collective-permute-start.6 = (bf16[528,256]{1,0:T(8,128)(2,1)S(1)}, bf16[528,256]{1,0:T(8,128)(2,1)S(1)}, u32[]{:S(2)}, u32[]{:S(2)}) collective-permute-start(bf16[528,256]{1,0:T(8,128)(2,1)S(1)} %collective-permute-done.5.refs_4_), channel_id=1, source_target_pairs={{0,1},{1,0},{2,3},{3,2},{4,5},{5,4},{6,7},{7,6},{8,9},{9,8},{10,11... | collective-permute-start | bytes 811016 | tf_op jit(solution)/shard_map/ppermute | solution.py:246
  39.9 0.4 collective-permute-done.1.refs_0_
  40.3 2.5 %collective-permute-start.2 = (bf16[528,256]{1,0:T(8,128)(2,1)S(1)}, bf16[528,256]{1,0:T(8,128)(2,1)S(1)}, u32[]{:S(2)}, u32[]{:S(2)}) collective-permute-start(bf16[528,256]{1,0:T(8,128)(2,1)S(1)} %collective-permute-done.1.refs_0_), channel_id=1, source_target_pairs={{0,1},{1,0},{2,3},{3,2},{4,5},{5,4},{6,7},{7,6},{8,9},{9,8},{10,11... | collective-permute-start | bytes 811016 | tf_op jit(solution)/shard_map/ppermute | solution.py:246
  42.8 1.2 %shard_map.85 = (f32[512,256]{1,0:T(8,128)S(1)}, f32[512,256]{1,0:T(8,128)S(1)}, f32[512,128]{1,0:T(8,128)S(1)}) custom-call(bf16[528,256]{1,0:T(8,128)(2,1)S(1)} %shard_map.84.refs_0_, bf16[528,256]{1,0:T(8,128)(2,1)S(1)} %collective-permute-done.3.refs_1_, bf16[528,256]{1,0:T(8,128)(2,1)S(1)} %collective-permute-done.refs_2_, ...), custom_call_target="tpu_custom_call" | custom-call | flops 805306368 | tf_op jit(solution)/shard_map/pallas_call | solution.py:212
  44.0 0.7 shard_map.86.own_ref
  44.7 0.4 collective-permute-start.7
  45.1 1.2 %collective-permute-done.7.other_ref = bf16[512,256]{1,0:T(8,128)(2,1)S(1)} collective-permute-done((bf16[512,256]{1,0:T(8,128)(2,1)S(1)}, bf16[512,256]{1,0:T(8,128)(2,1)S(1)}, u32[]{:S(2)}, u32[]{:S(2)}) %collective-permute-start.7) | collective-permute-done | bytes 262176 | tf_op jit(solution)/shard_map/ppermute | solution.py:246
  46.3 0.7 shard_map.87
  47.1 0.3 collective-permute-start.11
  47.4 0.1 collective-permute-start.9
  47.5 5.2 %collective-permute-done.11 = bf16[512,256]{1,0:T(8,128)(2,1)S(1)} collective-permute-done((bf16[512,256]{1,0:T(8,128)(2,1)S(1)}, bf16[512,256]{1,0:T(8,128)(2,1)S(1)}, u32[]{:S(2)}, u32[]{:S(2)}) %collective-permute-start.11) | collective-permute-done | bytes 262176 | tf_op jit(solution)/shard_map/ppermute | solution.py:242
  52.7 1.2 %collective-permute-start.12 = (bf16[512,256]{1,0:T(8,128)(2,1)S(1)}, bf16[512,256]{1,0:T(8,128)(2,1)S(1)}, u32[]{:S(2)}, u32[]{:S(2)}) collective-permute-start(bf16[512,256]{1,0:T(8,128)(2,1)S(1)} %add_convert_fusion.1), channel_id=1, source_target_pairs={{0,2},{1,7},{2,4},{3,1},{4,6},{5,3},{6,0},{7,5},{8,10},{9,15},{10,... | collective-permute-start | bytes 786440 | tf_op jit(solution)/shard_map/ppermute | solution.py:242
  53.9 1.5 %collective-permute-done.9 = bf16[512,256]{1,0:T(8,128)(2,1)S(1)} collective-permute-done((bf16[512,256]{1,0:T(8,128)(2,1)S(1)}, bf16[512,256]{1,0:T(8,128)(2,1)S(1)}, u32[]{:S(2)}, u32[]{:S(2)}) %collective-permute-start.9) | collective-permute-done | bytes 262176 | tf_op jit(solution)/shard_map/ppermute | solution.py:242
  55.5 2.4 %collective-permute-start.10 = (bf16[512,256]{1,0:T(8,128)(2,1)S(1)}, bf16[512,256]{1,0:T(8,128)(2,1)S(1)}, u32[]{:S(2)}, u32[]{:S(2)}) collective-permute-start(bf16[512,256]{1,0:T(8,128)(2,1)S(1)} %collective-permute-done.9), channel_id=1, source_target_pairs={{0,1},{1,0},{2,3},{3,2},{4,5},{5,4},{6,7},{7,6},{8,9},{9,8},{10,11... | collective-permute-start | bytes 786440 | tf_op jit(solution)/shard_map/ppermute | solution.py:246
  57.8 0.2 collective-permute-done.12
  58.0 1.0 %collective-permute-done.10 = bf16[512,256]{1,0:T(8,128)(2,1)S(1)} collective-permute-done((bf16[512,256]{1,0:T(8,128)(2,1)S(1)}, bf16[512,256]{1,0:T(8,128)(2,1)S(1)}, u32[]{:S(2)}, u32[]{:S(2)}) %collective-permute-start.10) | collective-permute-done | bytes 262176 | tf_op jit(solution)/shard_map/ppermute | solution.py:246
  59.0 0.1 add_convert_fusion
  59.1 13.9 %all_to_all.16 = bf16[32,16,256]{2,1,0:T(8,128)(2,1)S(1)} all-to-all(bf16[32,16,256]{2,1,0:T(8,128)(2,1)S(1)} %bitcast.17), channel_id=1, replica_groups=mesh['ep'=32,'tp'=8] {'ep'}, dimensions={0} | all-to-all | bytes 524288 | tf_op jit(solution)/shard_map/all_to_all | solution.py:342
  73.0 0.4 shard_map.88
  73.4 12.2 %all_to_all.17.squares_ref = f32[8,8,128]{2,1,0:T(8,128)S(1)} all-to-all(f32[8,8,128]{2,1,0:T(8,128)S(1)} %get-tuple-element.35), channel_id=1, replica_groups=mesh['ep'=32,'tp'=8] {'tp'}, dimensions={0} | all-to-all | bytes 65536 | tf_op jit(solution)/shard_map/all_to_all | solution.py:349
  85.6 0.7 shard_map.89
  (7 shorter events, 0.1 us)
Async XLA Ops:
  24.3 7.3 %collective-permute-start.3 = (bf16[528,256]{1,0:T(8,128)(2,1)S(1)}, bf16[528,256]{1,0:T(8,128)(2,1)S(1)}, u32[]{:S(2)}, u32[]{:S(2)}) collective-permute-start(bf16[528,256]{1,0:T(8,128)(2,1)S(1)} %shard_map.84.refs_0_), channel_id=1, source_target_pairs={{0,1},{1,0},{2,3},{3,2},{4,5},{5,4},{6,7},{7,6},{8,9},{9,8},{10,11... | collective-permute-start | bytes 811016 | tf_op jit(solution)/shard_map/ppermute | solution.py:246
  26.9 6.1 %collective-permute-start = (bf16[528,256]{1,0:T(8,128)(2,1)S(1)}, bf16[528,256]{1,0:T(8,128)(2,1)S(1)}, u32[]{:S(2)}, u32[]{:S(2)}) collective-permute-start(bf16[528,256]{1,0:T(8,128)(2,1)S(1)} %shard_map.84.refs_0_), channel_id=1, source_target_pairs={{0,2},{1,7},{2,4},{3,1},{4,6},{5,3},{6,0},{7,5},{8,10},{9,15},{10,... | collective-permute-start | bytes 811016 | tf_op jit(solution)/shard_map/ppermute | solution.py:242
  31.6 13.5 %collective-permute-start.8 = (bf16[256,2048]{1,0:T(8,128)(2,1)S(1)}, bf16[256,2048]{1,0:T(8,128)(2,1)S(1)}, u32[]{:S(2)}, u32[]{:S(2)}) collective-permute-start(bf16[256,2048]{1,0:T(8,128)(2,1)S(1)} %get-tuple-element.29.down_ref), channel_id=1, source_target_pairs={{0,1},{1,0},{2,3},{3,2},{4,5},{5,4},{6,7},{7,6},{8,9},{9,8},{10,11... | collective-permute-start | bytes 3145736 | tf_op jit(solution)/shard_map/ppermute | solution.py:246
  31.7 5.7 %collective-permute-start.5 = (bf16[528,256]{1,0:T(8,128)(2,1)S(1)}, bf16[528,256]{1,0:T(8,128)(2,1)S(1)}, u32[]{:S(2)}, u32[]{:S(2)}) collective-permute-start(bf16[528,256]{1,0:T(8,128)(2,1)S(1)} %collective-permute-done.3.refs_1_), channel_id=1, source_target_pairs={{0,2},{1,7},{2,4},{3,1},{4,6},{5,3},{6,0},{7,5},{8,10},{9,15},{10,... | collective-permute-start | bytes 811016 | tf_op jit(solution)/shard_map/ppermute | solution.py:242
  33.0 7.2 %collective-permute-start.1 = (bf16[528,256]{1,0:T(8,128)(2,1)S(1)}, bf16[528,256]{1,0:T(8,128)(2,1)S(1)}, u32[]{:S(2)}, u32[]{:S(2)}) collective-permute-start(bf16[528,256]{1,0:T(8,128)(2,1)S(1)} %collective-permute-done.refs_2_), channel_id=1, source_target_pairs={{0,2},{1,7},{2,4},{3,1},{4,6},{5,3},{6,0},{7,5},{8,10},{9,15},{10,... | collective-permute-start | bytes 811016 | tf_op jit(solution)/shard_map/ppermute | solution.py:242
  36.2 6.6 %collective-permute-start.4 = (bf16[528,256]{1,0:T(8,128)(2,1)S(1)}, bf16[528,256]{1,0:T(8,128)(2,1)S(1)}, u32[]{:S(2)}, u32[]{:S(2)}) collective-permute-start(bf16[528,256]{1,0:T(8,128)(2,1)S(1)} %collective-permute-done.refs_2_), channel_id=1, source_target_pairs={{0,1},{1,0},{2,3},{3,2},{4,5},{5,4},{6,7},{7,6},{8,9},{9,8},{10,11... | collective-permute-start | bytes 811016 | tf_op jit(solution)/shard_map/ppermute | solution.py:246
  37.4 5.4 %collective-permute-start.6 = (bf16[528,256]{1,0:T(8,128)(2,1)S(1)}, bf16[528,256]{1,0:T(8,128)(2,1)S(1)}, u32[]{:S(2)}, u32[]{:S(2)}) collective-permute-start(bf16[528,256]{1,0:T(8,128)(2,1)S(1)} %collective-permute-done.5.refs_4_), channel_id=1, source_target_pairs={{0,1},{1,0},{2,3},{3,2},{4,5},{5,4},{6,7},{7,6},{8,9},{9,8},{10,11... | collective-permute-start | bytes 811016 | tf_op jit(solution)/shard_map/ppermute | solution.py:246
  40.3 3.7 %collective-permute-start.2 = (bf16[528,256]{1,0:T(8,128)(2,1)S(1)}, bf16[528,256]{1,0:T(8,128)(2,1)S(1)}, u32[]{:S(2)}, u32[]{:S(2)}) collective-permute-start(bf16[528,256]{1,0:T(8,128)(2,1)S(1)} %collective-permute-done.1.refs_0_), channel_id=1, source_target_pairs={{0,1},{1,0},{2,3},{3,2},{4,5},{5,4},{6,7},{7,6},{8,9},{9,8},{10,11... | collective-permute-start | bytes 811016 | tf_op jit(solution)/shard_map/ppermute | solution.py:246
  44.7 1.6 %collective-permute-start.7 = (bf16[512,256]{1,0:T(8,128)(2,1)S(1)}, bf16[512,256]{1,0:T(8,128)(2,1)S(1)}, u32[]{:S(2)}, u32[]{:S(2)}) collective-permute-start(bf16[512,256]{1,0:T(8,128)(2,1)S(1)} %shard_map.86.own_ref), channel_id=1, source_target_pairs={{0,1},{1,0},{2,3},{3,2},{4,5},{5,4},{6,7},{7,6},{8,9},{9,8},{10,11... | collective-permute-start | bytes 786440 | tf_op jit(solution)/shard_map/ppermute | solution.py:246
  47.1 5.6 %collective-permute-start.11 = (bf16[512,256]{1,0:T(8,128)(2,1)S(1)}, bf16[512,256]{1,0:T(8,128)(2,1)S(1)}, u32[]{:S(2)}, u32[]{:S(2)}) collective-permute-start(bf16[512,256]{1,0:T(8,128)(2,1)S(1)} %get-tuple-element.33), channel_id=1, source_target_pairs={{0,2},{1,7},{2,4},{3,1},{4,6},{5,3},{6,0},{7,5},{8,10},{9,15},{10,... | collective-permute-start | bytes 786440 | tf_op jit(solution)/shard_map/ppermute | solution.py:242
  47.4 8.1 %collective-permute-start.9 = (bf16[512,256]{1,0:T(8,128)(2,1)S(1)}, bf16[512,256]{1,0:T(8,128)(2,1)S(1)}, u32[]{:S(2)}, u32[]{:S(2)}) collective-permute-start(bf16[512,256]{1,0:T(8,128)(2,1)S(1)} %get-tuple-element.31), channel_id=1, source_target_pairs={{0,2},{1,7},{2,4},{3,1},{4,6},{5,3},{6,0},{7,5},{8,10},{9,15},{10,... | collective-permute-start | bytes 786440 | tf_op jit(solution)/shard_map/ppermute | solution.py:242
  52.7 5.3 %collective-permute-start.12 = (bf16[512,256]{1,0:T(8,128)(2,1)S(1)}, bf16[512,256]{1,0:T(8,128)(2,1)S(1)}, u32[]{:S(2)}, u32[]{:S(2)}) collective-permute-start(bf16[512,256]{1,0:T(8,128)(2,1)S(1)} %add_convert_fusion.1), channel_id=1, source_target_pairs={{0,2},{1,7},{2,4},{3,1},{4,6},{5,3},{6,0},{7,5},{8,10},{9,15},{10,... | collective-permute-start | bytes 786440 | tf_op jit(solution)/shard_map/ppermute | solution.py:242
  55.5 3.5 %collective-permute-start.10 = (bf16[512,256]{1,0:T(8,128)(2,1)S(1)}, bf16[512,256]{1,0:T(8,128)(2,1)S(1)}, u32[]{:S(2)}, u32[]{:S(2)}) collective-permute-start(bf16[512,256]{1,0:T(8,128)(2,1)S(1)} %collective-permute-done.9), channel_id=1, source_target_pairs={{0,1},{1,0},{2,3},{3,2},{4,5},{5,4},{6,7},{7,6},{8,9},{9,8},{10,11... | collective-permute-start | bytes 786440 | tf_op jit(solution)/shard_map/ppermute | solution.py:246
where the time goes:
time: 86.5 us; the launch traced here: 86.3 us
  blocking collectives  49 us (57%)
  starting transfers between devices  18.4 us (21%)
  waiting for transfers between devices  11.6 us (13%)
  Pallas kernels  7.06 us (8%)
    all_to_all x1, blocking collectives, local(): lax.all_to_all(outbound.reshape(experts, capacity, width), 'ep', split_ax...  23 us
    all_to_all x1, blocking collectives, local(): lax.all_to_all(expert_out, 'ep', split_axis=0, concat_axis=0, tiled=True)  13.9 us
    all_to_all x1, blocking collectives, local(): lax.all_to_all(squares, 'tp', split_axis=0, concat_axis=0, tiled=True)  12.2 us
    ppermute x7, starting transfers between devices, swap(): return lax.ppermute(value, 'tp', pairs)  10.3 us
    ppermute x6, waiting for transfers between devices, onward(): return lax.ppermute(value, 'tp', pairs)  9.35 us
    ppermute x6, starting transfers between devices, onward(): return lax.ppermute(value, 'tp', pairs)  8.01 us
    pallas_call x8, Pallas kernels, call(): pl.pallas_call(kernel, out_shape=outs, in_specs=[space] * len(args), out_...  7.06 us
    ppermute x7, waiting for transfers between devices, swap(): return lax.ppermute(value, 'tp', pairs)  2.21 us
  transfers between devices with their start and end apart: 13, of which 8 were waited for; matrix products, arithmetic and copies ran while one was open for 0% of the time, Pallas kernels for 4%

commit v1 on v0

--- a/solution.py
+++ b/solution.py
@@ -72,9 +72,10 @@
 
 
 def load_kernel(experts, capacity, *refs):
-    ids_hbm, weights_hbm, *sources = refs[:6]
-    share_ref, *targets = refs[6:11]
-    ids_ref, weights_ref, sems = refs[11:]
+    *refs, ids_ref, weights_ref, sems = refs
+    count = (len(refs) + 1) // 2
+    ids_hbm, weights_hbm, *sources = refs[:count]
+    share_ref, *targets = refs[count:]
     pairs = [(ids_hbm, ids_ref), (weights_hbm, weights_ref), *zip(sources, targets)]
     copies = [pltpu.make_async_copy(*pair, sems.at[i]) for i, pair in enumerate(pairs)]
     for copy in copies:
@@ -94,10 +95,14 @@
         copy.wait()
 
 
-def mid_kernel(rows_ref, gain_ref, out_ref):
+def mid_kernel(rows_ref, gain_ref, out_ref, out_a_ref, out_b_ref):
     rows, width = rows_ref.shape
+    half = rows // 2
     x = rows_ref[...].astype(jnp.float32)
-    out_ref[0:rows, :] = (x * gain_ref[...]).astype(jnp.bfloat16)
+    scaled = (x * gain_ref[...]).astype(jnp.bfloat16)
+    out_ref[0:rows, :] = scaled
+    out_a_ref[0:half, :] = scaled[:half]
+    out_b_ref[...] = scaled[half:]
     hi, mid, _ = split3(x * x)
     ones = jnp.ones((8, width), jnp.bfloat16)
     sums = dot_t(ones, hi) + dot_t(ones, mid)
@@ -112,7 +117,9 @@
                 jnp.where(row == 1, pieces[1], jnp.where(row == 2, pieces[2], 0.0)),
             )
         )
-    out_ref[rows : rows + TAIL, :] = jnp.concatenate(tail, axis=0).astype(jnp.bfloat16)
+    tail = jnp.concatenate(tail, axis=0).astype(jnp.bfloat16)
+    out_ref[rows : rows + TAIL, :] = tail
+    out_a_ref[half : half + TAIL, :] = tail
 
 
 def ahead(step, other, chips):
@@ -121,62 +128,88 @@
     return (me // CORES + step * (1 - 2 * core) + chips) % chips * CORES + (core + other) % CORES
 
 
-def products(part, width, places, pieces, gate_ref, up_ref, gate, up, squares):
-    rows = pieces[0].shape[0] - TAIL
-    at = part * width
+def products(part, pieces, gate_ref, up_ref, gate, up, squares):
+    width = gate_ref.shape[1]
     row = lax.broadcasted_iota(jnp.int32, (TAIL, 128), 0)
     ones = jnp.where(row // 8 == part, 1.0, 0.0).astype(jnp.bfloat16)
-    for where, piece in zip(places, pieces):
+    for where, refs in pieces:
         from_row = pl.ds(pl.multiple_of(ahead(*where) * width, width), width)
-        x = piece[at : at + width, :]
+        at = part * width if len(refs) == 1 else 0
+        x = refs[part if len(refs) > 1 else 0][at : at + width, :]
+        end = refs[0].shape[0]
         gate += jnp.dot(x, gate_ref[from_row, :], preferred_element_type=jnp.float32)
         up += jnp.dot(x, up_ref[from_row, :], preferred_element_type=jnp.float32)
-        squares += dot_0(piece[rows : rows + TAIL, :], ones)
+        squares += dot_0(refs[0][end - TAIL : end, :], ones)
     return gate, up, squares
 
 
-def first_kernel(places, *refs):
-    count = len(places)
-    gate_ref, up_ref, gate_out, up_out, squares_out = refs[count:]
+def grouped(places, sizes, refs):
+    pieces, at = [], 0
+    for where, size in zip(places, sizes):
+        pieces.append((where, refs[at : at + size]))
+        at += size
+    return pieces, refs[at:]
+
+
+def first_kernel(places, sizes, *refs):
+    pieces, (gate_ref, up_ref, gate_out, up_out, squares_out) = grouped(places, sizes, refs)
     width = gate_ref.shape[1]
     for part in range(gate_out.shape[0] // width):
         at = slice(part * width, (part + 1) * width)
         zero = jnp.zeros((width, width), jnp.float32)
-        gate, up, squares = products(
-            part, width, places, refs[:count], gate_ref, up_ref, zero, zero, zero[:, :128]
-        )
+        gate, up, squares = products(part, pieces, gate_ref, up_ref, zero, zero, zero[:, :128])
         gate_out[at, :] = gate
         up_out[at, :] = up
         squares_out[at, :] = squares
 
 
-def last_kernel(places, *refs):
-    count = len(places)
-    gate_ref, up_ref, gate_in, up_in, squares_in, act_ref = refs[count:]
+def last_kernel(places, sizes, part, *refs):
+    pieces, refs = grouped(places, sizes, refs)
+    gate_ref, up_ref, gate_in, up_in, squares_in, act_ref = refs
     model_width, width = gate_ref.shape
-    for part in range(gate_in.shape[0] // width):
-        at = slice(part * width, (part + 1) * width)
-        gate, up, squares = products(
-            part, width, places, refs[:count], gate_ref, up_ref,
-            gate_in[at, :], up_in[at, :], squares_in[at, :],
-        )
-        scale = lax.rsqrt(squares / model_width + EPSILON)
-        scale = jnp.concatenate([scale] * (width // 128), axis=1)
-        gate = jnp.minimum(gate * scale, CLAMP_LIMIT)
-        up = jnp.clip(up * scale, -CLAMP_LIMIT, CLAMP_LIMIT)
-        act = (up + 1.0) * gate * jax.nn.sigmoid(SIGMOID_SLOPE * gate)
-        act_ref[at, :] = act.astype(jnp.bfloat16)
-
-
-def down_kernel(places, own_ref, other_ref, down_ref, down_other_ref, *outs):
+    at = slice(part * width, (part + 1) * width)
+    gate, up, squares = products(
+        part, pieces, gate_ref, up_ref, gate_in[at, :], up_in[at, :], squares_in[at, :]
+    )
+    scale = lax.rsqrt(squares / model_width + EPSILON)
+    scale = jnp.concatenate([scale] * (width // 128), axis=1)
+    gate = jnp.minimum(gate * scale, CLAMP_LIMIT)
+    up = jnp.clip(up * scale, -CLAMP_LIMIT, CLAMP_LIMIT)
+    act = (up + 1.0) * gate * jax.nn.sigmoid(SIGMOID_SLOPE * gate)
+    act_ref[...] = act.astype(jnp.bfloat16)
+
+
+def down_part(where, own_ref, other_ref, down_ref, down_other_ref):
     width = own_ref.shape[1]
-    for where, out in zip(places, outs):
-        columns = pl.ds(pl.multiple_of(ahead(*where) * width, width), width)
-        total = jnp.dot(own_ref[...], down_ref[:, columns], preferred_element_type=jnp.float32)
-        total += jnp.dot(
-            other_ref[...], down_other_ref[:, columns], preferred_element_type=jnp.float32
-        )
-        out[...] = total.astype(jnp.bfloat16)
+    columns = pl.ds(pl.multiple_of(ahead(*where) * width, width), width)
+    total = jnp.dot(own_ref[...], down_ref[:, columns], preferred_element_type=jnp.float32)
+    total += jnp.dot(
+        other_ref[...], down_other_ref[:, columns], preferred_element_type=jnp.float32
+    )
+    return total.astype(jnp.bfloat16)
+
+
+def far_kernel(where, own_ref, other_ref, down_ref, down_other_ref, out_ref):
+    out_ref[...] = down_part(where, own_ref, other_ref, down_ref, down_other_ref)
+
+
+def rest_kernel(chips, *refs):
+    acts, weights, (other_ref, near_a_ref, near_b_ref, kept_ref) = refs[:4], refs[4:6], refs[6:]
+    for part in range(2):
+        half = acts[2 * part : 2 * part + 2]
+        at = slice(part * half[0].shape[0], (part + 1) * half[0].shape[0])
+        other_ref[at, :] = down_part((1, 1, chips), *half, *weights)
+        near_ref = near_b_ref if part else near_a_ref
+        near_ref[...] = down_part((1, 0, chips), *half, *weights)
+        kept_ref[at, :] = down_part((0, 0, chips), *half, *weights)
+
+
+def sum_kernel(kept_ref, other_ref, near_a_ref, near_b_ref, out_ref):
+    half = near_a_ref.shape[0]
+    for part, near_ref in enumerate((near_a_ref, near_b_ref)):
+        at = slice(part * half, (part + 1) * half)
+        total = kept_ref[at, :].astype(jnp.float32) + other_ref[at, :].astype(jnp.float32)
+        out_ref[at, :] = (total + near_ref[...].astype(jnp.float32)).astype(jnp.bfloat16)
 
 
 def combine_kernel(share_ref, rows_ref, mix_ref, squares_ref):
@@ -188,7 +221,7 @@
     sums = functools.reduce(jnp.add, [dot_t(ones, part) for part in split3(mix * mix)])
     sums = jnp.concatenate([sums, jnp.zeros_like(sums)], axis=1)
     for i in range(squares_ref.shape[0]):
-        squares_ref[i] = sums
+        squares_ref[i] = sums[0:1]
 
 
 def final_kernel(model_width, mix_ref, squares_ref, gain_ref, out_ref):
@@ -197,7 +230,7 @@
         total += squares_ref[i]
     mix = mix_ref[...]
     tokens = mix.shape[0]
-    wide = jnp.concatenate([total] * (tokens // 8), axis=0)
+    wide = jnp.broadcast_to(total, (tokens, total.shape[1]))
     row = lax.broadcasted_iota(jnp.int32, wide.shape, 0)
     lane = lax.broadcasted_iota(jnp.int32, wide.shape, 1)
     column = jnp.sum(jnp.where(row == lane, wide, 0.0), axis=1, keepdims=True)
@@ -263,12 +296,24 @@
     received = lax.all_to_all(
         outbound.reshape(experts, capacity, width), "ep", split_axis=0, concat_axis=0, tiled=True
     ).reshape(rows, width)
-    own = call(mid_kernel, shape_of((rows + TAIL, width), jnp.bfloat16), received, gain)
-
-    first = onward(own)
+    half = rows // 2
+    whole, head, rest = [
+        shape_of((n, width), jnp.bfloat16) for n in (rows + TAIL, half + TAIL, half)
+    ]
+    own, own_a, own_b = call(mid_kernel, [whole, head, rest], received, gain)
+
+    first_a = onward(own_a)
     own_other = swap(own)
-    sources = (ids, route_weights.T, final_gain[None, :], gate_proj[0], up_proj[0], down_proj[0])
-    share, final_gain, gate, up, down = call(
+    first_b = onward(own_b)
+    second = onward(own_other)
+    third_a = onward(first_a)
+    third_b = onward(first_b)
+    first_other = (swap(first_a), swap(first_b))
+    second_other = swap(second)
+    third_other_a = swap(third_a)
+    third_other_b = swap(third_b)
+    sources = (ids, route_weights.T, final_gain[None, :], up_proj[0])
+    share, final_gain, up = call(
         functools.partial(load_kernel, experts, capacity),
         [shape_of((3 * tok_rows, rows), jnp.bfloat16)]
         + [shape_of(source.shape, source.dtype) for source in sources[2:]],
@@ -280,69 +325,87 @@
             pltpu.SemaphoreType.DMA((len(sources),)),
         ),
     )
+    gate, down = gate_proj[0], down_proj[0]
     down_other = swap(down)
-    second = onward(own_other)
-    third = onward(first)
-    first_other = swap(first)
-    second_other = swap(second)
-    third_other = swap(third)
-    held = [
-        (own, (0, 0)),
-        (own_other, (0, 1)),
-        (first, (-1, 0)),
-        (first_other, (1, 1)),
-        (second, (-1, 1)),
-        (second_other, (1, 0)),
-        (third, (-2, 0)),
-        (third_other, (2, 1)),
+    early = [
+        ((0, 0, chips), (own,)),
+        ((0, 1, chips), (own_other,)),
+        ((-1, 0, chips), (first_a, first_b)),
+        ((1, 1, chips), first_other),
+        ((-1, 1, chips), (second,)),
+        ((1, 0, chips), (second_other,)),
     ]
-    places = [where + (chips,) for _, where in held]
-    early = 6
+    late = [(-2, 0, chips), (2, 1, chips)]
     wide = shape_of((rows, width), jnp.float32)
     flops = 4 * rows * width * width
     sums = call(
-        functools.partial(first_kernel, places[:early]),
+        functools.partial(
+            first_kernel, [where for where, _ in early], [len(held) for _, held in early]
+        ),
         [wide, wide, shape_of((rows, 128), jnp.float32)],
-        *[piece for piece, _ in held[:early]],
+        *[part for _, held in early for part in held],
         gate,
         up,
         limit=16,
-        flops=early * flops,
-    )
-    act = call(
-        functools.partial(last_kernel, places[early:]),
-        narrow,
-        *[piece for piece, _ in held[early:]],
-        gate,
-        up,
-        *sums,
-        limit=16,
-        flops=(len(held) - early) * flops,
-    )
-    act_other = swap(act)
-    wanted = [(2, 0, chips), (1, 1, chips), (1, 0, chips), (0, 0, chips)]
-    far, near_other, near, kept = call(
-        functools.partial(down_kernel, wanted),
-        [narrow] * len(wanted),
-        act,
-        act_other,
+        flops=len(early) * flops,
+    )
+
+    def last(part, *held):
+        act = call(
+            functools.partial(last_kernel, late, [len(held) // 2] * 2, part),
+            rest,
+            *held,
+            gate,
+            up,
+            *sums,
+            limit=16,
+            flops=flops,
+        )
+        return act, swap(act)
+
+    act_a = last(0, third_a, third_other_a)
+    act_b = last(1, third_a, third_b, third_other_a, third_other_b)
+
+    def far(acts):
+        out = call(
+            functools.partial(far_kernel, (2, 0, chips)),
+            rest,
+            *acts,
+            down,
+            down_other,
+            limit=16,
+            flops=flops // 2,
+        )
+        return onward(out)
+
+    far_a = far(act_a)
+    far_b = far(act_b)
+    narrow = shape_of((rows, width), jnp.bfloat16)
+    near_other, near_a, near_b, kept = call(
+        functools.partial(rest_kernel, chips),
+        [narrow, rest, rest, narrow],
+        *act_a,
+        *act_b,
         down,
         down_other,
         limit=16,
-        flops=len(wanted) * flops,
-    )
-    far = onward(far)
-    near_other = swap(onward(near_other))
-    near = (near.astype(jnp.float32) + far.astype(jnp.float32)).astype(jnp.bfloat16)
-    near = onward(near)
-    total = functools.reduce(
-        jnp.add, [part.astype(jnp.float32) for part in (kept, near_other, near)]
-    )
-    expert_out = total.astype(jnp.bfloat16).reshape(experts, capacity, width)
+        flops=3 * flops,
+    )
+    near_other = onward(near_other)
+
+    def near(mine, came):
+        total = mine.astype(jnp.float32) + came.astype(jnp.float32)
+        return onward(total.astype(jnp.bfloat16))
+
+    near_a = near(near_a, far_a)
+    near_b = near(near_b, far_b)
+    near_other = swap(near_other)
+    total = call(sum_kernel, narrow, kept, near_other, near_a, near_b)
+    expert_out = total.reshape(experts, capacity, width)
     returned = lax.all_to_all(expert_out, "ep", split_axis=0, concat_axis=0, tiled=True)
     mixture, squares = call(
         combine_kernel,
-        [shape_of((tok_rows, width), jnp.float32), shape_of((peers, 8, 128), jnp.float32)],
+        [shape_of((tok_rows, width), jnp.float32), shape_of((peers, 1, 128), jnp.float32)],
         share,
         returned.reshape(rows, width),
     )

time: 86.5 us -> 93.2 us (1.077)
  blocking collectives: 49 us -> 26 us
  starting transfers between devices: 18.4 us -> 35.6 us
  waiting for transfers between devices: 11.6 us -> 23.2 us
    all_to_all x1 -> x0, blocking collectives: 23 us -> none  [local(): lax.all_to_all(outbound.reshape(experts, capacity, width), 'ep', split_ax...]
    all_to_all x0 -> x1, starting transfers between devices: none -> 11.9 us  [local(): lax.all_to_all(outbound.reshape(experts, capacity, width), 'ep', split_ax...]
    all_to_all x0 -> x1, waiting for transfers between devices: none -> 10.3 us  [local(): lax.all_to_all(outbound.reshape(experts, capacity, width), 'ep', split_ax...]
    ppermute x7 -> x10, starting transfers between devices: 10.3 us -> 13.5 us  [swap(): return lax.ppermute(value, 'tp', pairs)]
    ppermute x6 -> x10, starting transfers between devices: 8.01 us -> 10.2 us  [onward(): return lax.ppermute(value, 'tp', pairs)]
    ppermute x6 -> x10, waiting for transfers between devices: 9.35 us -> 11.5 us  [onward(): return lax.ppermute(value, 'tp', pairs)]
    pallas_call x8 -> x12, Pallas kernels: 7.06 us -> 7.86 us  [call(): pl.pallas_call(kernel, out_shape=outs, in_specs=[space] * len(args), out_...]
    ppermute x7 -> x10, waiting for transfers between devices: 2.21 us -> 1.48 us  [swap(): return lax.ppermute(value, 'tp', pairs)]
  transfers between devices with their start and end apart: 13 -> 21, of which waited for: 8 -> 8; matrix products, arithmetic and copies ran while one was open for 0% -> 0% of each run, Pallas kernels for 4% -> 5%
where the time goes in v1:
time: 93.2 us; the launch traced here: 92.9 us
  starting transfers between devices  35.6 us (38%)
  blocking collectives  26 us (28%)
  waiting for transfers between devices  23.2 us (25%)
  Pallas kernels  7.86 us (8%)
    all_to_all x1, blocking collectives, local(): lax.all_to_all(expert_out, 'ep', split_axis=0, concat_axis=0, tiled=True)  13.9 us
    ppermute x10, starting transfers between devices, swap(): return lax.ppermute(value, 'tp', pairs)  13.5 us
    all_to_all x1, blocking collectives, local(): lax.all_to_all(squares, 'tp', split_axis=0, concat_axis=0, tiled=True)  12 us
    all_to_all x1, starting transfers between devices, local(): lax.all_to_all(outbound.reshape(experts, capacity, width), 'ep', split_ax...  11.9 us
    ppermute x10, waiting for transfers between devices, onward(): return lax.ppermute(value, 'tp', pairs)  11.5 us
    all_to_all x1, waiting for transfers between devices, local(): lax.all_to_all(outbound.reshape(experts, capacity, width), 'ep', split_ax...  10.3 us
    ppermute x10, starting transfers between devices, onward(): return lax.ppermute(value, 'tp', pairs)  10.2 us
    pallas_call x12, Pallas kernels, call(): pl.pallas_call(kernel, out_shape=outs, in_specs=[space] * len(args), out_...  7.86 us
  transfers between devices with their start and end apart: 21, of which 8 were waited for; matrix products, arithmetic and copies ran while one was open for 0% of the time, Pallas kernels for 5%

profile of v1, /device:TPU:1, one launch (start us, length us, event | category | flops | bytes accessed | tf_op | source)
XLA Modules:
  0.0 92.9 jit_solution(8764189505173793148)
XLA Ops:
  0.0 1.9 %shard_map.83 = (bf16[512,256]{1,0:T(8,128)(2,1)}, f32[1,256]{1,0:T(1,128)S(1)}) custom-call(s32[4,64]{1,0:T(4,128)} %bitcast.22, bf16[64,256]{1,0:T(8,128)(2,1)} %tokens_hbm.1, f32[1,256]{1,0:T(1,128)} %bitcast.26), custom_call_target="tpu_custom_call" | custom-call | tf_op jit(solution)/shard_map/pallas_call | solution.py:245
  1.9 11.9 %all-to-all-start = ((bf16[32,16,256]{2,1,0:T(8,128)(2,1)}), bf16[32,16,256]{2,1,0:T(8,128)(2,1)S(1)}, u32[]{:S(2)}, u32[]{:S(2)}) async-start(bf16[32,16,256]{2,1,0:T(8,128)(2,1)} %bitcast.5), calls=%async_computation | async-start | bytes 524288 | tf_op jit(solution)/shard_map/all_to_all | solution.py:296
  13.7 1.0 %collective-permute-start.13 = (bf16[256,2048]{1,0:T(8,128)(2,1)}, bf16[256,2048]{1,0:T(8,128)(2,1)S(1)}, u32[]{:S(2)}, u32[]{:S(2)}) collective-permute-start(bf16[256,2048]{1,0:T(8,128)(2,1)} %bitcast.11), channel_id=1, source_target_pairs={{0,1},{1,0},{2,3},{3,2},{4,5},{5,4},{6,7},{7,6},{8,9},{9,8},{10,11... | collective-permute-start | bytes 3145736 | tf_op jit(solution)/shard_map/ppermute | solution.py:279
  14.8 10.3 %all-to-all-done = bf16[32,16,256]{2,1,0:T(8,128)(2,1)S(1)} async-done(((bf16[32,16,256]{2,1,0:T(8,128)(2,1)}), bf16[32,16,256]{2,1,0:T(8,128)(2,1)S(1)}, u32[]{:S(2)}, u32[]{:S(2)}) %all-to-all-start) | async-done | bytes 262176 | tf_op jit(solution)/shard_map/all_to_all | solution.py:296
  25.4 2.5 %collective-permute-start.3 = (bf16[528,256]{1,0:T(8,128)(2,1)S(1)}, bf16[528,256]{1,0:T(8,128)(2,1)S(1)}, u32[]{:S(2)}, u32[]{:S(2)}) collective-permute-start(bf16[528,256]{1,0:T(8,128)(2,1)S(1)} %get-tuple-element.27.refs_0_), channel_id=1, source_target_pairs={{0,1},{1,0},{2,3},{3,2},{4,5},{5,4},{6,7},{7,6},{8,9},{9,8},{10,11... | collective-permute-start | bytes 811016 | tf_op jit(solution)/shard_map/ppermute | solution.py:279
  27.9 1.2 %collective-permute-done.3.refs_1_ = bf16[528,256]{1,0:T(8,128)(2,1)S(1)} collective-permute-done((bf16[528,256]{1,0:T(8,128)(2,1)S(1)}, bf16[528,256]{1,0:T(8,128)(2,1)S(1)}, u32[]{:S(2)}, u32[]{:S(2)}) %collective-permute-start.3) | collective-permute-done | bytes 270368 | tf_op jit(solution)/shard_map/ppermute | solution.py:279
  29.1 2.7 %collective-permute-start.7 = (bf16[528,256]{1,0:T(8,128)(2,1)S(1)}, bf16[528,256]{1,0:T(8,128)(2,1)S(1)}, u32[]{:S(2)}, u32[]{:S(2)}) collective-permute-start(bf16[528,256]{1,0:T(8,128)(2,1)S(1)} %collective-permute-done.3.refs_1_), channel_id=1, source_target_pairs={{0,2},{1,7},{2,4},{3,1},{4,6},{5,3},{6,0},{7,5},{8,10},{9,15},{10,... | collective-permute-start | bytes 811016 | tf_op jit(solution)/shard_map/ppermute | solution.py:275
  31.8 0.5 collective-permute-start.4
  32.4 4.2 %collective-permute-done.4.refs_3_ = bf16[256,256]{1,0:T(8,128)(2,1)S(1)} collective-permute-done((bf16[256,256]{1,0:T(8,128)(2,1)S(1)}, bf16[256,256]{1,0:T(8,128)(2,1)S(1)}, u32[]{:S(2)}, u32[]{:S(2)}) %collective-permute-start.4) | collective-permute-done | bytes 131104 | tf_op jit(solution)/shard_map/ppermute | solution.py:275
  36.6 1.9 %collective-permute-start.6 = (bf16[256,256]{1,0:T(8,128)(2,1)S(1)}, bf16[256,256]{1,0:T(8,128)(2,1)S(1)}, u32[]{:S(2)}, u32[]{:S(2)}) collective-permute-start(bf16[256,256]{1,0:T(8,128)(2,1)S(1)} %collective-permute-done.4.refs_3_), channel_id=1, source_target_pairs={{0,1},{1,0},{2,3},{3,2},{4,5},{5,4},{6,7},{7,6},{8,9},{9,8},{10,11... | collective-permute-start | bytes 393224 | tf_op jit(solution)/shard_map/ppermute | solution.py:279
  38.5 2.7 %collective-permute-start.1 = (bf16[272,256]{1,0:T(8,128)(2,1)S(1)}, bf16[272,256]{1,0:T(8,128)(2,1)S(1)}, u32[]{:S(2)}, u32[]{:S(2)}) collective-permute-start(bf16[272,256]{1,0:T(8,128)(2,1)S(1)} %collective-permute-done.refs_2_), channel_id=1, source_target_pairs={{0,2},{1,7},{2,4},{3,1},{4,6},{5,3},{6,0},{7,5},{8,10},{9,15},{10,... | collective-permute-start | bytes 417800 | tf_op jit(solution)/shard_map/ppermute | solution.py:275
  41.3 0.7 collective-permute-start.5
  42.0 1.3 %collective-permute-done.1.refs_0_ = bf16[272,256]{1,0:T(8,128)(2,1)S(1)} collective-permute-done((bf16[272,256]{1,0:T(8,128)(2,1)S(1)}, bf16[272,256]{1,0:T(8,128)(2,1)S(1)}, u32[]{:S(2)}, u32[]{:S(2)}) %collective-permute-start.1) | collective-permute-done | bytes 139296 | tf_op jit(solution)/shard_map/ppermute | solution.py:275
  43.3 3.0 %collective-permute-start.2 = (bf16[272,256]{1,0:T(8,128)(2,1)S(1)}, bf16[272,256]{1,0:T(8,128)(2,1)S(1)}, u32[]{:S(2)}, u32[]{:S(2)}) collective-permute-start(bf16[272,256]{1,0:T(8,128)(2,1)S(1)} %collective-permute-done.1.refs_0_), channel_id=1, source_target_pairs={{0,1},{1,0},{2,3},{3,2},{4,5},{5,4},{6,7},{7,6},{8,9},{9,8},{10,11... | collective-permute-start | bytes 417800 | tf_op jit(solution)/shard_map/ppermute | solution.py:279
  46.3 1.4 %collective-permute-start.11 = (bf16[256,256]{1,0:T(8,128)(2,1)S(1)}, bf16[256,256]{1,0:T(8,128)(2,1)S(1)}, u32[]{:S(2)}, u32[]{:S(2)}) collective-permute-start(bf16[256,256]{1,0:T(8,128)(2,1)S(1)} %collective-permute-done.10.refs_1_), channel_id=1, source_target_pairs={{0,1},{1,0},{2,3},{3,2},{4,5},{5,4},{6,7},{7,6},{8,9},{9,8},{10,11... | collective-permute-start | bytes 393224 | tf_op jit(solution)/shard_map/ppermute | solution.py:279
  47.7 1.3 %shard_map.82 = (bf16[192,512]{1,0:T(8,128)(2,1)S(1)}, f32[1,256]{1,0:T(1,128)S(1)}, bf16[2048,256]{1,0:T(8,128)(2,1)S(1)}) custom-call(s32[4,64]{1,0:T(4,128)} %bitcast.23, f32[4,64]{1,0:T(4,128)} %bitcast.24, f32[1,256]{1,0:T(1,128)} %bitcast.25, bf16[2048,256]{1,0:T(8,128)(2,1)} %bitcast.21), custom_call_target="tpu_custom_call" | custom-call | tf_op jit(solution)/shard_map/pallas_call | solution.py:245
  49.0 1.2 %shard_map.85 = (f32[512,256]{1,0:T(8,128)S(1)}, f32[512,256]{1,0:T(8,128)S(1)}, f32[512,128]{1,0:T(8,128)S(1)}) custom-call(bf16[528,256]{1,0:T(8,128)(2,1)S(1)} %get-tuple-element.27.refs_0_, bf16[528,256]{1,0:T(8,128)(2,1)S(1)} %collective-permute-done.3.refs_1_, bf16[272,256]{1,0:T(8,128)(2,1)S(1)} %collective-permute-done.refs_2_, ...), custom_call_target="tpu_custom_call" | custom-call | flops 805306368 | tf_op jit(solution)/shard_map/pallas_call | solution.py:245
  50.3 0.5 shard_map.87.refs_2_.own_ref
  50.9 0.5 shard_map.86.refs_0_.own_ref
  51.3 0.6 collective-permute-start.9
  52.4 0.6 collective-permute-start.18
  53.0 0.6 shard_map.88
  53.6 0.5 collective-permute-start.14
  54.8 1.8 %collective-permute-done.18 = bf16[256,256]{1,0:T(8,128)(2,1)S(1)} collective-permute-done((bf16[256,256]{1,0:T(8,128)(2,1)S(1)}, bf16[256,256]{1,0:T(8,128)(2,1)S(1)}, u32[]{:S(2)}, u32[]{:S(2)}) %collective-permute-start.18) | collective-permute-done | bytes 131104 | tf_op jit(solution)/shard_map/ppermute | solution.py:275
  56.6 1.6 %collective-permute-start.19 = (bf16[256,256]{1,0:T(8,128)(2,1)S(1)}, bf16[256,256]{1,0:T(8,128)(2,1)S(1)}, u32[]{:S(2)}, u32[]{:S(2)}) collective-permute-start(bf16[256,256]{1,0:T(8,128)(2,1)S(1)} %add_convert_fusion), channel_id=1, source_target_pairs={{0,2},{1,7},{2,4},{3,1},{4,6},{5,3},{6,0},{7,5},{8,10},{9,15},{10,... | collective-permute-start | bytes 393224 | tf_op jit(solution)/shard_map/ppermute | solution.py:275
  58.2 1.5 %collective-permute-done.14 = bf16[512,256]{1,0:T(8,128)(2,1)S(1)} collective-permute-done((bf16[512,256]{1,0:T(8,128)(2,1)S(1)}, bf16[512,256]{1,0:T(8,128)(2,1)S(1)}, u32[]{:S(2)}, u32[]{:S(2)}) %collective-permute-start.14) | collective-permute-done | bytes 262176 | tf_op jit(solution)/shard_map/ppermute | solution.py:275
  59.6 2.2 %collective-permute-start.15 = (bf16[512,256]{1,0:T(8,128)(2,1)S(1)}, bf16[512,256]{1,0:T(8,128)(2,1)S(1)}, u32[]{:S(2)}, u32[]{:S(2)}) collective-permute-start(bf16[512,256]{1,0:T(8,128)(2,1)S(1)} %collective-permute-done.14), channel_id=1, source_target_pairs={{0,1},{1,0},{2,3},{3,2},{4,5},{5,4},{6,7},{7,6},{8,9},{9,8},{10,11... | collective-permute-start | bytes 786440 | tf_op jit(solution)/shard_map/ppermute | solution.py:279
  61.9 1.1 %collective-permute-start.17 = (bf16[256,256]{1,0:T(8,128)(2,1)S(1)}, bf16[256,256]{1,0:T(8,128)(2,1)S(1)}, u32[]{:S(2)}, u32[]{:S(2)}) collective-permute-start(bf16[256,256]{1,0:T(8,128)(2,1)S(1)} %add_convert_fusion.1), channel_id=1, source_target_pairs={{0,2},{1,7},{2,4},{3,1},{4,6},{5,3},{6,0},{7,5},{8,10},{9,15},{10,... | collective-permute-start | bytes 393224 | tf_op jit(solution)/shard_map/ppermute | solution.py:275
  63.0 2.8 %collective-permute-done.17.near_a_ref = bf16[256,256]{1,0:T(8,128)(2,1)S(1)} collective-permute-done((bf16[256,256]{1,0:T(8,128)(2,1)S(1)}, bf16[256,256]{1,0:T(8,128)(2,1)S(1)}, u32[]{:S(2)}, u32[]{:S(2)}) %collective-permute-start.17) | collective-permute-done | bytes 131104 | tf_op jit(solution)/shard_map/ppermute | solution.py:275
  65.9 13.9 %all_to_all.15 = bf16[32,16,256]{2,1,0:T(8,128)(2,1)S(1)} all-to-all(bf16[32,16,256]{2,1,0:T(8,128)(2,1)S(1)} %bitcast.20), channel_id=1, replica_groups=mesh['ep'=32,'tp'=8] {'ep'}, dimensions={0} | all-to-all | bytes 524288 | tf_op jit(solution)/shard_map/all_to_all | solution.py:405
  80.2 12.0 %all_to_all.16.squares_ref = f32[8,1,128]{2,1,0:T(1,128)S(1)} all-to-all(f32[8,1,128]{2,1,0:T(1,128)S(1)} %get-tuple-element.37), channel_id=1, replica_groups=mesh['ep'=32,'tp'=8] {'tp'}, dimensions={0} | all-to-all | bytes 8192 | tf_op jit(solution)/shard_map/all_to_all | solution.py:412
  92.2 0.7 shard_map.93
  (30 shorter events, 2.3 us)
Async XLA Ops:
  0.0 49.0 %copy-start.1 = (bf16[1,2048,256]{2,1,0:T(8,128)(2,1)S(1)}, bf16[1,2048,256]{2,1,0:T(8,128)(2,1)}, u32[]{:S(2)}) copy-start(bf16[1,2048,256]{2,1,0:T(8,128)(2,1)} %param.12) | copy-start | bytes 3145732
  1.9 23.2 %all-to-all-start = ((bf16[32,16,256]{2,1,0:T(8,128)(2,1)}), bf16[32,16,256]{2,1,0:T(8,128)(2,1)S(1)}, u32[]{:S(2)}, u32[]{:S(2)}) async-start(bf16[32,16,256]{2,1,0:T(8,128)(2,1)} %bitcast.5), calls=%async_computation | async-start | bytes 524288 | tf_op jit(solution)/shard_map/all_to_all | solution.py:296
  13.7 38.2 %collective-permute-start.13 = (bf16[256,2048]{1,0:T(8,128)(2,1)}, bf16[256,2048]{1,0:T(8,128)(2,1)S(1)}, u32[]{:S(2)}, u32[]{:S(2)}) collective-permute-start(bf16[256,2048]{1,0:T(8,128)(2,1)} %bitcast.11), channel_id=1, source_target_pairs={{0,1},{1,0},{2,3},{3,2},{4,5},{5,4},{6,7},{7,6},{8,9},{9,8},{10,11... | collective-permute-start | bytes 3145736 | tf_op jit(solution)/shard_map/ppermute | solution.py:279
  25.4 3.7 %collective-permute-start.3 = (bf16[528,256]{1,0:T(8,128)(2,1)S(1)}, bf16[528,256]{1,0:T(8,128)(2,1)S(1)}, u32[]{:S(2)}, u32[]{:S(2)}) collective-permute-start(bf16[528,256]{1,0:T(8,128)(2,1)S(1)} %get-tuple-element.27.refs_0_), channel_id=1, source_target_pairs={{0,1},{1,0},{2,3},{3,2},{4,5},{5,4},{6,7},{7,6},{8,9},{9,8},{10,11... | collective-permute-start | bytes 811016 | tf_op jit(solution)/shard_map/ppermute | solution.py:279
  29.1 9.5 %collective-permute-start.7 = (bf16[528,256]{1,0:T(8,128)(2,1)S(1)}, bf16[528,256]{1,0:T(8,128)(2,1)S(1)}, u32[]{:S(2)}, u32[]{:S(2)}) collective-permute-start(bf16[528,256]{1,0:T(8,128)(2,1)S(1)} %collective-permute-done.3.refs_1_), channel_id=1, source_target_pairs={{0,2},{1,7},{2,4},{3,1},{4,6},{5,3},{6,0},{7,5},{8,10},{9,15},{10,... | collective-permute-start | bytes 811016 | tf_op jit(solution)/shard_map/ppermute | solution.py:275
  31.8 4.8 %collective-permute-start.4 = (bf16[256,256]{1,0:T(8,128)(2,1)S(1)}, bf16[256,256]{1,0:T(8,128)(2,1)S(1)}, u32[]{:S(2)}, u32[]{:S(2)}) collective-permute-start(bf16[256,256]{1,0:T(8,128)(2,1)S(1)} %get-tuple-element.28), channel_id=1, source_target_pairs={{0,2},{1,7},{2,4},{3,1},{4,6},{5,3},{6,0},{7,5},{8,10},{9,15},{10,... | collective-permute-start | bytes 393224 | tf_op jit(solution)/shard_map/ppermute | solution.py:275
  32.3 6.3 %collective-permute-start = (bf16[272,256]{1,0:T(8,128)(2,1)S(1)}, bf16[272,256]{1,0:T(8,128)(2,1)S(1)}, u32[]{:S(2)}, u32[]{:S(2)}) collective-permute-start(bf16[272,256]{1,0:T(8,128)(2,1)S(1)} %get-tuple-element.25), channel_id=1, source_target_pairs={{0,2},{1,7},{2,4},{3,1},{4,6},{5,3},{6,0},{7,5},{8,10},{9,15},{10,... | collective-permute-start | bytes 417800 | tf_op jit(solution)/shard_map/ppermute | solution.py:275
  36.6 4.6 %collective-permute-start.6 = (bf16[256,256]{1,0:T(8,128)(2,1)S(1)}, bf16[256,256]{1,0:T(8,128)(2,1)S(1)}, u32[]{:S(2)}, u32[]{:S(2)}) collective-permute-start(bf16[256,256]{1,0:T(8,128)(2,1)S(1)} %collective-permute-done.4.refs_3_), channel_id=1, source_target_pairs={{0,1},{1,0},{2,3},{3,2},{4,5},{5,4},{6,7},{7,6},{8,9},{9,8},{10,11... | collective-permute-start | bytes 393224 | tf_op jit(solution)/shard_map/ppermute | solution.py:279
  38.5 10.5 %collective-permute-start.8 = (bf16[528,256]{1,0:T(8,128)(2,1)S(1)}, bf16[528,256]{1,0:T(8,128)(2,1)S(1)}, u32[]{:S(2)}, u32[]{:S(2)}) collective-permute-start(bf16[528,256]{1,0:T(8,128)(2,1)S(1)} %collective-permute-done.7.refs_6_), channel_id=1, source_target_pairs={{0,1},{1,0},{2,3},{3,2},{4,5},{5,4},{6,7},{7,6},{8,9},{9,8},{10,11... | collective-permute-start | bytes 811016 | tf_op jit(solution)/shard_map/ppermute | solution.py:279
  38.5 4.7 %collective-permute-start.1 = (bf16[272,256]{1,0:T(8,128)(2,1)S(1)}, bf16[272,256]{1,0:T(8,128)(2,1)S(1)}, u32[]{:S(2)}, u32[]{:S(2)}) collective-permute-start(bf16[272,256]{1,0:T(8,128)(2,1)S(1)} %collective-permute-done.refs_2_), channel_id=1, source_target_pairs={{0,2},{1,7},{2,4},{3,1},{4,6},{5,3},{6,0},{7,5},{8,10},{9,15},{10,... | collective-permute-start | bytes 417800 | tf_op jit(solution)/shard_map/ppermute | solution.py:275
  41.2 5.1 %collective-permute-start.10 = (bf16[256,256]{1,0:T(8,128)(2,1)S(1)}, bf16[256,256]{1,0:T(8,128)(2,1)S(1)}, u32[]{:S(2)}, u32[]{:S(2)}) collective-permute-start(bf16[256,256]{1,0:T(8,128)(2,1)S(1)} %collective-permute-done.4.refs_3_), channel_id=1, source_target_pairs={{0,2},{1,7},{2,4},{3,1},{4,6},{5,3},{6,0},{7,5},{8,10},{9,15},{10,... | collective-permute-start | bytes 393224 | tf_op jit(solution)/shard_map/ppermute | solution.py:275
  41.3 7.8 %collective-permute-start.5 = (bf16[272,256]{1,0:T(8,128)(2,1)S(1)}, bf16[272,256]{1,0:T(8,128)(2,1)S(1)}, u32[]{:S(2)}, u32[]{:S(2)}) collective-permute-start(bf16[272,256]{1,0:T(8,128)(2,1)S(1)} %collective-permute-done.refs_2_), channel_id=1, source_target_pairs={{0,1},{1,0},{2,3},{3,2},{4,5},{5,4},{6,7},{7,6},{8,9},{9,8},{10,11... | collective-permute-start | bytes 417800 | tf_op jit(solution)/shard_map/ppermute | solution.py:279
  43.3 7.0 %collective-permute-start.2 = (bf16[272,256]{1,0:T(8,128)(2,1)S(1)}, bf16[272,256]{1,0:T(8,128)(2,1)S(1)}, u32[]{:S(2)}, u32[]{:S(2)}) collective-permute-start(bf16[272,256]{1,0:T(8,128)(2,1)S(1)} %collective-permute-done.1.refs_0_), channel_id=1, source_target_pairs={{0,1},{1,0},{2,3},{3,2},{4,5},{5,4},{6,7},{7,6},{8,9},{9,8},{10,11... | collective-permute-start | bytes 417800 | tf_op jit(solution)/shard_map/ppermute | solution.py:279
  46.3 4.0 %collective-permute-start.11 = (bf16[256,256]{1,0:T(8,128)(2,1)S(1)}, bf16[256,256]{1,0:T(8,128)(2,1)S(1)}, u32[]{:S(2)}, u32[]{:S(2)}) collective-permute-start(bf16[256,256]{1,0:T(8,128)(2,1)S(1)} %collective-permute-done.10.refs_1_), channel_id=1, source_target_pairs={{0,1},{1,0},{2,3},{3,2},{4,5},{5,4},{6,7},{7,6},{8,9},{9,8},{10,11... | collective-permute-start | bytes 393224 | tf_op jit(solution)/shard_map/ppermute | solution.py:279
  50.8 1.4 %copy-start = (bf16[1,256,2048]{2,1,0:T(8,128)(2,1)S(1)}, bf16[1,256,2048]{2,1,0:T(8,128)(2,1)}, u32[]{:S(2)}) copy-start(bf16[1,256,2048]{2,1,0:T(8,128)(2,1)} %param.14) | copy-start | bytes 3145732
  50.8 1.4 %collective-permute-start.12 = (bf16[256,256]{1,0:T(8,128)(2,1)S(1)}, bf16[256,256]{1,0:T(8,128)(2,1)S(1)}, u32[]{:S(2)}, u32[]{:S(2)}) collective-permute-start(bf16[256,256]{1,0:T(8,128)(2,1)S(1)} %shard_map.87.refs_2_.own_ref), channel_id=1, source_target_pairs={{0,1},{1,0},{2,3},{3,2},{4,5},{5,4},{6,7},{7,6},{8,9},{9,8},{10,11... | collective-permute-start | bytes 393224 | tf_op jit(solution)/shard_map/ppermute | solution.py:279
  51.3 1.7 %collective-permute-start.9 = (bf16[256,256]{1,0:T(8,128)(2,1)S(1)}, bf16[256,256]{1,0:T(8,128)(2,1)S(1)}, u32[]{:S(2)}, u32[]{:S(2)}) collective-permute-start(bf16[256,256]{1,0:T(8,128)(2,1)S(1)} %shard_map.86.refs_0_.own_ref), channel_id=1, source_target_pairs={{0,1},{1,0},{2,3},{3,2},{4,5},{5,4},{6,7},{7,6},{8,9},{9,8},{10,11... | collective-permute-start | bytes 393224 | tf_op jit(solution)/shard_map/ppermute | solution.py:279
  52.4 4.1 %collective-permute-start.18 = (bf16[256,256]{1,0:T(8,128)(2,1)S(1)}, bf16[256,256]{1,0:T(8,128)(2,1)S(1)}, u32[]{:S(2)}, u32[]{:S(2)}) collective-permute-start(bf16[256,256]{1,0:T(8,128)(2,1)S(1)} %shard_map.90), channel_id=1, source_target_pairs={{0,2},{1,7},{2,4},{3,1},{4,6},{5,3},{6,0},{7,5},{8,10},{9,15},{10,... | collective-permute-start | bytes 393224 | tf_op jit(solution)/shard_map/ppermute | solution.py:275
  53.6 6.0 %collective-permute-start.14 = (bf16[512,256]{1,0:T(8,128)(2,1)S(1)}, bf16[512,256]{1,0:T(8,128)(2,1)S(1)}, u32[]{:S(2)}, u32[]{:S(2)}) collective-permute-start(bf16[512,256]{1,0:T(8,128)(2,1)S(1)} %get-tuple-element.33), channel_id=1, source_target_pairs={{0,2},{1,7},{2,4},{3,1},{4,6},{5,3},{6,0},{7,5},{8,10},{9,15},{10,... | collective-permute-start | bytes 786440 | tf_op jit(solution)/shard_map/ppermute | solution.py:275
  54.4 7.5 %collective-permute-start.16 = (bf16[256,256]{1,0:T(8,128)(2,1)S(1)}, bf16[256,256]{1,0:T(8,128)(2,1)S(1)}, u32[]{:S(2)}, u32[]{:S(2)}) collective-permute-start(bf16[256,256]{1,0:T(8,128)(2,1)S(1)} %shard_map.89), channel_id=1, source_target_pairs={{0,2},{1,7},{2,4},{3,1},{4,6},{5,3},{6,0},{7,5},{8,10},{9,15},{10,... | collective-permute-start | bytes 393224 | tf_op jit(solution)/shard_map/ppermute | solution.py:275
  56.6 6.4 %collective-permute-start.19 = (bf16[256,256]{1,0:T(8,128)(2,1)S(1)}, bf16[256,256]{1,0:T(8,128)(2,1)S(1)}, u32[]{:S(2)}, u32[]{:S(2)}) collective-permute-start(bf16[256,256]{1,0:T(8,128)(2,1)S(1)} %add_convert_fusion), channel_id=1, source_target_pairs={{0,2},{1,7},{2,4},{3,1},{4,6},{5,3},{6,0},{7,5},{8,10},{9,15},{10,... | collective-permute-start | bytes 393224 | tf_op jit(solution)/shard_map/ppermute | solution.py:275
  59.6 6.2 %collective-permute-start.15 = (bf16[512,256]{1,0:T(8,128)(2,1)S(1)}, bf16[512,256]{1,0:T(8,128)(2,1)S(1)}, u32[]{:S(2)}, u32[]{:S(2)}) collective-permute-start(bf16[512,256]{1,0:T(8,128)(2,1)S(1)} %collective-permute-done.14), channel_id=1, source_target_pairs={{0,1},{1,0},{2,3},{3,2},{4,5},{5,4},{6,7},{7,6},{8,9},{9,8},{10,11... | collective-permute-start | bytes 786440 | tf_op jit(solution)/shard_map/ppermute | solution.py:279
  61.9 3.9 %collective-permute-start.17 = (bf16[256,256]{1,0:T(8,128)(2,1)S(1)}, bf16[256,256]{1,0:T(8,128)(2,1)S(1)}, u32[]{:S(2)}, u32[]{:S(2)}) collective-permute-start(bf16[256,256]{1,0:T(8,128)(2,1)S(1)} %add_convert_fusion.1), channel_id=1, source_target_pairs={{0,2},{1,7},{2,4},{3,1},{4,6},{5,3},{6,0},{7,5},{8,10},{9,15},{10,... | collective-permute-start | bytes 393224 | tf_op jit(solution)/shard_map/ppermute | solution.py:275

commit v2 on v1

--- a/solution.py
+++ b/solution.py
@@ -152,12 +152,15 @@
 
 
 def first_kernel(places, sizes, *refs):
-    pieces, (gate_ref, up_ref, gate_out, up_out, squares_out) = grouped(places, sizes, refs)
+    pieces, (gate_ref, up_ref, *before, gate_out, up_out, squares_out) = grouped(
+        places, sizes, refs
+    )
     width = gate_ref.shape[1]
     for part in range(gate_out.shape[0] // width):
         at = slice(part * width, (part + 1) * width)
         zero = jnp.zeros((width, width), jnp.float32)
-        gate, up, squares = products(part, pieces, gate_ref, up_ref, zero, zero, zero[:, :128])
+        start = [ref[at, :] for ref in before] or [zero, zero, zero[:, :128]]
+        gate, up, squares = products(part, pieces, gate_ref, up_ref, *start)
         gate_out[at, :] = gate
         up_out[at, :] = up
         squares_out[at, :] = squares
@@ -338,17 +341,22 @@
     late = [(-2, 0, chips), (2, 1, chips)]
     wide = shape_of((rows, width), jnp.float32)
     flops = 4 * rows * width * width
-    sums = call(
-        functools.partial(
-            first_kernel, [where for where, _ in early], [len(held) for _, held in early]
-        ),
-        [wide, wide, shape_of((rows, 128), jnp.float32)],
-        *[part for _, held in early for part in held],
-        gate,
-        up,
-        limit=16,
-        flops=len(early) * flops,
-    )
+
+    def sums_of(pieces, *before):
+        return call(
+            functools.partial(
+                first_kernel, [where for where, _ in pieces], [len(held) for _, held in pieces]
+            ),
+            [wide, wide, shape_of((rows, 128), jnp.float32)],
+            *[part for _, held in pieces for part in held],
+            gate,
+            up,
+            *before,
+            limit=16,
+            flops=len(pieces) * flops,
+        )
+
+    sums = sums_of(early[4:], *sums_of(early[:4]))
 
     def last(part, *held):
         act = call(

time: 93.2 us -> 93.4 us (level)
    pallas_call x12 -> x13, Pallas kernels: 7.86 us -> 8.03 us  [call(): pl.pallas_call(kernel, out_shape=outs, in_specs=[space] * len(args), out_...]
where the time goes in v2:
time: 93.4 us; the launch traced here: 93.1 us
  starting transfers between devices  35.7 us (38%)
  blocking collectives  26 us (28%)
  waiting for transfers between devices  23.2 us (25%)
  Pallas kernels  8.03 us (9%)
    all_to_all x1, blocking collectives, local(): lax.all_to_all(expert_out, 'ep', split_axis=0, concat_axis=0, tiled=True)  13.9 us
    ppermute x10, starting transfers between devices, swap(): return lax.ppermute(value, 'tp', pairs)  13.5 us
    all_to_all x1, blocking collectives, local(): lax.all_to_all(squares, 'tp', split_axis=0, concat_axis=0, tiled=True)  12 us
    all_to_all x1, starting transfers between devices, local(): lax.all_to_all(outbound.reshape(experts, capacity, width), 'ep', split_ax...  11.9 us
    ppermute x10, waiting for transfers between devices, onward(): return lax.ppermute(value, 'tp', pairs)  11.5 us
    all_to_all x1, waiting for transfers between devices, local(): lax.all_to_all(outbound.reshape(experts, capacity, width), 'ep', split_ax...  10.3 us
    ppermute x10, starting transfers between devices, onward(): return lax.ppermute(value, 'tp', pairs)  10.3 us
    pallas_call x13, Pallas kernels, call(): pl.pallas_call(kernel, out_shape=outs, in_specs=[space] * len(args), out_...  8.03 us
  transfers between devices with their start and end apart: 21, of which 8 were waited for; matrix products, arithmetic and copies ran while one was open for 0% of the time, Pallas kernels for 5%

profile of v2, /device:TPU:1, one launch (start us, length us, event | category | flops | bytes accessed | tf_op | source)
XLA Modules:
  0.0 93.1 jit_solution(5835954461369691158)
XLA Ops:
  0.0 1.9 %shard_map.83 = (bf16[512,256]{1,0:T(8,128)(2,1)}, f32[1,256]{1,0:T(1,128)S(1)}) custom-call(s32[4,64]{1,0:T(4,128)} %bitcast.23, bf16[64,256]{1,0:T(8,128)(2,1)} %tokens_hbm.1, f32[1,256]{1,0:T(1,128)} %bitcast.27), custom_call_target="tpu_custom_call" | custom-call | tf_op jit(solution)/shard_map/pallas_call | solution.py:248
  1.9 11.9 %all-to-all-start = ((bf16[32,16,256]{2,1,0:T(8,128)(2,1)}), bf16[32,16,256]{2,1,0:T(8,128)(2,1)S(1)}, u32[]{:S(2)}, u32[]{:S(2)}) async-start(bf16[32,16,256]{2,1,0:T(8,128)(2,1)} %bitcast.5), calls=%async_computation | async-start | bytes 524288 | tf_op jit(solution)/shard_map/all_to_all | solution.py:299
  13.8 1.0 %collective-permute-start.13 = (bf16[256,2048]{1,0:T(8,128)(2,1)}, bf16[256,2048]{1,0:T(8,128)(2,1)S(1)}, u32[]{:S(2)}, u32[]{:S(2)}) collective-permute-start(bf16[256,2048]{1,0:T(8,128)(2,1)} %bitcast.15), channel_id=1, source_target_pairs={{0,1},{1,0},{2,3},{3,2},{4,5},{5,4},{6,7},{7,6},{8,9},{9,8},{10,11... | collective-permute-start | bytes 3145736 | tf_op jit(solution)/shard_map/ppermute | solution.py:282
  14.8 10.3 %all-to-all-done = bf16[32,16,256]{2,1,0:T(8,128)(2,1)S(1)} async-done(((bf16[32,16,256]{2,1,0:T(8,128)(2,1)}), bf16[32,16,256]{2,1,0:T(8,128)(2,1)S(1)}, u32[]{:S(2)}, u32[]{:S(2)}) %all-to-all-start) | async-done | bytes 262176 | tf_op jit(solution)/shard_map/all_to_all | solution.py:299
  25.4 2.5 %collective-permute-start.3 = (bf16[528,256]{1,0:T(8,128)(2,1)S(1)}, bf16[528,256]{1,0:T(8,128)(2,1)S(1)}, u32[]{:S(2)}, u32[]{:S(2)}) collective-permute-start(bf16[528,256]{1,0:T(8,128)(2,1)S(1)} %get-tuple-element.30.refs_0_), channel_id=1, source_target_pairs={{0,1},{1,0},{2,3},{3,2},{4,5},{5,4},{6,7},{7,6},{8,9},{9,8},{10,11... | collective-permute-start | bytes 811016 | tf_op jit(solution)/shard_map/ppermute | solution.py:282
  27.9 1.2 %collective-permute-done.3.refs_1_ = bf16[528,256]{1,0:T(8,128)(2,1)S(1)} collective-permute-done((bf16[528,256]{1,0:T(8,128)(2,1)S(1)}, bf16[528,256]{1,0:T(8,128)(2,1)S(1)}, u32[]{:S(2)}, u32[]{:S(2)}) %collective-permute-start.3) | collective-permute-done | bytes 270368 | tf_op jit(solution)/shard_map/ppermute | solution.py:282
  29.1 2.7 %collective-permute-start.4 = (bf16[528,256]{1,0:T(8,128)(2,1)S(1)}, bf16[528,256]{1,0:T(8,128)(2,1)S(1)}, u32[]{:S(2)}, u32[]{:S(2)}) collective-permute-start(bf16[528,256]{1,0:T(8,128)(2,1)S(1)} %collective-permute-done.3.refs_1_), channel_id=1, source_target_pairs={{0,2},{1,7},{2,4},{3,1},{4,6},{5,3},{6,0},{7,5},{8,10},{9,15},{10,... | collective-permute-start | bytes 811016 | tf_op jit(solution)/shard_map/ppermute | solution.py:278
  31.8 0.5 collective-permute-start.6
  32.4 4.2 %collective-permute-done.6.refs_3_ = bf16[256,256]{1,0:T(8,128)(2,1)S(1)} collective-permute-done((bf16[256,256]{1,0:T(8,128)(2,1)S(1)}, bf16[256,256]{1,0:T(8,128)(2,1)S(1)}, u32[]{:S(2)}, u32[]{:S(2)}) %collective-permute-start.6) | collective-permute-done | bytes 131104 | tf_op jit(solution)/shard_map/ppermute | solution.py:278
  36.6 1.9 %collective-permute-start.8 = (bf16[256,256]{1,0:T(8,128)(2,1)S(1)}, bf16[256,256]{1,0:T(8,128)(2,1)S(1)}, u32[]{:S(2)}, u32[]{:S(2)}) collective-permute-start(bf16[256,256]{1,0:T(8,128)(2,1)S(1)} %collective-permute-done.6.refs_3_), channel_id=1, source_target_pairs={{0,1},{1,0},{2,3},{3,2},{4,5},{5,4},{6,7},{7,6},{8,9},{9,8},{10,11... | collective-permute-start | bytes 393224 | tf_op jit(solution)/shard_map/ppermute | solution.py:282
  38.5 2.7 %collective-permute-start.1 = (bf16[272,256]{1,0:T(8,128)(2,1)S(1)}, bf16[272,256]{1,0:T(8,128)(2,1)S(1)}, u32[]{:S(2)}, u32[]{:S(2)}) collective-permute-start(bf16[272,256]{1,0:T(8,128)(2,1)S(1)} %collective-permute-done.refs_2_), channel_id=1, source_target_pairs={{0,2},{1,7},{2,4},{3,1},{4,6},{5,3},{6,0},{7,5},{8,10},{9,15},{10,... | collective-permute-start | bytes 417800 | tf_op jit(solution)/shard_map/ppermute | solution.py:278
  41.3 0.7 collective-permute-start.7
  42.0 1.3 %collective-permute-done.1.refs_0_ = bf16[272,256]{1,0:T(8,128)(2,1)S(1)} collective-permute-done((bf16[272,256]{1,0:T(8,128)(2,1)S(1)}, bf16[272,256]{1,0:T(8,128)(2,1)S(1)}, u32[]{:S(2)}, u32[]{:S(2)}) %collective-permute-start.1) | collective-permute-done | bytes 139296 | tf_op jit(solution)/shard_map/ppermute | solution.py:278
  43.3 3.0 %collective-permute-start.2 = (bf16[272,256]{1,0:T(8,128)(2,1)S(1)}, bf16[272,256]{1,0:T(8,128)(2,1)S(1)}, u32[]{:S(2)}, u32[]{:S(2)}) collective-permute-start(bf16[272,256]{1,0:T(8,128)(2,1)S(1)} %collective-permute-done.1.refs_0_), channel_id=1, source_target_pairs={{0,1},{1,0},{2,3},{3,2},{4,5},{5,4},{6,7},{7,6},{8,9},{9,8},{10,11... | collective-permute-start | bytes 417800 | tf_op jit(solution)/shard_map/ppermute | solution.py:282
  46.3 1.4 %collective-permute-start.11 = (bf16[256,256]{1,0:T(8,128)(2,1)S(1)}, bf16[256,256]{1,0:T(8,128)(2,1)S(1)}, u32[]{:S(2)}, u32[]{:S(2)}) collective-permute-start(bf16[256,256]{1,0:T(8,128)(2,1)S(1)} %collective-permute-done.10.refs_1_), channel_id=1, source_target_pairs={{0,1},{1,0},{2,3},{3,2},{4,5},{5,4},{6,7},{7,6},{8,9},{9,8},{10,11... | collective-permute-start | bytes 393224 | tf_op jit(solution)/shard_map/ppermute | solution.py:282
  47.7 1.3 %shard_map.82 = (bf16[192,512]{1,0:T(8,128)(2,1)S(1)}, f32[1,256]{1,0:T(1,128)S(1)}, bf16[2048,256]{1,0:T(8,128)(2,1)S(1)}) custom-call(s32[4,64]{1,0:T(4,128)} %bitcast.24, f32[4,64]{1,0:T(4,128)} %bitcast.25, f32[1,256]{1,0:T(1,128)} %bitcast.26, bf16[2048,256]{1,0:T(8,128)(2,1)} %bitcast.22), custom_call_target="tpu_custom_call" | custom-call | tf_op jit(solution)/shard_map/pallas_call | solution.py:248
  49.0 0.9 shard_map.85
  49.9 0.5 shard_map.86
  50.5 0.5 shard_map.88.refs_2_.own_ref
  51.5 0.6 collective-permute-start.9
  52.6 0.6 collective-permute-start.18
  53.2 0.6 shard_map.89
  53.8 0.5 collective-permute-start.14
  55.0 1.8 %collective-permute-done.18 = bf16[256,256]{1,0:T(8,128)(2,1)S(1)} collective-permute-done((bf16[256,256]{1,0:T(8,128)(2,1)S(1)}, bf16[256,256]{1,0:T(8,128)(2,1)S(1)}, u32[]{:S(2)}, u32[]{:S(2)}) %collective-permute-start.18) | collective-permute-done | bytes 131104 | tf_op jit(solution)/shard_map/ppermute | solution.py:278
  56.7 1.6 %collective-permute-start.19 = (bf16[256,256]{1,0:T(8,128)(2,1)S(1)}, bf16[256,256]{1,0:T(8,128)(2,1)S(1)}, u32[]{:S(2)}, u32[]{:S(2)}) collective-permute-start(bf16[256,256]{1,0:T(8,128)(2,1)S(1)} %add_convert_fusion), channel_id=1, source_target_pairs={{0,2},{1,7},{2,4},{3,1},{4,6},{5,3},{6,0},{7,5},{8,10},{9,15},{10,... | collective-permute-start | bytes 393224 | tf_op jit(solution)/shard_map/ppermute | solution.py:278
  58.4 1.4 %collective-permute-done.14 = bf16[512,256]{1,0:T(8,128)(2,1)S(1)} collective-permute-done((bf16[512,256]{1,0:T(8,128)(2,1)S(1)}, bf16[512,256]{1,0:T(8,128)(2,1)S(1)}, u32[]{:S(2)}, u32[]{:S(2)}) %collective-permute-start.14) | collective-permute-done | bytes 262176 | tf_op jit(solution)/shard_map/ppermute | solution.py:278
  59.8 2.2 %collective-permute-start.15 = (bf16[512,256]{1,0:T(8,128)(2,1)S(1)}, bf16[512,256]{1,0:T(8,128)(2,1)S(1)}, u32[]{:S(2)}, u32[]{:S(2)}) collective-permute-start(bf16[512,256]{1,0:T(8,128)(2,1)S(1)} %collective-permute-done.14), channel_id=1, source_target_pairs={{0,1},{1,0},{2,3},{3,2},{4,5},{5,4},{6,7},{7,6},{8,9},{9,8},{10,11... | collective-permute-start | bytes 786440 | tf_op jit(solution)/shard_map/ppermute | solution.py:282
  62.1 1.1 %collective-permute-start.17 = (bf16[256,256]{1,0:T(8,128)(2,1)S(1)}, bf16[256,256]{1,0:T(8,128)(2,1)S(1)}, u32[]{:S(2)}, u32[]{:S(2)}) collective-permute-start(bf16[256,256]{1,0:T(8,128)(2,1)S(1)} %add_convert_fusion.1), channel_id=1, source_target_pairs={{0,2},{1,7},{2,4},{3,1},{4,6},{5,3},{6,0},{7,5},{8,10},{9,15},{10,... | collective-permute-start | bytes 393224 | tf_op jit(solution)/shard_map/ppermute | solution.py:278
  63.2 2.8 %collective-permute-done.17.near_a_ref = bf16[256,256]{1,0:T(8,128)(2,1)S(1)} collective-permute-done((bf16[256,256]{1,0:T(8,128)(2,1)S(1)}, bf16[256,256]{1,0:T(8,128)(2,1)S(1)}, u32[]{:S(2)}, u32[]{:S(2)}) %collective-permute-start.17) | collective-permute-done | bytes 131104 | tf_op jit(solution)/shard_map/ppermute | solution.py:278
  66.1 13.9 %all_to_all.15 = bf16[32,16,256]{2,1,0:T(8,128)(2,1)S(1)} all-to-all(bf16[32,16,256]{2,1,0:T(8,128)(2,1)S(1)} %bitcast.21), channel_id=1, replica_groups=mesh['ep'=32,'tp'=8] {'ep'}, dimensions={0} | all-to-all | bytes 524288 | tf_op jit(solution)/shard_map/all_to_all | solution.py:413
  80.4 12.0 %all_to_all.16.squares_ref = f32[8,1,128]{2,1,0:T(1,128)S(1)} all-to-all(f32[8,1,128]{2,1,0:T(1,128)S(1)} %get-tuple-element.43), channel_id=1, replica_groups=mesh['ep'=32,'tp'=8] {'tp'}, dimensions={0} | all-to-all | bytes 8192 | tf_op jit(solution)/shard_map/all_to_all | solution.py:420
  92.4 0.7 shard_map.94
  (31 shorter events, 2.7 us)
Async XLA Ops:
  0.0 49.0 %copy-start = (bf16[1,2048,256]{2,1,0:T(8,128)(2,1)S(1)}, bf16[1,2048,256]{2,1,0:T(8,128)(2,1)}, u32[]{:S(2)}) copy-start(bf16[1,2048,256]{2,1,0:T(8,128)(2,1)} %param.12) | copy-start | bytes 3145732
  1.9 23.2 %all-to-all-start = ((bf16[32,16,256]{2,1,0:T(8,128)(2,1)}), bf16[32,16,256]{2,1,0:T(8,128)(2,1)S(1)}, u32[]{:S(2)}, u32[]{:S(2)}) async-start(bf16[32,16,256]{2,1,0:T(8,128)(2,1)} %bitcast.5), calls=%async_computation | async-start | bytes 524288 | tf_op jit(solution)/shard_map/all_to_all | solution.py:299
  13.8 38.4 %collective-permute-start.13 = (bf16[256,2048]{1,0:T(8,128)(2,1)}, bf16[256,2048]{1,0:T(8,128)(2,1)S(1)}, u32[]{:S(2)}, u32[]{:S(2)}) collective-permute-start(bf16[256,2048]{1,0:T(8,128)(2,1)} %bitcast.15), channel_id=1, source_target_pairs={{0,1},{1,0},{2,3},{3,2},{4,5},{5,4},{6,7},{7,6},{8,9},{9,8},{10,11... | collective-permute-start | bytes 3145736 | tf_op jit(solution)/shard_map/ppermute | solution.py:282
  25.4 3.7 %collective-permute-start.3 = (bf16[528,256]{1,0:T(8,128)(2,1)S(1)}, bf16[528,256]{1,0:T(8,128)(2,1)S(1)}, u32[]{:S(2)}, u32[]{:S(2)}) collective-permute-start(bf16[528,256]{1,0:T(8,128)(2,1)S(1)} %get-tuple-element.30.refs_0_), channel_id=1, source_target_pairs={{0,1},{1,0},{2,3},{3,2},{4,5},{5,4},{6,7},{7,6},{8,9},{9,8},{10,11... | collective-permute-start | bytes 811016 | tf_op jit(solution)/shard_map/ppermute | solution.py:282
  29.1 9.5 %collective-permute-start.4 = (bf16[528,256]{1,0:T(8,128)(2,1)S(1)}, bf16[528,256]{1,0:T(8,128)(2,1)S(1)}, u32[]{:S(2)}, u32[]{:S(2)}) collective-permute-start(bf16[528,256]{1,0:T(8,128)(2,1)S(1)} %collective-permute-done.3.refs_1_), channel_id=1, source_target_pairs={{0,2},{1,7},{2,4},{3,1},{4,6},{5,3},{6,0},{7,5},{8,10},{9,15},{10,... | collective-permute-start | bytes 811016 | tf_op jit(solution)/shard_map/ppermute | solution.py:278
  31.8 4.8 %collective-permute-start.6 = (bf16[256,256]{1,0:T(8,128)(2,1)S(1)}, bf16[256,256]{1,0:T(8,128)(2,1)S(1)}, u32[]{:S(2)}, u32[]{:S(2)}) collective-permute-start(bf16[256,256]{1,0:T(8,128)(2,1)S(1)} %get-tuple-element.31), channel_id=1, source_target_pairs={{0,2},{1,7},{2,4},{3,1},{4,6},{5,3},{6,0},{7,5},{8,10},{9,15},{10,... | collective-permute-start | bytes 393224 | tf_op jit(solution)/shard_map/ppermute | solution.py:278
  32.3 6.3 %collective-permute-start = (bf16[272,256]{1,0:T(8,128)(2,1)S(1)}, bf16[272,256]{1,0:T(8,128)(2,1)S(1)}, u32[]{:S(2)}, u32[]{:S(2)}) collective-permute-start(bf16[272,256]{1,0:T(8,128)(2,1)S(1)} %get-tuple-element.28), channel_id=1, source_target_pairs={{0,2},{1,7},{2,4},{3,1},{4,6},{5,3},{6,0},{7,5},{8,10},{9,15},{10,... | collective-permute-start | bytes 417800 | tf_op jit(solution)/shard_map/ppermute | solution.py:278
  36.6 4.6 %collective-permute-start.8 = (bf16[256,256]{1,0:T(8,128)(2,1)S(1)}, bf16[256,256]{1,0:T(8,128)(2,1)S(1)}, u32[]{:S(2)}, u32[]{:S(2)}) collective-permute-start(bf16[256,256]{1,0:T(8,128)(2,1)S(1)} %collective-permute-done.6.refs_3_), channel_id=1, source_target_pairs={{0,1},{1,0},{2,3},{3,2},{4,5},{5,4},{6,7},{7,6},{8,9},{9,8},{10,11... | collective-permute-start | bytes 393224 | tf_op jit(solution)/shard_map/ppermute | solution.py:282
  38.5 11.4 %collective-permute-start.5 = (bf16[528,256]{1,0:T(8,128)(2,1)S(1)}, bf16[528,256]{1,0:T(8,128)(2,1)S(1)}, u32[]{:S(2)}, u32[]{:S(2)}) collective-permute-start(bf16[528,256]{1,0:T(8,128)(2,1)S(1)} %collective-permute-done.4.refs_0_), channel_id=1, source_target_pairs={{0,1},{1,0},{2,3},{3,2},{4,5},{5,4},{6,7},{7,6},{8,9},{9,8},{10,11... | collective-permute-start | bytes 811016 | tf_op jit(solution)/shard_map/ppermute | solution.py:282
  38.5 4.7 %collective-permute-start.1 = (bf16[272,256]{1,0:T(8,128)(2,1)S(1)}, bf16[272,256]{1,0:T(8,128)(2,1)S(1)}, u32[]{:S(2)}, u32[]{:S(2)}) collective-permute-start(bf16[272,256]{1,0:T(8,128)(2,1)S(1)} %collective-permute-done.refs_2_), channel_id=1, source_target_pairs={{0,2},{1,7},{2,4},{3,1},{4,6},{5,3},{6,0},{7,5},{8,10},{9,15},{10,... | collective-permute-start | bytes 417800 | tf_op jit(solution)/shard_map/ppermute | solution.py:278
  41.2 5.1 %collective-permute-start.10 = (bf16[256,256]{1,0:T(8,128)(2,1)S(1)}, bf16[256,256]{1,0:T(8,128)(2,1)S(1)}, u32[]{:S(2)}, u32[]{:S(2)}) collective-permute-start(bf16[256,256]{1,0:T(8,128)(2,1)S(1)} %collective-permute-done.6.refs_3_), channel_id=1, source_target_pairs={{0,2},{1,7},{2,4},{3,1},{4,6},{5,3},{6,0},{7,5},{8,10},{9,15},{10,... | collective-permute-start | bytes 393224 | tf_op jit(solution)/shard_map/ppermute | solution.py:278
  41.3 7.8 %collective-permute-start.7 = (bf16[272,256]{1,0:T(8,128)(2,1)S(1)}, bf16[272,256]{1,0:T(8,128)(2,1)S(1)}, u32[]{:S(2)}, u32[]{:S(2)}) collective-permute-start(bf16[272,256]{1,0:T(8,128)(2,1)S(1)} %collective-permute-done.refs_2_), channel_id=1, source_target_pairs={{0,1},{1,0},{2,3},{3,2},{4,5},{5,4},{6,7},{7,6},{8,9},{9,8},{10,11... | collective-permute-start | bytes 417800 | tf_op jit(solution)/shard_map/ppermute | solution.py:282
  43.3 7.2 %collective-permute-start.2 = (bf16[272,256]{1,0:T(8,128)(2,1)S(1)}, bf16[272,256]{1,0:T(8,128)(2,1)S(1)}, u32[]{:S(2)}, u32[]{:S(2)}) collective-permute-start(bf16[272,256]{1,0:T(8,128)(2,1)S(1)} %collective-permute-done.1.refs_0_), channel_id=1, source_target_pairs={{0,1},{1,0},{2,3},{3,2},{4,5},{5,4},{6,7},{7,6},{8,9},{9,8},{10,11... | collective-permute-start | bytes 417800 | tf_op jit(solution)/shard_map/ppermute | solution.py:282
  46.3 4.2 %collective-permute-start.11 = (bf16[256,256]{1,0:T(8,128)(2,1)S(1)}, bf16[256,256]{1,0:T(8,128)(2,1)S(1)}, u32[]{:S(2)}, u32[]{:S(2)}) collective-permute-start(bf16[256,256]{1,0:T(8,128)(2,1)S(1)} %collective-permute-done.10.refs_1_), channel_id=1, source_target_pairs={{0,1},{1,0},{2,3},{3,2},{4,5},{5,4},{6,7},{7,6},{8,9},{9,8},{10,11... | collective-permute-start | bytes 393224 | tf_op jit(solution)/shard_map/ppermute | solution.py:282
  50.9 1.4 %copy-start.1 = (bf16[1,256,2048]{2,1,0:T(8,128)(2,1)S(1)}, bf16[1,256,2048]{2,1,0:T(8,128)(2,1)}, u32[]{:S(2)}) copy-start(bf16[1,256,2048]{2,1,0:T(8,128)(2,1)} %param.14) | copy-start | bytes 3145732
  51.0 1.4 %collective-permute-start.12 = (bf16[256,256]{1,0:T(8,128)(2,1)S(1)}, bf16[256,256]{1,0:T(8,128)(2,1)S(1)}, u32[]{:S(2)}, u32[]{:S(2)}) collective-permute-start(bf16[256,256]{1,0:T(8,128)(2,1)S(1)} %shard_map.88.refs_2_.own_ref), channel_id=1, source_target_pairs={{0,1},{1,0},{2,3},{3,2},{4,5},{5,4},{6,7},{7,6},{8,9},{9,8},{10,11... | collective-permute-start | bytes 393224 | tf_op jit(solution)/shard_map/ppermute | solution.py:282
  51.5 1.7 %collective-permute-start.9 = (bf16[256,256]{1,0:T(8,128)(2,1)S(1)}, bf16[256,256]{1,0:T(8,128)(2,1)S(1)}, u32[]{:S(2)}, u32[]{:S(2)}) collective-permute-start(bf16[256,256]{1,0:T(8,128)(2,1)S(1)} %shard_map.87.refs_0_.own_ref), channel_id=1, source_target_pairs={{0,1},{1,0},{2,3},{3,2},{4,5},{5,4},{6,7},{7,6},{8,9},{9,8},{10,11... | collective-permute-start | bytes 393224 | tf_op jit(solution)/shard_map/ppermute | solution.py:282
  52.6 4.1 %collective-permute-start.18 = (bf16[256,256]{1,0:T(8,128)(2,1)S(1)}, bf16[256,256]{1,0:T(8,128)(2,1)S(1)}, u32[]{:S(2)}, u32[]{:S(2)}) collective-permute-start(bf16[256,256]{1,0:T(8,128)(2,1)S(1)} %shard_map.91), channel_id=1, source_target_pairs={{0,2},{1,7},{2,4},{3,1},{4,6},{5,3},{6,0},{7,5},{8,10},{9,15},{10,... | collective-permute-start | bytes 393224 | tf_op jit(solution)/shard_map/ppermute | solution.py:278
  53.8 6.0 %collective-permute-start.14 = (bf16[512,256]{1,0:T(8,128)(2,1)S(1)}, bf16[512,256]{1,0:T(8,128)(2,1)S(1)}, u32[]{:S(2)}, u32[]{:S(2)}) collective-permute-start(bf16[512,256]{1,0:T(8,128)(2,1)S(1)} %get-tuple-element.39), channel_id=1, source_target_pairs={{0,2},{1,7},{2,4},{3,1},{4,6},{5,3},{6,0},{7,5},{8,10},{9,15},{10,... | collective-permute-start | bytes 786440 | tf_op jit(solution)/shard_map/ppermute | solution.py:278
  54.6 7.5 %collective-permute-start.16 = (bf16[256,256]{1,0:T(8,128)(2,1)S(1)}, bf16[256,256]{1,0:T(8,128)(2,1)S(1)}, u32[]{:S(2)}, u32[]{:S(2)}) collective-permute-start(bf16[256,256]{1,0:T(8,128)(2,1)S(1)} %shard_map.90), channel_id=1, source_target_pairs={{0,2},{1,7},{2,4},{3,1},{4,6},{5,3},{6,0},{7,5},{8,10},{9,15},{10,... | collective-permute-start | bytes 393224 | tf_op jit(solution)/shard_map/ppermute | solution.py:278
  56.7 6.4 %collective-permute-start.19 = (bf16[256,256]{1,0:T(8,128)(2,1)S(1)}, bf16[256,256]{1,0:T(8,128)(2,1)S(1)}, u32[]{:S(2)}, u32[]{:S(2)}) collective-permute-start(bf16[256,256]{1,0:T(8,128)(2,1)S(1)} %add_convert_fusion), channel_id=1, source_target_pairs={{0,2},{1,7},{2,4},{3,1},{4,6},{5,3},{6,0},{7,5},{8,10},{9,15},{10,... | collective-permute-start | bytes 393224 | tf_op jit(solution)/shard_map/ppermute | solution.py:278
  59.8 6.2 %collective-permute-start.15 = (bf16[512,256]{1,0:T(8,128)(2,1)S(1)}, bf16[512,256]{1,0:T(8,128)(2,1)S(1)}, u32[]{:S(2)}, u32[]{:S(2)}) collective-permute-start(bf16[512,256]{1,0:T(8,128)(2,1)S(1)} %collective-permute-done.14), channel_id=1, source_target_pairs={{0,1},{1,0},{2,3},{3,2},{4,5},{5,4},{6,7},{7,6},{8,9},{9,8},{10,11... | collective-permute-start | bytes 786440 | tf_op jit(solution)/shard_map/ppermute | solution.py:282
  62.1 3.9 %collective-permute-start.17 = (bf16[256,256]{1,0:T(8,128)(2,1)S(1)}, bf16[256,256]{1,0:T(8,128)(2,1)S(1)}, u32[]{:S(2)}, u32[]{:S(2)}) collective-permute-start(bf16[256,256]{1,0:T(8,128)(2,1)S(1)} %add_convert_fusion.1), channel_id=1, source_target_pairs={{0,2},{1,7},{2,4},{3,1},{4,6},{5,3},{6,0},{7,5},{8,10},{9,15},{10,... | collective-permute-start | bytes 393224 | tf_op jit(solution)/shard_map/ppermute | solution.py:278

commit v3 on v2

--- a/solution.py
+++ b/solution.py
@@ -223,14 +223,11 @@
     ones = jnp.ones((8, mix.shape[1]), jnp.bfloat16)
     sums = functools.reduce(jnp.add, [dot_t(ones, part) for part in split3(mix * mix)])
     sums = jnp.concatenate([sums, jnp.zeros_like(sums)], axis=1)
-    for i in range(squares_ref.shape[0]):
-        squares_ref[i] = sums[0:1]
-
-
-def final_kernel(model_width, mix_ref, squares_ref, gain_ref, out_ref):
-    total = squares_ref[0]
-    for i in range(1, squares_ref.shape[0]):
-        total += squares_ref[i]
+    squares_ref[...] = sums
+
+
+def final_kernel(model_width, mix_ref, squares_ref, other_ref, gain_ref, out_ref):
+    total = squares_ref[0:1, :] + other_ref[0:1, :]
     mix = mix_ref[...]
     tokens = mix.shape[0]
     wide = jnp.broadcast_to(total, (tokens, total.shape[1]))
@@ -272,6 +269,14 @@
     def onward(value):
         pairs = [
             (y * CORES + c, ((y + 1 - 2 * c) % chips) * CORES + c)
+            for y in range(chips)
+            for c in range(CORES)
+        ]
+        return lax.ppermute(value, "tp", pairs)
+
+    def along(value, step):
+        pairs = [
+            (y * CORES + c, ((y + step) % chips) * CORES + c)
             for y in range(chips)
             for c in range(CORES)
         ]
@@ -413,16 +418,18 @@
     returned = lax.all_to_all(expert_out, "ep", split_axis=0, concat_axis=0, tiled=True)
     mixture, squares = call(
         combine_kernel,
-        [shape_of((tok_rows, width), jnp.float32), shape_of((peers, 1, 128), jnp.float32)],
+        [shape_of((tok_rows, width), jnp.float32), shape_of((8, 128), jnp.float32)],
         share,
         returned.reshape(rows, width),
     )
-    squares = lax.all_to_all(squares, "tp", split_axis=0, concat_axis=0, tiled=True)
+    around = [along(squares, step) for step in (2, 1, chips - 1)]
+    squares = functools.reduce(jnp.add, around, squares)
     return call(
         functools.partial(final_kernel, model_width),
         shape_of((tok_rows, width), jnp.bfloat16),
         mixture,
         squares,
+        swap(squares),
         final_gain,
     )
 

time: 93.4 us -> 92.7 us (level)
  blocking collectives: 26 us -> 13.9 us
  starting transfers between devices: 35.7 us -> 44.6 us
  waiting for transfers between devices: 23.2 us -> 25.6 us
    all_to_all x1 -> x0, blocking collectives: 12 us -> none  [local(): lax.all_to_all(squares, 'tp', split_axis=0, concat_axis=0, tiled=True)]
    ppermute x10 -> x11, starting transfers between devices: 13.5 us -> 18.8 us  [swap(): return lax.ppermute(value, 'tp', pairs)]
    ppermute x0 -> x3, starting transfers between devices: none -> 3.71 us  [along(): return lax.ppermute(value, 'tp', pairs)]
    ppermute x0 -> x3, waiting for transfers between devices: none -> 1.6 us  [along(): return lax.ppermute(value, 'tp', pairs)]
    ppermute x10 -> x11, waiting for transfers between devices: 1.48 us -> 2.3 us  [swap(): return lax.ppermute(value, 'tp', pairs)]
  transfers between devices with their start and end apart: 21 -> 25, of which waited for: 8 -> 12; matrix products, arithmetic and copies ran while one was open for 0% -> 0% of each run, Pallas kernels for 5% -> 5%
where the time goes in v3:
time: 92.7 us; the launch traced here: 92.4 us
  starting transfers between devices  44.6 us (48%)
  waiting for transfers between devices  25.6 us (28%)
  blocking collectives  13.9 us (15%)
  Pallas kernels  8.02 us (9%)
    ppermute x11, starting transfers between devices, swap(): return lax.ppermute(value, 'tp', pairs)  18.8 us
    all_to_all x1, blocking collectives, local(): lax.all_to_all(expert_out, 'ep', split_axis=0, concat_axis=0, tiled=True)  13.9 us
    all_to_all x1, starting transfers between devices, local(): lax.all_to_all(outbound.reshape(experts, capacity, width), 'ep', split_ax...  11.9 us
    ppermute x10, waiting for transfers between devices, onward(): return lax.ppermute(value, 'tp', pairs)  11.5 us
    all_to_all x1, waiting for transfers between devices, local(): lax.all_to_all(outbound.reshape(experts, capacity, width), 'ep', split_ax...  10.3 us
    ppermute x10, starting transfers between devices, onward(): return lax.ppermute(value, 'tp', pairs)  10.3 us
    pallas_call x13, Pallas kernels, call(): pl.pallas_call(kernel, out_shape=outs, in_specs=[space] * len(args), out_...  8.02 us
    ppermute x3, starting transfers between devices, along(): return lax.ppermute(value, 'tp', pairs)  3.71 us
  transfers between devices with their start and end apart: 25, of which 12 were waited for; matrix products, arithmetic and copies ran while one was open for 0% of the time, Pallas kernels for 5%

profile of v3, /device:TPU:1, one launch (start us, length us, event | category | flops | bytes accessed | tf_op | source)
XLA Modules:
  0.0 92.4 jit_solution(1188599954674311819)
XLA Ops:
  0.0 1.9 %shard_map.83 = (bf16[512,256]{1,0:T(8,128)(2,1)}, f32[1,256]{1,0:T(1,128)S(1)}) custom-call(s32[4,64]{1,0:T(4,128)} %bitcast.23, bf16[64,256]{1,0:T(8,128)(2,1)} %tokens_hbm.1, f32[1,256]{1,0:T(1,128)} %bitcast.27), custom_call_target="tpu_custom_call" | custom-call | tf_op jit(solution)/shard_map/pallas_call | solution.py:245
  1.9 11.9 %all-to-all-start = ((bf16[32,16,256]{2,1,0:T(8,128)(2,1)}), bf16[32,16,256]{2,1,0:T(8,128)(2,1)S(1)}, u32[]{:S(2)}, u32[]{:S(2)}) async-start(bf16[32,16,256]{2,1,0:T(8,128)(2,1)} %bitcast.5), calls=%async_computation | async-start | bytes 524288 | tf_op jit(solution)/shard_map/all_to_all | solution.py:304
  13.7 1.0 %collective-permute-start.13 = (bf16[256,2048]{1,0:T(8,128)(2,1)}, bf16[256,2048]{1,0:T(8,128)(2,1)S(1)}, u32[]{:S(2)}, u32[]{:S(2)}) collective-permute-start(bf16[256,2048]{1,0:T(8,128)(2,1)} %bitcast.15), channel_id=1, source_target_pairs={{0,1},{1,0},{2,3},{3,2},{4,5},{5,4},{6,7},{7,6},{8,9},{9,8},{10,11... | collective-permute-start | bytes 3145736 | tf_op jit(solution)/shard_map/ppermute | solution.py:287
  14.8 10.3 %all-to-all-done = bf16[32,16,256]{2,1,0:T(8,128)(2,1)S(1)} async-done(((bf16[32,16,256]{2,1,0:T(8,128)(2,1)}), bf16[32,16,256]{2,1,0:T(8,128)(2,1)S(1)}, u32[]{:S(2)}, u32[]{:S(2)}) %all-to-all-start) | async-done | bytes 262176 | tf_op jit(solution)/shard_map/all_to_all | solution.py:304
  25.4 2.5 %collective-permute-start.3 = (bf16[528,256]{1,0:T(8,128)(2,1)S(1)}, bf16[528,256]{1,0:T(8,128)(2,1)S(1)}, u32[]{:S(2)}, u32[]{:S(2)}) collective-permute-start(bf16[528,256]{1,0:T(8,128)(2,1)S(1)} %get-tuple-element.30.refs_0_), channel_id=1, source_target_pairs={{0,1},{1,0},{2,3},{3,2},{4,5},{5,4},{6,7},{7,6},{8,9},{9,8},{10,11... | collective-permute-start | bytes 811016 | tf_op jit(solution)/shard_map/ppermute | solution.py:287
  27.9 1.2 %collective-permute-done.3.refs_1_ = bf16[528,256]{1,0:T(8,128)(2,1)S(1)} collective-permute-done((bf16[528,256]{1,0:T(8,128)(2,1)S(1)}, bf16[528,256]{1,0:T(8,128)(2,1)S(1)}, u32[]{:S(2)}, u32[]{:S(2)}) %collective-permute-start.3) | collective-permute-done | bytes 270368 | tf_op jit(solution)/shard_map/ppermute | solution.py:287
  29.1 2.7 %collective-permute-start.4 = (bf16[528,256]{1,0:T(8,128)(2,1)S(1)}, bf16[528,256]{1,0:T(8,128)(2,1)S(1)}, u32[]{:S(2)}, u32[]{:S(2)}) collective-permute-start(bf16[528,256]{1,0:T(8,128)(2,1)S(1)} %collective-permute-done.3.refs_1_), channel_id=1, source_target_pairs={{0,2},{1,7},{2,4},{3,1},{4,6},{5,3},{6,0},{7,5},{8,10},{9,15},{10,... | collective-permute-start | bytes 811016 | tf_op jit(solution)/shard_map/ppermute | solution.py:275
  32.4 4.2 %collective-permute-done.6.refs_3_ = bf16[256,256]{1,0:T(8,128)(2,1)S(1)} collective-permute-done((bf16[256,256]{1,0:T(8,128)(2,1)S(1)}, bf16[256,256]{1,0:T(8,128)(2,1)S(1)}, u32[]{:S(2)}, u32[]{:S(2)}) %collective-permute-start.6) | collective-permute-done | bytes 131104 | tf_op jit(solution)/shard_map/ppermute | solution.py:275
  36.6 1.9 %collective-permute-start.8 = (bf16[256,256]{1,0:T(8,128)(2,1)S(1)}, bf16[256,256]{1,0:T(8,128)(2,1)S(1)}, u32[]{:S(2)}, u32[]{:S(2)}) collective-permute-start(bf16[256,256]{1,0:T(8,128)(2,1)S(1)} %collective-permute-done.6.refs_3_), channel_id=1, source_target_pairs={{0,1},{1,0},{2,3},{3,2},{4,5},{5,4},{6,7},{7,6},{8,9},{9,8},{10,11... | collective-permute-start | bytes 393224 | tf_op jit(solution)/shard_map/ppermute | solution.py:287
  38.5 2.7 %collective-permute-start.1 = (bf16[272,256]{1,0:T(8,128)(2,1)S(1)}, bf16[272,256]{1,0:T(8,128)(2,1)S(1)}, u32[]{:S(2)}, u32[]{:S(2)}) collective-permute-start(bf16[272,256]{1,0:T(8,128)(2,1)S(1)} %collective-permute-done.refs_2_), channel_id=1, source_target_pairs={{0,2},{1,7},{2,4},{3,1},{4,6},{5,3},{6,0},{7,5},{8,10},{9,15},{10,... | collective-permute-start | bytes 417800 | tf_op jit(solution)/shard_map/ppermute | solution.py:275
  41.2 0.7 collective-permute-start.7
  42.0 1.3 %collective-permute-done.1.refs_0_ = bf16[272,256]{1,0:T(8,128)(2,1)S(1)} collective-permute-done((bf16[272,256]{1,0:T(8,128)(2,1)S(1)}, bf16[272,256]{1,0:T(8,128)(2,1)S(1)}, u32[]{:S(2)}, u32[]{:S(2)}) %collective-permute-start.1) | collective-permute-done | bytes 139296 | tf_op jit(solution)/shard_map/ppermute | solution.py:275
  43.2 3.0 %collective-permute-start.2 = (bf16[272,256]{1,0:T(8,128)(2,1)S(1)}, bf16[272,256]{1,0:T(8,128)(2,1)S(1)}, u32[]{:S(2)}, u32[]{:S(2)}) collective-permute-start(bf16[272,256]{1,0:T(8,128)(2,1)S(1)} %collective-permute-done.1.refs_0_), channel_id=1, source_target_pairs={{0,1},{1,0},{2,3},{3,2},{4,5},{5,4},{6,7},{7,6},{8,9},{9,8},{10,11... | collective-permute-start | bytes 417800 | tf_op jit(solution)/shard_map/ppermute | solution.py:287
  46.3 1.4 %collective-permute-start.11 = (bf16[256,256]{1,0:T(8,128)(2,1)S(1)}, bf16[256,256]{1,0:T(8,128)(2,1)S(1)}, u32[]{:S(2)}, u32[]{:S(2)}) collective-permute-start(bf16[256,256]{1,0:T(8,128)(2,1)S(1)} %collective-permute-done.10.refs_1_), channel_id=1, source_target_pairs={{0,1},{1,0},{2,3},{3,2},{4,5},{5,4},{6,7},{7,6},{8,9},{9,8},{10,11... | collective-permute-start | bytes 393224 | tf_op jit(solution)/shard_map/ppermute | solution.py:287
  47.7 1.3 %shard_map.82 = (bf16[192,512]{1,0:T(8,128)(2,1)S(1)}, f32[1,256]{1,0:T(1,128)S(1)}, bf16[2048,256]{1,0:T(8,128)(2,1)S(1)}) custom-call(s32[4,64]{1,0:T(4,128)} %bitcast.24, f32[4,64]{1,0:T(4,128)} %bitcast.25, f32[1,256]{1,0:T(1,128)} %bitcast.26, bf16[2048,256]{1,0:T(8,128)(2,1)} %bitcast.22), custom_call_target="tpu_custom_call" | custom-call | tf_op jit(solution)/shard_map/pallas_call | solution.py:245
  49.0 0.9 shard_map.85
  52.6 0.6 collective-permute-start.18
  53.2 0.6 shard_map.89
  54.9 1.8 %collective-permute-done.18 = bf16[256,256]{1,0:T(8,128)(2,1)S(1)} collective-permute-done((bf16[256,256]{1,0:T(8,128)(2,1)S(1)}, bf16[256,256]{1,0:T(8,128)(2,1)S(1)}, u32[]{:S(2)}, u32[]{:S(2)}) %collective-permute-start.18) | collective-permute-done | bytes 131104 | tf_op jit(solution)/shard_map/ppermute | solution.py:275
  56.7 1.6 %collective-permute-start.19 = (bf16[256,256]{1,0:T(8,128)(2,1)S(1)}, bf16[256,256]{1,0:T(8,128)(2,1)S(1)}, u32[]{:S(2)}, u32[]{:S(2)}) collective-permute-start(bf16[256,256]{1,0:T(8,128)(2,1)S(1)} %add_convert_fusion), channel_id=1, source_target_pairs={{0,2},{1,7},{2,4},{3,1},{4,6},{5,3},{6,0},{7,5},{8,10},{9,15},{10,... | collective-permute-start | bytes 393224 | tf_op jit(solution)/shard_map/ppermute | solution.py:275
  58.3 1.5 %collective-permute-done.14 = bf16[512,256]{1,0:T(8,128)(2,1)S(1)} collective-permute-done((bf16[512,256]{1,0:T(8,128)(2,1)S(1)}, bf16[512,256]{1,0:T(8,128)(2,1)S(1)}, u32[]{:S(2)}, u32[]{:S(2)}) %collective-permute-start.14) | collective-permute-done | bytes 262176 | tf_op jit(solution)/shard_map/ppermute | solution.py:275
  59.8 2.2 %collective-permute-start.15 = (bf16[512,256]{1,0:T(8,128)(2,1)S(1)}, bf16[512,256]{1,0:T(8,128)(2,1)S(1)}, u32[]{:S(2)}, u32[]{:S(2)}) collective-permute-start(bf16[512,256]{1,0:T(8,128)(2,1)S(1)} %collective-permute-done.14), channel_id=1, source_target_pairs={{0,1},{1,0},{2,3},{3,2},{4,5},{5,4},{6,7},{7,6},{8,9},{9,8},{10,11... | collective-permute-start | bytes 786440 | tf_op jit(solution)/shard_map/ppermute | solution.py:287
  62.1 1.1 %collective-permute-start.17 = (bf16[256,256]{1,0:T(8,128)(2,1)S(1)}, bf16[256,256]{1,0:T(8,128)(2,1)S(1)}, u32[]{:S(2)}, u32[]{:S(2)}) collective-permute-start(bf16[256,256]{1,0:T(8,128)(2,1)S(1)} %add_convert_fusion.1), channel_id=1, source_target_pairs={{0,2},{1,7},{2,4},{3,1},{4,6},{5,3},{6,0},{7,5},{8,10},{9,15},{10,... | collective-permute-start | bytes 393224 | tf_op jit(solution)/shard_map/ppermute | solution.py:275
  63.2 2.8 %collective-permute-done.17.near_a_ref = bf16[256,256]{1,0:T(8,128)(2,1)S(1)} collective-permute-done((bf16[256,256]{1,0:T(8,128)(2,1)S(1)}, bf16[256,256]{1,0:T(8,128)(2,1)S(1)}, u32[]{:S(2)}, u32[]{:S(2)}) %collective-permute-start.17) | collective-permute-done | bytes 131104 | tf_op jit(solution)/shard_map/ppermute | solution.py:275
  66.1 13.9 %all_to_all.10 = bf16[32,16,256]{2,1,0:T(8,128)(2,1)S(1)} all-to-all(bf16[32,16,256]{2,1,0:T(8,128)(2,1)S(1)} %bitcast.21), channel_id=1, replica_groups=mesh['ep'=32,'tp'=8] {'ep'}, dimensions={0} | all-to-all | bytes 524288 | tf_op jit(solution)/shard_map/all_to_all | solution.py:418
  80.4 1.0 %collective-permute-start.20 = (f32[8,128]{1,0:T(8,128)S(1)}, f32[8,128]{1,0:T(8,128)S(1)}, u32[]{:S(2)}, u32[]{:S(2)}) collective-permute-start(f32[8,128]{1,0:T(8,128)S(1)} %get-tuple-element.43), channel_id=1, source_target_pairs={{0,4},{1,5},{2,6},{3,7},{4,0},{5,1},{6,2},{7,3},{8,12},{9,13},{10,... | collective-permute-start | bytes 12296 | tf_op jit(solution)/shard_map/ppermute | solution.py:283
  81.4 1.8 %collective-permute-start.21 = (f32[8,128]{1,0:T(8,128)S(1)}, f32[8,128]{1,0:T(8,128)S(1)}, u32[]{:S(2)}, u32[]{:S(2)}) collective-permute-start(f32[8,128]{1,0:T(8,128)S(1)} %get-tuple-element.43), channel_id=1, source_target_pairs={{0,2},{1,3},{2,4},{3,5},{4,6},{5,7},{6,0},{7,1},{8,10},{9,11},{10,... | collective-permute-start | bytes 12296 | tf_op jit(solution)/shard_map/ppermute | solution.py:283
  83.2 0.9 collective-permute-start.22
  85.1 0.6 collective-permute-done.22
  85.7 5.2 %collective-permute-start.23 = (f32[8,128]{1,0:T(8,128)S(1)}, f32[8,128]{1,0:T(8,128)S(1)}, u32[]{:S(2)}, u32[]{:S(2)}) collective-permute-start(f32[8,128]{1,0:T(8,128)S(1)} %add_add_fusion.squares_ref), channel_id=1, source_target_pairs={{0,1},{1,0},{2,3},{3,2},{4,5},{5,4},{6,7},{7,6},{8,9},{9,8},{10,11... | collective-permute-start | bytes 12296 | tf_op jit(solution)/shard_map/ppermute | solution.py:287
  90.9 0.8 collective-permute-done.23.other_ref
  91.7 0.7 shard_map.94
  (39 shorter events, 6.3 us)
Async XLA Ops:
  0.0 49.0 %copy-start = (bf16[1,2048,256]{2,1,0:T(8,128)(2,1)S(1)}, bf16[1,2048,256]{2,1,0:T(8,128)(2,1)}, u32[]{:S(2)}) copy-start(bf16[1,2048,256]{2,1,0:T(8,128)(2,1)} %param.12) | copy-start | bytes 3145732
  1.9 23.2 %all-to-all-start = ((bf16[32,16,256]{2,1,0:T(8,128)(2,1)}), bf16[32,16,256]{2,1,0:T(8,128)(2,1)S(1)}, u32[]{:S(2)}, u32[]{:S(2)}) async-start(bf16[32,16,256]{2,1,0:T(8,128)(2,1)} %bitcast.5), calls=%async_computation | async-start | bytes 524288 | tf_op jit(solution)/shard_map/all_to_all | solution.py:304
  13.7 38.4 %collective-permute-start.13 = (bf16[256,2048]{1,0:T(8,128)(2,1)}, bf16[256,2048]{1,0:T(8,128)(2,1)S(1)}, u32[]{:S(2)}, u32[]{:S(2)}) collective-permute-start(bf16[256,2048]{1,0:T(8,128)(2,1)} %bitcast.15), channel_id=1, source_target_pairs={{0,1},{1,0},{2,3},{3,2},{4,5},{5,4},{6,7},{7,6},{8,9},{9,8},{10,11... | collective-permute-start | bytes 3145736 | tf_op jit(solution)/shard_map/ppermute | solution.py:287
  25.4 3.7 %collective-permute-start.3 = (bf16[528,256]{1,0:T(8,128)(2,1)S(1)}, bf16[528,256]{1,0:T(8,128)(2,1)S(1)}, u32[]{:S(2)}, u32[]{:S(2)}) collective-permute-start(bf16[528,256]{1,0:T(8,128)(2,1)S(1)} %get-tuple-element.30.refs_0_), channel_id=1, source_target_pairs={{0,1},{1,0},{2,3},{3,2},{4,5},{5,4},{6,7},{7,6},{8,9},{9,8},{10,11... | collective-permute-start | bytes 811016 | tf_op jit(solution)/shard_map/ppermute | solution.py:287
  29.1 9.5 %collective-permute-start.4 = (bf16[528,256]{1,0:T(8,128)(2,1)S(1)}, bf16[528,256]{1,0:T(8,128)(2,1)S(1)}, u32[]{:S(2)}, u32[]{:S(2)}) collective-permute-start(bf16[528,256]{1,0:T(8,128)(2,1)S(1)} %collective-permute-done.3.refs_1_), channel_id=1, source_target_pairs={{0,2},{1,7},{2,4},{3,1},{4,6},{5,3},{6,0},{7,5},{8,10},{9,15},{10,... | collective-permute-start | bytes 811016 | tf_op jit(solution)/shard_map/ppermute | solution.py:275
  31.8 4.8 %collective-permute-start.6 = (bf16[256,256]{1,0:T(8,128)(2,1)S(1)}, bf16[256,256]{1,0:T(8,128)(2,1)S(1)}, u32[]{:S(2)}, u32[]{:S(2)}) collective-permute-start(bf16[256,256]{1,0:T(8,128)(2,1)S(1)} %get-tuple-element.31), channel_id=1, source_target_pairs={{0,2},{1,7},{2,4},{3,1},{4,6},{5,3},{6,0},{7,5},{8,10},{9,15},{10,... | collective-permute-start | bytes 393224 | tf_op jit(solution)/shard_map/ppermute | solution.py:275
  32.3 6.3 %collective-permute-start = (bf16[272,256]{1,0:T(8,128)(2,1)S(1)}, bf16[272,256]{1,0:T(8,128)(2,1)S(1)}, u32[]{:S(2)}, u32[]{:S(2)}) collective-permute-start(bf16[272,256]{1,0:T(8,128)(2,1)S(1)} %get-tuple-element.28), channel_id=1, source_target_pairs={{0,2},{1,7},{2,4},{3,1},{4,6},{5,3},{6,0},{7,5},{8,10},{9,15},{10,... | collective-permute-start | bytes 417800 | tf_op jit(solution)/shard_map/ppermute | solution.py:275
  36.6 4.6 %collective-permute-start.8 = (bf16[256,256]{1,0:T(8,128)(2,1)S(1)}, bf16[256,256]{1,0:T(8,128)(2,1)S(1)}, u32[]{:S(2)}, u32[]{:S(2)}) collective-permute-start(bf16[256,256]{1,0:T(8,128)(2,1)S(1)} %collective-permute-done.6.refs_3_), channel_id=1, source_target_pairs={{0,1},{1,0},{2,3},{3,2},{4,5},{5,4},{6,7},{7,6},{8,9},{9,8},{10,11... | collective-permute-start | bytes 393224 | tf_op jit(solution)/shard_map/ppermute | solution.py:287
  38.5 11.4 %collective-permute-start.5 = (bf16[528,256]{1,0:T(8,128)(2,1)S(1)}, bf16[528,256]{1,0:T(8,128)(2,1)S(1)}, u32[]{:S(2)}, u32[]{:S(2)}) collective-permute-start(bf16[528,256]{1,0:T(8,128)(2,1)S(1)} %collective-permute-done.4.refs_0_), channel_id=1, source_target_pairs={{0,1},{1,0},{2,3},{3,2},{4,5},{5,4},{6,7},{7,6},{8,9},{9,8},{10,11... | collective-permute-start | bytes 811016 | tf_op jit(solution)/shard_map/ppermute | solution.py:287
  38.5 4.7 %collective-permute-start.1 = (bf16[272,256]{1,0:T(8,128)(2,1)S(1)}, bf16[272,256]{1,0:T(8,128)(2,1)S(1)}, u32[]{:S(2)}, u32[]{:S(2)}) collective-permute-start(bf16[272,256]{1,0:T(8,128)(2,1)S(1)} %collective-permute-done.refs_2_), channel_id=1, source_target_pairs={{0,2},{1,7},{2,4},{3,1},{4,6},{5,3},{6,0},{7,5},{8,10},{9,15},{10,... | collective-permute-start | bytes 417800 | tf_op jit(solution)/shard_map/ppermute | solution.py:275
  41.2 5.1 %collective-permute-start.10 = (bf16[256,256]{1,0:T(8,128)(2,1)S(1)}, bf16[256,256]{1,0:T(8,128)(2,1)S(1)}, u32[]{:S(2)}, u32[]{:S(2)}) collective-permute-start(bf16[256,256]{1,0:T(8,128)(2,1)S(1)} %collective-permute-done.6.refs_3_), channel_id=1, source_target_pairs={{0,2},{1,7},{2,4},{3,1},{4,6},{5,3},{6,0},{7,5},{8,10},{9,15},{10,... | collective-permute-start | bytes 393224 | tf_op jit(solution)/shard_map/ppermute | solution.py:275
  41.2 7.8 %collective-permute-start.7 = (bf16[272,256]{1,0:T(8,128)(2,1)S(1)}, bf16[272,256]{1,0:T(8,128)(2,1)S(1)}, u32[]{:S(2)}, u32[]{:S(2)}) collective-permute-start(bf16[272,256]{1,0:T(8,128)(2,1)S(1)} %collective-permute-done.refs_2_), channel_id=1, source_target_pairs={{0,1},{1,0},{2,3},{3,2},{4,5},{5,4},{6,7},{7,6},{8,9},{9,8},{10,11... | collective-permute-start | bytes 417800 | tf_op jit(solution)/shard_map/ppermute | solution.py:287
  43.2 7.2 %collective-permute-start.2 = (bf16[272,256]{1,0:T(8,128)(2,1)S(1)}, bf16[272,256]{1,0:T(8,128)(2,1)S(1)}, u32[]{:S(2)}, u32[]{:S(2)}) collective-permute-start(bf16[272,256]{1,0:T(8,128)(2,1)S(1)} %collective-permute-done.1.refs_0_), channel_id=1, source_target_pairs={{0,1},{1,0},{2,3},{3,2},{4,5},{5,4},{6,7},{7,6},{8,9},{9,8},{10,11... | collective-permute-start | bytes 417800 | tf_op jit(solution)/shard_map/ppermute | solution.py:287
  46.3 4.2 %collective-permute-start.11 = (bf16[256,256]{1,0:T(8,128)(2,1)S(1)}, bf16[256,256]{1,0:T(8,128)(2,1)S(1)}, u32[]{:S(2)}, u32[]{:S(2)}) collective-permute-start(bf16[256,256]{1,0:T(8,128)(2,1)S(1)} %collective-permute-done.10.refs_1_), channel_id=1, source_target_pairs={{0,1},{1,0},{2,3},{3,2},{4,5},{5,4},{6,7},{7,6},{8,9},{9,8},{10,11... | collective-permute-start | bytes 393224 | tf_op jit(solution)/shard_map/ppermute | solution.py:287
  50.9 1.4 %copy-start.1 = (bf16[1,256,2048]{2,1,0:T(8,128)(2,1)S(1)}, bf16[1,256,2048]{2,1,0:T(8,128)(2,1)}, u32[]{:S(2)}) copy-start(bf16[1,256,2048]{2,1,0:T(8,128)(2,1)} %param.14) | copy-start | bytes 3145732
  50.9 1.4 %collective-permute-start.12 = (bf16[256,256]{1,0:T(8,128)(2,1)S(1)}, bf16[256,256]{1,0:T(8,128)(2,1)S(1)}, u32[]{:S(2)}, u32[]{:S(2)}) collective-permute-start(bf16[256,256]{1,0:T(8,128)(2,1)S(1)} %shard_map.88.refs_2_.own_ref), channel_id=1, source_target_pairs={{0,1},{1,0},{2,3},{3,2},{4,5},{5,4},{6,7},{7,6},{8,9},{9,8},{10,11... | collective-permute-start | bytes 393224 | tf_op jit(solution)/shard_map/ppermute | solution.py:287
  51.5 1.7 %collective-permute-start.9 = (bf16[256,256]{1,0:T(8,128)(2,1)S(1)}, bf16[256,256]{1,0:T(8,128)(2,1)S(1)}, u32[]{:S(2)}, u32[]{:S(2)}) collective-permute-start(bf16[256,256]{1,0:T(8,128)(2,1)S(1)} %shard_map.87.refs_0_.own_ref), channel_id=1, source_target_pairs={{0,1},{1,0},{2,3},{3,2},{4,5},{5,4},{6,7},{7,6},{8,9},{9,8},{10,11... | collective-permute-start | bytes 393224 | tf_op jit(solution)/shard_map/ppermute | solution.py:287
  52.6 4.1 %collective-permute-start.18 = (bf16[256,256]{1,0:T(8,128)(2,1)S(1)}, bf16[256,256]{1,0:T(8,128)(2,1)S(1)}, u32[]{:S(2)}, u32[]{:S(2)}) collective-permute-start(bf16[256,256]{1,0:T(8,128)(2,1)S(1)} %shard_map.91), channel_id=1, source_target_pairs={{0,2},{1,7},{2,4},{3,1},{4,6},{5,3},{6,0},{7,5},{8,10},{9,15},{10,... | collective-permute-start | bytes 393224 | tf_op jit(solution)/shard_map/ppermute | solution.py:275
  53.8 6.0 %collective-permute-start.14 = (bf16[512,256]{1,0:T(8,128)(2,1)S(1)}, bf16[512,256]{1,0:T(8,128)(2,1)S(1)}, u32[]{:S(2)}, u32[]{:S(2)}) collective-permute-start(bf16[512,256]{1,0:T(8,128)(2,1)S(1)} %get-tuple-element.39), channel_id=1, source_target_pairs={{0,2},{1,7},{2,4},{3,1},{4,6},{5,3},{6,0},{7,5},{8,10},{9,15},{10,... | collective-permute-start | bytes 786440 | tf_op jit(solution)/shard_map/ppermute | solution.py:275
  54.6 7.5 %collective-permute-start.16 = (bf16[256,256]{1,0:T(8,128)(2,1)S(1)}, bf16[256,256]{1,0:T(8,128)(2,1)S(1)}, u32[]{:S(2)}, u32[]{:S(2)}) collective-permute-start(bf16[256,256]{1,0:T(8,128)(2,1)S(1)} %shard_map.90), channel_id=1, source_target_pairs={{0,2},{1,7},{2,4},{3,1},{4,6},{5,3},{6,0},{7,5},{8,10},{9,15},{10,... | collective-permute-start | bytes 393224 | tf_op jit(solution)/shard_map/ppermute | solution.py:275
  56.7 6.4 %collective-permute-start.19 = (bf16[256,256]{1,0:T(8,128)(2,1)S(1)}, bf16[256,256]{1,0:T(8,128)(2,1)S(1)}, u32[]{:S(2)}, u32[]{:S(2)}) collective-permute-start(bf16[256,256]{1,0:T(8,128)(2,1)S(1)} %add_convert_fusion), channel_id=1, source_target_pairs={{0,2},{1,7},{2,4},{3,1},{4,6},{5,3},{6,0},{7,5},{8,10},{9,15},{10,... | collective-permute-start | bytes 393224 | tf_op jit(solution)/shard_map/ppermute | solution.py:275
  59.8 6.2 %collective-permute-start.15 = (bf16[512,256]{1,0:T(8,128)(2,1)S(1)}, bf16[512,256]{1,0:T(8,128)(2,1)S(1)}, u32[]{:S(2)}, u32[]{:S(2)}) collective-permute-start(bf16[512,256]{1,0:T(8,128)(2,1)S(1)} %collective-permute-done.14), channel_id=1, source_target_pairs={{0,1},{1,0},{2,3},{3,2},{4,5},{5,4},{6,7},{7,6},{8,9},{9,8},{10,11... | collective-permute-start | bytes 786440 | tf_op jit(solution)/shard_map/ppermute | solution.py:287
  62.1 3.9 %collective-permute-start.17 = (bf16[256,256]{1,0:T(8,128)(2,1)S(1)}, bf16[256,256]{1,0:T(8,128)(2,1)S(1)}, u32[]{:S(2)}, u32[]{:S(2)}) collective-permute-start(bf16[256,256]{1,0:T(8,128)(2,1)S(1)} %add_convert_fusion.1), channel_id=1, source_target_pairs={{0,2},{1,7},{2,4},{3,1},{4,6},{5,3},{6,0},{7,5},{8,10},{9,15},{10,... | collective-permute-start | bytes 393224 | tf_op jit(solution)/shard_map/ppermute | solution.py:275
  80.4 4.3 %collective-permute-start.20 = (f32[8,128]{1,0:T(8,128)S(1)}, f32[8,128]{1,0:T(8,128)S(1)}, u32[]{:S(2)}, u32[]{:S(2)}) collective-permute-start(f32[8,128]{1,0:T(8,128)S(1)} %get-tuple-element.43), channel_id=1, source_target_pairs={{0,4},{1,5},{2,6},{3,7},{4,0},{5,1},{6,2},{7,3},{8,12},{9,13},{10,... | collective-permute-start | bytes 12296 | tf_op jit(solution)/shard_map/ppermute | solution.py:283
  81.4 3.7 %collective-permute-start.21 = (f32[8,128]{1,0:T(8,128)S(1)}, f32[8,128]{1,0:T(8,128)S(1)}, u32[]{:S(2)}, u32[]{:S(2)}) collective-permute-start(f32[8,128]{1,0:T(8,128)S(1)} %get-tuple-element.43), channel_id=1, source_target_pairs={{0,2},{1,3},{2,4},{3,5},{4,6},{5,7},{6,0},{7,1},{8,10},{9,11},{10,... | collective-permute-start | bytes 12296 | tf_op jit(solution)/shard_map/ppermute | solution.py:283
  83.2 2.5 %collective-permute-start.22 = (f32[8,128]{1,0:T(8,128)S(1)}, f32[8,128]{1,0:T(8,128)S(1)}, u32[]{:S(2)}, u32[]{:S(2)}) collective-permute-start(f32[8,128]{1,0:T(8,128)S(1)} %get-tuple-element.43), channel_id=1, source_target_pairs={{0,6},{1,7},{2,0},{3,1},{4,2},{5,3},{6,4},{7,5},{8,14},{9,15},{10,... | collective-permute-start | bytes 12296 | tf_op jit(solution)/shard_map/ppermute | solution.py:283
  85.7 6.0 %collective-permute-start.23 = (f32[8,128]{1,0:T(8,128)S(1)}, f32[8,128]{1,0:T(8,128)S(1)}, u32[]{:S(2)}, u32[]{:S(2)}) collective-permute-start(f32[8,128]{1,0:T(8,128)S(1)} %add_add_fusion.squares_ref), channel_id=1, source_target_pairs={{0,1},{1,0},{2,3},{3,2},{4,5},{5,4},{6,7},{7,6},{8,9},{9,8},{10,11... | collective-permute-start | bytes 12296 | tf_op jit(solution)/shard_map/ppermute | solution.py:287

commit v4 on v3

--- a/solution.py
+++ b/solution.py
@@ -226,8 +226,8 @@
     squares_ref[...] = sums
 
 
-def final_kernel(model_width, mix_ref, squares_ref, other_ref, gain_ref, out_ref):
-    total = squares_ref[0:1, :] + other_ref[0:1, :]
+def final_kernel(model_width, mix_ref, squares_ref, around_ref, other_ref, gain_ref, out_ref):
+    total = squares_ref[0:1, :] + around_ref[0:1, :] + other_ref[0:1, :]
     mix = mix_ref[...]
     tokens = mix.shape[0]
     wide = jnp.broadcast_to(total, (tokens, total.shape[1]))
@@ -274,11 +274,10 @@
         ]
         return lax.ppermute(value, "tp", pairs)
 
-    def along(value, step):
+    def opposite(value):
+        last = CORES - 1
         pairs = [
-            (y * CORES + c, ((y + step) % chips) * CORES + c)
-            for y in range(chips)
-            for c in range(CORES)
+            (y * CORES + last, ((y + chips // 2) % chips) * CORES + last) for y in range(chips)
         ]
         return lax.ppermute(value, "tp", pairs)
 
@@ -422,14 +421,16 @@
         share,
         returned.reshape(rows, width),
     )
-    around = [along(squares, step) for step in (2, 1, chips - 1)]
-    squares = functools.reduce(jnp.add, around, squares)
+    squares += swap(squares)
+    across = opposite(squares)
+    around = onward(squares) + across
     return call(
         functools.partial(final_kernel, model_width),
         shape_of((tok_rows, width), jnp.bfloat16),
         mixture,
         squares,
-        swap(squares),
+        around,
+        swap(around),
         final_gain,
     )
 

time: 92.7 us -> 95 us (1.025)
  waiting for transfers between devices: 25.6 us -> 29.1 us
  starting transfers between devices: 44.6 us -> 43.4 us
    ppermute x3 -> x1, waiting for transfers between devices: 1.6 us -> 3.92 us  [opposite(): return lax.ppermute(value, 'tp', pairs)]
    ppermute x3 -> x1, starting transfers between devices: 3.71 us -> 1.91 us  [opposite(): return lax.ppermute(value, 'tp', pairs)]
    ppermute x11 -> x12, waiting for transfers between devices: 2.3 us -> 3.47 us  [swap(): return lax.ppermute(value, 'tp', pairs)]
    ppermute x10 -> x11, starting transfers between devices: 10.3 us -> 11 us  [onward(): return lax.ppermute(value, 'tp', pairs)]
    ppermute x11 -> x12, starting transfers between devices: 18.8 us -> 18.6 us  [swap(): return lax.ppermute(value, 'tp', pairs)]
    ppermute x10 -> x11, waiting for transfers between devices: 11.5 us -> 11.5 us  [onward(): return lax.ppermute(value, 'tp', pairs)]
  transfers between devices with their start and end apart: 25 -> 25, of which waited for: 12 -> 11; matrix products, arithmetic and copies ran while one was open for 0% -> 0% of each run, Pallas kernels for 5% -> 5%
where the time goes in v4:
time: 95 us; the launch traced here: 94.7 us
  starting transfers between devices  43.4 us (46%)
  waiting for transfers between devices  29.1 us (31%)
  blocking collectives  13.9 us (15%)
  Pallas kernels  8.02 us (8%)
    ppermute x12, starting transfers between devices, swap(): return lax.ppermute(value, 'tp', pairs)  18.6 us
    all_to_all x1, blocking collectives, local(): lax.all_to_all(expert_out, 'ep', split_axis=0, concat_axis=0, tiled=True)  13.9 us
    all_to_all x1, starting transfers between devices, local(): lax.all_to_all(outbound.reshape(experts, capacity, width), 'ep', split_ax...  11.9 us
    ppermute x11, waiting for transfers between devices, onward(): return lax.ppermute(value, 'tp', pairs)  11.5 us
    ppermute x11, starting transfers between devices, onward(): return lax.ppermute(value, 'tp', pairs)  11 us
    all_to_all x1, waiting for transfers between devices, local(): lax.all_to_all(outbound.reshape(experts, capacity, width), 'ep', split_ax...  10.3 us
    pallas_call x13, Pallas kernels, call(): pl.pallas_call(kernel, out_shape=outs, in_specs=[space] * len(args), out_...  8.02 us
    ppermute x1, waiting for transfers between devices, opposite(): return lax.ppermute(value, 'tp', pairs)  3.92 us
  transfers between devices with their start and end apart: 25, of which 11 were waited for; matrix products, arithmetic and copies ran while one was open for 0% of the time, Pallas kernels for 5%

profile of v4, /device:TPU:1, one launch (start us, length us, event | category | flops | bytes accessed | tf_op | source)
XLA Modules:
  0.0 94.7 jit_solution(13815571188772160335)
XLA Ops:
  0.0 1.9 %shard_map.83 = (bf16[512,256]{1,0:T(8,128)(2,1)}, f32[1,256]{1,0:T(1,128)S(1)}) custom-call(s32[4,64]{1,0:T(4,128)} %bitcast.23, bf16[64,256]{1,0:T(8,128)(2,1)} %tokens_hbm.1, f32[1,256]{1,0:T(1,128)} %bitcast.27), custom_call_target="tpu_custom_call" | custom-call | tf_op jit(solution)/shard_map/pallas_call | solution.py:245
  1.9 11.9 %all-to-all-start = ((bf16[32,16,256]{2,1,0:T(8,128)(2,1)}), bf16[32,16,256]{2,1,0:T(8,128)(2,1)S(1)}, u32[]{:S(2)}, u32[]{:S(2)}) async-start(bf16[32,16,256]{2,1,0:T(8,128)(2,1)} %bitcast.5), calls=%async_computation | async-start | bytes 524288 | tf_op jit(solution)/shard_map/all_to_all | solution.py:303
  13.7 1.0 %collective-permute-start.13 = (bf16[256,2048]{1,0:T(8,128)(2,1)}, bf16[256,2048]{1,0:T(8,128)(2,1)S(1)}, u32[]{:S(2)}, u32[]{:S(2)}) collective-permute-start(bf16[256,2048]{1,0:T(8,128)(2,1)} %bitcast.15), channel_id=1, source_target_pairs={{0,1},{1,0},{2,3},{3,2},{4,5},{5,4},{6,7},{7,6},{8,9},{9,8},{10,11... | collective-permute-start | bytes 3145736 | tf_op jit(solution)/shard_map/ppermute | solution.py:286
  14.8 10.3 %all-to-all-done = bf16[32,16,256]{2,1,0:T(8,128)(2,1)S(1)} async-done(((bf16[32,16,256]{2,1,0:T(8,128)(2,1)}), bf16[32,16,256]{2,1,0:T(8,128)(2,1)S(1)}, u32[]{:S(2)}, u32[]{:S(2)}) %all-to-all-start) | async-done | bytes 262176 | tf_op jit(solution)/shard_map/all_to_all | solution.py:303
  25.4 2.5 %collective-permute-start.3 = (bf16[528,256]{1,0:T(8,128)(2,1)S(1)}, bf16[528,256]{1,0:T(8,128)(2,1)S(1)}, u32[]{:S(2)}, u32[]{:S(2)}) collective-permute-start(bf16[528,256]{1,0:T(8,128)(2,1)S(1)} %get-tuple-element.30.refs_0_), channel_id=1, source_target_pairs={{0,1},{1,0},{2,3},{3,2},{4,5},{5,4},{6,7},{7,6},{8,9},{9,8},{10,11... | collective-permute-start | bytes 811016 | tf_op jit(solution)/shard_map/ppermute | solution.py:286
  27.9 1.2 %collective-permute-done.3.refs_1_ = bf16[528,256]{1,0:T(8,128)(2,1)S(1)} collective-permute-done((bf16[528,256]{1,0:T(8,128)(2,1)S(1)}, bf16[528,256]{1,0:T(8,128)(2,1)S(1)}, u32[]{:S(2)}, u32[]{:S(2)}) %collective-permute-start.3) | collective-permute-done | bytes 270368 | tf_op jit(solution)/shard_map/ppermute | solution.py:286
  29.1 2.7 %collective-permute-start.4 = (bf16[528,256]{1,0:T(8,128)(2,1)S(1)}, bf16[528,256]{1,0:T(8,128)(2,1)S(1)}, u32[]{:S(2)}, u32[]{:S(2)}) collective-permute-start(bf16[528,256]{1,0:T(8,128)(2,1)S(1)} %collective-permute-done.3.refs_1_), channel_id=1, source_target_pairs={{0,2},{1,7},{2,4},{3,1},{4,6},{5,3},{6,0},{7,5},{8,10},{9,15},{10,... | collective-permute-start | bytes 811016 | tf_op jit(solution)/shard_map/ppermute | solution.py:275
  32.4 4.2 %collective-permute-done.6.refs_3_ = bf16[256,256]{1,0:T(8,128)(2,1)S(1)} collective-permute-done((bf16[256,256]{1,0:T(8,128)(2,1)S(1)}, bf16[256,256]{1,0:T(8,128)(2,1)S(1)}, u32[]{:S(2)}, u32[]{:S(2)}) %collective-permute-start.6) | collective-permute-done | bytes 131104 | tf_op jit(solution)/shard_map/ppermute | solution.py:275
  36.6 1.9 %collective-permute-start.8 = (bf16[256,256]{1,0:T(8,128)(2,1)S(1)}, bf16[256,256]{1,0:T(8,128)(2,1)S(1)}, u32[]{:S(2)}, u32[]{:S(2)}) collective-permute-start(bf16[256,256]{1,0:T(8,128)(2,1)S(1)} %collective-permute-done.6.refs_3_), channel_id=1, source_target_pairs={{0,1},{1,0},{2,3},{3,2},{4,5},{5,4},{6,7},{7,6},{8,9},{9,8},{10,11... | collective-permute-start | bytes 393224 | tf_op jit(solution)/shard_map/ppermute | solution.py:286
  38.5 2.7 %collective-permute-start.1 = (bf16[272,256]{1,0:T(8,128)(2,1)S(1)}, bf16[272,256]{1,0:T(8,128)(2,1)S(1)}, u32[]{:S(2)}, u32[]{:S(2)}) collective-permute-start(bf16[272,256]{1,0:T(8,128)(2,1)S(1)} %collective-permute-done.refs_2_), channel_id=1, source_target_pairs={{0,2},{1,7},{2,4},{3,1},{4,6},{5,3},{6,0},{7,5},{8,10},{9,15},{10,... | collective-permute-start | bytes 417800 | tf_op jit(solution)/shard_map/ppermute | solution.py:275
  41.2 0.7 collective-permute-start.7
  42.0 1.3 %collective-permute-done.1.refs_0_ = bf16[272,256]{1,0:T(8,128)(2,1)S(1)} collective-permute-done((bf16[272,256]{1,0:T(8,128)(2,1)S(1)}, bf16[272,256]{1,0:T(8,128)(2,1)S(1)}, u32[]{:S(2)}, u32[]{:S(2)}) %collective-permute-start.1) | collective-permute-done | bytes 139296 | tf_op jit(solution)/shard_map/ppermute | solution.py:275
  43.2 3.0 %collective-permute-start.2 = (bf16[272,256]{1,0:T(8,128)(2,1)S(1)}, bf16[272,256]{1,0:T(8,128)(2,1)S(1)}, u32[]{:S(2)}, u32[]{:S(2)}) collective-permute-start(bf16[272,256]{1,0:T(8,128)(2,1)S(1)} %collective-permute-done.1.refs_0_), channel_id=1, source_target_pairs={{0,1},{1,0},{2,3},{3,2},{4,5},{5,4},{6,7},{7,6},{8,9},{9,8},{10,11... | collective-permute-start | bytes 417800 | tf_op jit(solution)/shard_map/ppermute | solution.py:286
  46.3 1.4 %collective-permute-start.11 = (bf16[256,256]{1,0:T(8,128)(2,1)S(1)}, bf16[256,256]{1,0:T(8,128)(2,1)S(1)}, u32[]{:S(2)}, u32[]{:S(2)}) collective-permute-start(bf16[256,256]{1,0:T(8,128)(2,1)S(1)} %collective-permute-done.10.refs_1_), channel_id=1, source_target_pairs={{0,1},{1,0},{2,3},{3,2},{4,5},{5,4},{6,7},{7,6},{8,9},{9,8},{10,11... | collective-permute-start | bytes 393224 | tf_op jit(solution)/shard_map/ppermute | solution.py:286
  47.7 1.3 %shard_map.82 = (bf16[192,512]{1,0:T(8,128)(2,1)S(1)}, f32[1,256]{1,0:T(1,128)S(1)}, bf16[2048,256]{1,0:T(8,128)(2,1)S(1)}) custom-call(s32[4,64]{1,0:T(4,128)} %bitcast.24, f32[4,64]{1,0:T(4,128)} %bitcast.25, f32[1,256]{1,0:T(1,128)} %bitcast.26, bf16[2048,256]{1,0:T(8,128)(2,1)} %bitcast.22), custom_call_target="tpu_custom_call" | custom-call | tf_op jit(solution)/shard_map/pallas_call | solution.py:245
  49.0 0.9 shard_map.85
  52.6 0.6 collective-permute-start.18
  53.2 0.6 shard_map.89
  54.9 1.8 %collective-permute-done.18 = bf16[256,256]{1,0:T(8,128)(2,1)S(1)} collective-permute-done((bf16[256,256]{1,0:T(8,128)(2,1)S(1)}, bf16[256,256]{1,0:T(8,128)(2,1)S(1)}, u32[]{:S(2)}, u32[]{:S(2)}) %collective-permute-start.18) | collective-permute-done | bytes 131104 | tf_op jit(solution)/shard_map/ppermute | solution.py:275
  56.7 1.6 %collective-permute-start.19 = (bf16[256,256]{1,0:T(8,128)(2,1)S(1)}, bf16[256,256]{1,0:T(8,128)(2,1)S(1)}, u32[]{:S(2)}, u32[]{:S(2)}) collective-permute-start(bf16[256,256]{1,0:T(8,128)(2,1)S(1)} %add_convert_fusion), channel_id=1, source_target_pairs={{0,2},{1,7},{2,4},{3,1},{4,6},{5,3},{6,0},{7,5},{8,10},{9,15},{10,... | collective-permute-start | bytes 393224 | tf_op jit(solution)/shard_map/ppermute | solution.py:275
  58.3 1.5 %collective-permute-done.14 = bf16[512,256]{1,0:T(8,128)(2,1)S(1)} collective-permute-done((bf16[512,256]{1,0:T(8,128)(2,1)S(1)}, bf16[512,256]{1,0:T(8,128)(2,1)S(1)}, u32[]{:S(2)}, u32[]{:S(2)}) %collective-permute-start.14) | collective-permute-done | bytes 262176 | tf_op jit(solution)/shard_map/ppermute | solution.py:275
  59.8 2.2 %collective-permute-start.15 = (bf16[512,256]{1,0:T(8,128)(2,1)S(1)}, bf16[512,256]{1,0:T(8,128)(2,1)S(1)}, u32[]{:S(2)}, u32[]{:S(2)}) collective-permute-start(bf16[512,256]{1,0:T(8,128)(2,1)S(1)} %collective-permute-done.14), channel_id=1, source_target_pairs={{0,1},{1,0},{2,3},{3,2},{4,5},{5,4},{6,7},{7,6},{8,9},{9,8},{10,11... | collective-permute-start | bytes 786440 | tf_op jit(solution)/shard_map/ppermute | solution.py:286
  62.1 1.1 %collective-permute-start.17 = (bf16[256,256]{1,0:T(8,128)(2,1)S(1)}, bf16[256,256]{1,0:T(8,128)(2,1)S(1)}, u32[]{:S(2)}, u32[]{:S(2)}) collective-permute-start(bf16[256,256]{1,0:T(8,128)(2,1)S(1)} %add_convert_fusion.1), channel_id=1, source_target_pairs={{0,2},{1,7},{2,4},{3,1},{4,6},{5,3},{6,0},{7,5},{8,10},{9,15},{10,... | collective-permute-start | bytes 393224 | tf_op jit(solution)/shard_map/ppermute | solution.py:275
  63.2 2.8 %collective-permute-done.17.near_a_ref = bf16[256,256]{1,0:T(8,128)(2,1)S(1)} collective-permute-done((bf16[256,256]{1,0:T(8,128)(2,1)S(1)}, bf16[256,256]{1,0:T(8,128)(2,1)S(1)}, u32[]{:S(2)}, u32[]{:S(2)}) %collective-permute-start.17) | collective-permute-done | bytes 131104 | tf_op jit(solution)/shard_map/ppermute | solution.py:275
  66.1 13.9 %all_to_all.10 = bf16[32,16,256]{2,1,0:T(8,128)(2,1)S(1)} all-to-all(bf16[32,16,256]{2,1,0:T(8,128)(2,1)S(1)} %bitcast.21), channel_id=1, replica_groups=mesh['ep'=32,'tp'=8] {'ep'}, dimensions={0} | all-to-all | bytes 524288 | tf_op jit(solution)/shard_map/all_to_all | solution.py:417
  80.4 5.1 %collective-permute-start.20 = (f32[8,128]{1,0:T(8,128)S(1)}, f32[8,128]{1,0:T(8,128)S(1)}, u32[]{:S(2)}, u32[]{:S(2)}) collective-permute-start(f32[8,128]{1,0:T(8,128)S(1)} %get-tuple-element.43), channel_id=1, source_target_pairs={{0,1},{1,0},{2,3},{3,2},{4,5},{5,4},{6,7},{7,6},{8,9},{9,8},{10,11... | collective-permute-start | bytes 12296 | tf_op jit(solution)/shard_map/ppermute | solution.py:286
  85.5 0.8 collective-permute-done.20
  86.3 0.7 collective-permute-start.21
  87.0 1.9 %collective-permute-start.22 = (f32[8,128]{1,0:T(8,128)S(1)}, f32[8,128]{1,0:T(8,128)S(1)}, u32[]{:S(2)}, u32[]{:S(2)}) collective-permute-start(f32[8,128]{1,0:T(8,128)S(1)} %add.14.squares_ref), channel_id=1, source_target_pairs={{1,5},{3,7},{5,1},{7,3},{9,13},{11,15},{13,9},{15,11},{17,21},{19,... | collective-permute-start | bytes 12296 | tf_op jit(solution)/shard_map/ppermute | solution.py:282
  88.9 3.9 %collective-permute-done.22 = f32[8,128]{1,0:T(8,128)S(1)} collective-permute-done((f32[8,128]{1,0:T(8,128)S(1)}, f32[8,128]{1,0:T(8,128)S(1)}, u32[]{:S(2)}, u32[]{:S(2)}) %collective-permute-start.22) | collective-permute-done | bytes 4128 | tf_op jit(solution)/shard_map/ppermute | solution.py:282
  92.8 1.2 %collective-permute-done.23.other_ref = f32[8,128]{1,0:T(8,128)S(1)} collective-permute-done((f32[8,128]{1,0:T(8,128)S(1)}, f32[8,128]{1,0:T(8,128)S(1)}, u32[]{:S(2)}, u32[]{:S(2)}) %collective-permute-start.23) | collective-permute-done | bytes 4128 | tf_op jit(solution)/shard_map/ppermute | solution.py:286
  94.0 0.7 shard_map.94
  (40 shorter events, 5.3 us)
Async XLA Ops:
  0.0 49.0 %copy-start = (bf16[1,2048,256]{2,1,0:T(8,128)(2,1)S(1)}, bf16[1,2048,256]{2,1,0:T(8,128)(2,1)}, u32[]{:S(2)}) copy-start(bf16[1,2048,256]{2,1,0:T(8,128)(2,1)} %param.12) | copy-start | bytes 3145732
  1.9 23.2 %all-to-all-start = ((bf16[32,16,256]{2,1,0:T(8,128)(2,1)}), bf16[32,16,256]{2,1,0:T(8,128)(2,1)S(1)}, u32[]{:S(2)}, u32[]{:S(2)}) async-start(bf16[32,16,256]{2,1,0:T(8,128)(2,1)} %bitcast.5), calls=%async_computation | async-start | bytes 524288 | tf_op jit(solution)/shard_map/all_to_all | solution.py:303
  13.7 38.4 %collective-permute-start.13 = (bf16[256,2048]{1,0:T(8,128)(2,1)}, bf16[256,2048]{1,0:T(8,128)(2,1)S(1)}, u32[]{:S(2)}, u32[]{:S(2)}) collective-permute-start(bf16[256,2048]{1,0:T(8,128)(2,1)} %bitcast.15), channel_id=1, source_target_pairs={{0,1},{1,0},{2,3},{3,2},{4,5},{5,4},{6,7},{7,6},{8,9},{9,8},{10,11... | collective-permute-start | bytes 3145736 | tf_op jit(solution)/shard_map/ppermute | solution.py:286
  25.4 3.7 %collective-permute-start.3 = (bf16[528,256]{1,0:T(8,128)(2,1)S(1)}, bf16[528,256]{1,0:T(8,128)(2,1)S(1)}, u32[]{:S(2)}, u32[]{:S(2)}) collective-permute-start(bf16[528,256]{1,0:T(8,128)(2,1)S(1)} %get-tuple-element.30.refs_0_), channel_id=1, source_target_pairs={{0,1},{1,0},{2,3},{3,2},{4,5},{5,4},{6,7},{7,6},{8,9},{9,8},{10,11... | collective-permute-start | bytes 811016 | tf_op jit(solution)/shard_map/ppermute | solution.py:286
  29.1 9.5 %collective-permute-start.4 = (bf16[528,256]{1,0:T(8,128)(2,1)S(1)}, bf16[528,256]{1,0:T(8,128)(2,1)S(1)}, u32[]{:S(2)}, u32[]{:S(2)}) collective-permute-start(bf16[528,256]{1,0:T(8,128)(2,1)S(1)} %collective-permute-done.3.refs_1_), channel_id=1, source_target_pairs={{0,2},{1,7},{2,4},{3,1},{4,6},{5,3},{6,0},{7,5},{8,10},{9,15},{10,... | collective-permute-start | bytes 811016 | tf_op jit(solution)/shard_map/ppermute | solution.py:275
  31.8 4.8 %collective-permute-start.6 = (bf16[256,256]{1,0:T(8,128)(2,1)S(1)}, bf16[256,256]{1,0:T(8,128)(2,1)S(1)}, u32[]{:S(2)}, u32[]{:S(2)}) collective-permute-start(bf16[256,256]{1,0:T(8,128)(2,1)S(1)} %get-tuple-element.31), channel_id=1, source_target_pairs={{0,2},{1,7},{2,4},{3,1},{4,6},{5,3},{6,0},{7,5},{8,10},{9,15},{10,... | collective-permute-start | bytes 393224 | tf_op jit(solution)/shard_map/ppermute | solution.py:275
  32.3 6.3 %collective-permute-start = (bf16[272,256]{1,0:T(8,128)(2,1)S(1)}, bf16[272,256]{1,0:T(8,128)(2,1)S(1)}, u32[]{:S(2)}, u32[]{:S(2)}) collective-permute-start(bf16[272,256]{1,0:T(8,128)(2,1)S(1)} %get-tuple-element.28), channel_id=1, source_target_pairs={{0,2},{1,7},{2,4},{3,1},{4,6},{5,3},{6,0},{7,5},{8,10},{9,15},{10,... | collective-permute-start | bytes 417800 | tf_op jit(solution)/shard_map/ppermute | solution.py:275
  36.6 4.6 %collective-permute-start.8 = (bf16[256,256]{1,0:T(8,128)(2,1)S(1)}, bf16[256,256]{1,0:T(8,128)(2,1)S(1)}, u32[]{:S(2)}, u32[]{:S(2)}) collective-permute-start(bf16[256,256]{1,0:T(8,128)(2,1)S(1)} %collective-permute-done.6.refs_3_), channel_id=1, source_target_pairs={{0,1},{1,0},{2,3},{3,2},{4,5},{5,4},{6,7},{7,6},{8,9},{9,8},{10,11... | collective-permute-start | bytes 393224 | tf_op jit(solution)/shard_map/ppermute | solution.py:286
  38.5 11.4 %collective-permute-start.5 = (bf16[528,256]{1,0:T(8,128)(2,1)S(1)}, bf16[528,256]{1,0:T(8,128)(2,1)S(1)}, u32[]{:S(2)}, u32[]{:S(2)}) collective-permute-start(bf16[528,256]{1,0:T(8,128)(2,1)S(1)} %collective-permute-done.4.refs_0_), channel_id=1, source_target_pairs={{0,1},{1,0},{2,3},{3,2},{4,5},{5,4},{6,7},{7,6},{8,9},{9,8},{10,11... | collective-permute-start | bytes 811016 | tf_op jit(solution)/shard_map/ppermute | solution.py:286
  38.5 4.7 %collective-permute-start.1 = (bf16[272,256]{1,0:T(8,128)(2,1)S(1)}, bf16[272,256]{1,0:T(8,128)(2,1)S(1)}, u32[]{:S(2)}, u32[]{:S(2)}) collective-permute-start(bf16[272,256]{1,0:T(8,128)(2,1)S(1)} %collective-permute-done.refs_2_), channel_id=1, source_target_pairs={{0,2},{1,7},{2,4},{3,1},{4,6},{5,3},{6,0},{7,5},{8,10},{9,15},{10,... | collective-permute-start | bytes 417800 | tf_op jit(solution)/shard_map/ppermute | solution.py:275
  41.2 5.1 %collective-permute-start.10 = (bf16[256,256]{1,0:T(8,128)(2,1)S(1)}, bf16[256,256]{1,0:T(8,128)(2,1)S(1)}, u32[]{:S(2)}, u32[]{:S(2)}) collective-permute-start(bf16[256,256]{1,0:T(8,128)(2,1)S(1)} %collective-permute-done.6.refs_3_), channel_id=1, source_target_pairs={{0,2},{1,7},{2,4},{3,1},{4,6},{5,3},{6,0},{7,5},{8,10},{9,15},{10,... | collective-permute-start | bytes 393224 | tf_op jit(solution)/shard_map/ppermute | solution.py:275
  41.2 7.8 %collective-permute-start.7 = (bf16[272,256]{1,0:T(8,128)(2,1)S(1)}, bf16[272,256]{1,0:T(8,128)(2,1)S(1)}, u32[]{:S(2)}, u32[]{:S(2)}) collective-permute-start(bf16[272,256]{1,0:T(8,128)(2,1)S(1)} %collective-permute-done.refs_2_), channel_id=1, source_target_pairs={{0,1},{1,0},{2,3},{3,2},{4,5},{5,4},{6,7},{7,6},{8,9},{9,8},{10,11... | collective-permute-start | bytes 417800 | tf_op jit(solution)/shard_map/ppermute | solution.py:286
  43.2 7.2 %collective-permute-start.2 = (bf16[272,256]{1,0:T(8,128)(2,1)S(1)}, bf16[272,256]{1,0:T(8,128)(2,1)S(1)}, u32[]{:S(2)}, u32[]{:S(2)}) collective-permute-start(bf16[272,256]{1,0:T(8,128)(2,1)S(1)} %collective-permute-done.1.refs_0_), channel_id=1, source_target_pairs={{0,1},{1,0},{2,3},{3,2},{4,5},{5,4},{6,7},{7,6},{8,9},{9,8},{10,11... | collective-permute-start | bytes 417800 | tf_op jit(solution)/shard_map/ppermute | solution.py:286
  46.3 4.2 %collective-permute-start.11 = (bf16[256,256]{1,0:T(8,128)(2,1)S(1)}, bf16[256,256]{1,0:T(8,128)(2,1)S(1)}, u32[]{:S(2)}, u32[]{:S(2)}) collective-permute-start(bf16[256,256]{1,0:T(8,128)(2,1)S(1)} %collective-permute-done.10.refs_1_), channel_id=1, source_target_pairs={{0,1},{1,0},{2,3},{3,2},{4,5},{5,4},{6,7},{7,6},{8,9},{9,8},{10,11... | collective-permute-start | bytes 393224 | tf_op jit(solution)/shard_map/ppermute | solution.py:286
  50.9 1.4 %copy-start.1 = (bf16[1,256,2048]{2,1,0:T(8,128)(2,1)S(1)}, bf16[1,256,2048]{2,1,0:T(8,128)(2,1)}, u32[]{:S(2)}) copy-start(bf16[1,256,2048]{2,1,0:T(8,128)(2,1)} %param.14) | copy-start | bytes 3145732
  50.9 1.4 %collective-permute-start.12 = (bf16[256,256]{1,0:T(8,128)(2,1)S(1)}, bf16[256,256]{1,0:T(8,128)(2,1)S(1)}, u32[]{:S(2)}, u32[]{:S(2)}) collective-permute-start(bf16[256,256]{1,0:T(8,128)(2,1)S(1)} %shard_map.88.refs_2_.own_ref), channel_id=1, source_target_pairs={{0,1},{1,0},{2,3},{3,2},{4,5},{5,4},{6,7},{7,6},{8,9},{9,8},{10,11... | collective-permute-start | bytes 393224 | tf_op jit(solution)/shard_map/ppermute | solution.py:286
  51.5 1.7 %collective-permute-start.9 = (bf16[256,256]{1,0:T(8,128)(2,1)S(1)}, bf16[256,256]{1,0:T(8,128)(2,1)S(1)}, u32[]{:S(2)}, u32[]{:S(2)}) collective-permute-start(bf16[256,256]{1,0:T(8,128)(2,1)S(1)} %shard_map.87.refs_0_.own_ref), channel_id=1, source_target_pairs={{0,1},{1,0},{2,3},{3,2},{4,5},{5,4},{6,7},{7,6},{8,9},{9,8},{10,11... | collective-permute-start | bytes 393224 | tf_op jit(solution)/shard_map/ppermute | solution.py:286
  52.6 4.1 %collective-permute-start.18 = (bf16[256,256]{1,0:T(8,128)(2,1)S(1)}, bf16[256,256]{1,0:T(8,128)(2,1)S(1)}, u32[]{:S(2)}, u32[]{:S(2)}) collective-permute-start(bf16[256,256]{1,0:T(8,128)(2,1)S(1)} %shard_map.91), channel_id=1, source_target_pairs={{0,2},{1,7},{2,4},{3,1},{4,6},{5,3},{6,0},{7,5},{8,10},{9,15},{10,... | collective-permute-start | bytes 393224 | tf_op jit(solution)/shard_map/ppermute | solution.py:275
  53.8 6.0 %collective-permute-start.14 = (bf16[512,256]{1,0:T(8,128)(2,1)S(1)}, bf16[512,256]{1,0:T(8,128)(2,1)S(1)}, u32[]{:S(2)}, u32[]{:S(2)}) collective-permute-start(bf16[512,256]{1,0:T(8,128)(2,1)S(1)} %get-tuple-element.39), channel_id=1, source_target_pairs={{0,2},{1,7},{2,4},{3,1},{4,6},{5,3},{6,0},{7,5},{8,10},{9,15},{10,... | collective-permute-start | bytes 786440 | tf_op jit(solution)/shard_map/ppermute | solution.py:275
  54.6 7.5 %collective-permute-start.16 = (bf16[256,256]{1,0:T(8,128)(2,1)S(1)}, bf16[256,256]{1,0:T(8,128)(2,1)S(1)}, u32[]{:S(2)}, u32[]{:S(2)}) collective-permute-start(bf16[256,256]{1,0:T(8,128)(2,1)S(1)} %shard_map.90), channel_id=1, source_target_pairs={{0,2},{1,7},{2,4},{3,1},{4,6},{5,3},{6,0},{7,5},{8,10},{9,15},{10,... | collective-permute-start | bytes 393224 | tf_op jit(solution)/shard_map/ppermute | solution.py:275
  56.7 6.4 %collective-permute-start.19 = (bf16[256,256]{1,0:T(8,128)(2,1)S(1)}, bf16[256,256]{1,0:T(8,128)(2,1)S(1)}, u32[]{:S(2)}, u32[]{:S(2)}) collective-permute-start(bf16[256,256]{1,0:T(8,128)(2,1)S(1)} %add_convert_fusion), channel_id=1, source_target_pairs={{0,2},{1,7},{2,4},{3,1},{4,6},{5,3},{6,0},{7,5},{8,10},{9,15},{10,... | collective-permute-start | bytes 393224 | tf_op jit(solution)/shard_map/ppermute | solution.py:275
  59.8 6.2 %collective-permute-start.15 = (bf16[512,256]{1,0:T(8,128)(2,1)S(1)}, bf16[512,256]{1,0:T(8,128)(2,1)S(1)}, u32[]{:S(2)}, u32[]{:S(2)}) collective-permute-start(bf16[512,256]{1,0:T(8,128)(2,1)S(1)} %collective-permute-done.14), channel_id=1, source_target_pairs={{0,1},{1,0},{2,3},{3,2},{4,5},{5,4},{6,7},{7,6},{8,9},{9,8},{10,11... | collective-permute-start | bytes 786440 | tf_op jit(solution)/shard_map/ppermute | solution.py:286
  62.1 3.9 %collective-permute-start.17 = (bf16[256,256]{1,0:T(8,128)(2,1)S(1)}, bf16[256,256]{1,0:T(8,128)(2,1)S(1)}, u32[]{:S(2)}, u32[]{:S(2)}) collective-permute-start(bf16[256,256]{1,0:T(8,128)(2,1)S(1)} %add_convert_fusion.1), channel_id=1, source_target_pairs={{0,2},{1,7},{2,4},{3,1},{4,6},{5,3},{6,0},{7,5},{8,10},{9,15},{10,... | collective-permute-start | bytes 393224 | tf_op jit(solution)/shard_map/ppermute | solution.py:275
  80.4 5.9 %collective-permute-start.20 = (f32[8,128]{1,0:T(8,128)S(1)}, f32[8,128]{1,0:T(8,128)S(1)}, u32[]{:S(2)}, u32[]{:S(2)}) collective-permute-start(f32[8,128]{1,0:T(8,128)S(1)} %get-tuple-element.43), channel_id=1, source_target_pairs={{0,1},{1,0},{2,3},{3,2},{4,5},{5,4},{6,7},{7,6},{8,9},{9,8},{10,11... | collective-permute-start | bytes 12296 | tf_op jit(solution)/shard_map/ppermute | solution.py:286
  86.3 2.6 %collective-permute-start.21 = (f32[8,128]{1,0:T(8,128)S(1)}, f32[8,128]{1,0:T(8,128)S(1)}, u32[]{:S(2)}, u32[]{:S(2)}) collective-permute-start(f32[8,128]{1,0:T(8,128)S(1)} %add.14.squares_ref), channel_id=1, source_target_pairs={{0,2},{1,7},{2,4},{3,1},{4,6},{5,3},{6,0},{7,5},{8,10},{9,15},{10,... | collective-permute-start | bytes 12296 | tf_op jit(solution)/shard_map/ppermute | solution.py:275
  87.0 5.8 %collective-permute-start.22 = (f32[8,128]{1,0:T(8,128)S(1)}, f32[8,128]{1,0:T(8,128)S(1)}, u32[]{:S(2)}, u32[]{:S(2)}) collective-permute-start(f32[8,128]{1,0:T(8,128)S(1)} %add.14.squares_ref), channel_id=1, source_target_pairs={{1,5},{3,7},{5,1},{7,3},{9,13},{11,15},{13,9},{15,11},{17,21},{19,... | collective-permute-start | bytes 12296 | tf_op jit(solution)/shard_map/ppermute | solution.py:282
  92.8 1.2 %collective-permute-start.23 = (f32[8,128]{1,0:T(8,128)S(1)}, f32[8,128]{1,0:T(8,128)S(1)}, u32[]{:S(2)}, u32[]{:S(2)}) collective-permute-start(f32[8,128]{1,0:T(8,128)S(1)} %add.15.around_ref), channel_id=1, source_target_pairs={{0,1},{1,0},{2,3},{3,2},{4,5},{5,4},{6,7},{7,6},{8,9},{9,8},{10,11... | collective-permute-start | bytes 12296 | tf_op jit(solution)/shard_map/ppermute | solution.py:286

commit v5 on v4

--- a/solution.py
+++ b/solution.py
@@ -226,8 +226,9 @@
     squares_ref[...] = sums
 
 
-def final_kernel(model_width, mix_ref, squares_ref, around_ref, other_ref, gain_ref, out_ref):
-    total = squares_ref[0:1, :] + around_ref[0:1, :] + other_ref[0:1, :]
+def final_kernel(model_width, mix_ref, *refs):
+    *squares, gain_ref, out_ref = refs
+    total = functools.reduce(jnp.add, [part[0:1, :] for part in squares])
     mix = mix_ref[...]
     tokens = mix.shape[0]
     wide = jnp.broadcast_to(total, (tokens, total.shape[1]))
@@ -275,9 +276,10 @@
         return lax.ppermute(value, "tp", pairs)
 
     def opposite(value):
-        last = CORES - 1
         pairs = [
-            (y * CORES + last, ((y + chips // 2) % chips) * CORES + last) for y in range(chips)
+            (y * CORES + c, ((y + chips // 2) % chips) * CORES + c)
+            for y in range(chips)
+            for c in range(CORES)
         ]
         return lax.ppermute(value, "tp", pairs)
 
@@ -422,8 +424,8 @@
         returned.reshape(rows, width),
     )
     squares += swap(squares)
+    around = onward(squares)
     across = opposite(squares)
-    around = onward(squares) + across
     return call(
         functools.partial(final_kernel, model_width),
         shape_of((tok_rows, width), jnp.bfloat16),
@@ -431,6 +433,7 @@
         squares,
         around,
         swap(around),
+        across,
         final_gain,
     )
 

time: 95 us -> 93.2 us (0.981)
  waiting for transfers between devices: 29.1 us -> 26.6 us
    ppermute x1, waiting for transfers between devices: 3.92 us -> 0.01 us  [opposite(): return lax.ppermute(value, 'tp', pairs)]
    ppermute x12, starting transfers between devices: 18.6 us -> 21.3 us  [swap(): return lax.ppermute(value, 'tp', pairs)]
    ppermute x1, starting transfers between devices: 1.91 us -> 0.01 us  [opposite(): return lax.ppermute(value, 'tp', pairs)]
    ppermute x11, waiting for transfers between devices: 11.5 us -> 13.2 us  [onward(): return lax.ppermute(value, 'tp', pairs)]
where the time goes in v5:
time: 93.2 us; the launch traced here: 93 us
  starting transfers between devices  44.1 us (47%)
  waiting for transfers between devices  26.6 us (29%)
  blocking collectives  13.9 us (15%)
  Pallas kernels  8.02 us (9%)
    ppermute x12, starting transfers between devices, swap(): return lax.ppermute(value, 'tp', pairs)  21.3 us
    all_to_all x1, blocking collectives, local(): lax.all_to_all(expert_out, 'ep', split_axis=0, concat_axis=0, tiled=True)  13.9 us
    ppermute x11, waiting for transfers between devices, onward(): return lax.ppermute(value, 'tp', pairs)  13.2 us
    all_to_all x1, starting transfers between devices, local(): lax.all_to_all(outbound.reshape(experts, capacity, width), 'ep', split_ax...  11.9 us
    ppermute x11, starting transfers between devices, onward(): return lax.ppermute(value, 'tp', pairs)  11 us
    all_to_all x1, waiting for transfers between devices, local(): lax.all_to_all(outbound.reshape(experts, capacity, width), 'ep', split_ax...  10.3 us
    pallas_call x13, Pallas kernels, call(): pl.pallas_call(kernel, out_shape=outs, in_specs=[space] * len(args), out_...  8.02 us
    ppermute x12, waiting for transfers between devices, swap(): return lax.ppermute(value, 'tp', pairs)  3.12 us
  transfers between devices with their start and end apart: 25, of which 11 were waited for; matrix products, arithmetic and copies ran while one was open for 0% of the time, Pallas kernels for 5%

profile of v5, /device:TPU:1, one launch (start us, length us, event | category | flops | bytes accessed | tf_op | source)
XLA Modules:
  0.0 93.0 jit_solution(10845041790589380294)
XLA Ops:
  0.0 1.9 %shard_map.83 = (bf16[512,256]{1,0:T(8,128)(2,1)}, f32[1,256]{1,0:T(1,128)S(1)}) custom-call(s32[4,64]{1,0:T(4,128)} %bitcast.23, bf16[64,256]{1,0:T(8,128)(2,1)} %tokens_hbm.1, f32[1,256]{1,0:T(1,128)} %bitcast.27), custom_call_target="tpu_custom_call" | custom-call | tf_op jit(solution)/shard_map/pallas_call | solution.py:246
  1.9 11.9 %all-to-all-start = ((bf16[32,16,256]{2,1,0:T(8,128)(2,1)}), bf16[32,16,256]{2,1,0:T(8,128)(2,1)S(1)}, u32[]{:S(2)}, u32[]{:S(2)}) async-start(bf16[32,16,256]{2,1,0:T(8,128)(2,1)} %bitcast.5), calls=%async_computation | async-start | bytes 524288 | tf_op jit(solution)/shard_map/all_to_all | solution.py:305
  13.7 1.0 %collective-permute-start.13 = (bf16[256,2048]{1,0:T(8,128)(2,1)}, bf16[256,2048]{1,0:T(8,128)(2,1)S(1)}, u32[]{:S(2)}, u32[]{:S(2)}) collective-permute-start(bf16[256,2048]{1,0:T(8,128)(2,1)} %bitcast.15), channel_id=1, source_target_pairs={{0,1},{1,0},{2,3},{3,2},{4,5},{5,4},{6,7},{7,6},{8,9},{9,8},{10,11... | collective-permute-start | bytes 3145736 | tf_op jit(solution)/shard_map/ppermute | solution.py:288
  14.8 10.3 %all-to-all-done = bf16[32,16,256]{2,1,0:T(8,128)(2,1)S(1)} async-done(((bf16[32,16,256]{2,1,0:T(8,128)(2,1)}), bf16[32,16,256]{2,1,0:T(8,128)(2,1)S(1)}, u32[]{:S(2)}, u32[]{:S(2)}) %all-to-all-start) | async-done | bytes 262176 | tf_op jit(solution)/shard_map/all_to_all | solution.py:305
  25.4 2.5 %collective-permute-start.3 = (bf16[528,256]{1,0:T(8,128)(2,1)S(1)}, bf16[528,256]{1,0:T(8,128)(2,1)S(1)}, u32[]{:S(2)}, u32[]{:S(2)}) collective-permute-start(bf16[528,256]{1,0:T(8,128)(2,1)S(1)} %get-tuple-element.30.refs_0_), channel_id=1, source_target_pairs={{0,1},{1,0},{2,3},{3,2},{4,5},{5,4},{6,7},{7,6},{8,9},{9,8},{10,11... | collective-permute-start | bytes 811016 | tf_op jit(solution)/shard_map/ppermute | solution.py:288
  27.9 1.2 %collective-permute-done.3.refs_1_ = bf16[528,256]{1,0:T(8,128)(2,1)S(1)} collective-permute-done((bf16[528,256]{1,0:T(8,128)(2,1)S(1)}, bf16[528,256]{1,0:T(8,128)(2,1)S(1)}, u32[]{:S(2)}, u32[]{:S(2)}) %collective-permute-start.3) | collective-permute-done | bytes 270368 | tf_op jit(solution)/shard_map/ppermute | solution.py:288
  29.1 2.7 %collective-permute-start.4 = (bf16[528,256]{1,0:T(8,128)(2,1)S(1)}, bf16[528,256]{1,0:T(8,128)(2,1)S(1)}, u32[]{:S(2)}, u32[]{:S(2)}) collective-permute-start(bf16[528,256]{1,0:T(8,128)(2,1)S(1)} %collective-permute-done.3.refs_1_), channel_id=1, source_target_pairs={{0,2},{1,7},{2,4},{3,1},{4,6},{5,3},{6,0},{7,5},{8,10},{9,15},{10,... | collective-permute-start | bytes 811016 | tf_op jit(solution)/shard_map/ppermute | solution.py:276
  32.4 4.2 %collective-permute-done.6.refs_3_ = bf16[256,256]{1,0:T(8,128)(2,1)S(1)} collective-permute-done((bf16[256,256]{1,0:T(8,128)(2,1)S(1)}, bf16[256,256]{1,0:T(8,128)(2,1)S(1)}, u32[]{:S(2)}, u32[]{:S(2)}) %collective-permute-start.6) | collective-permute-done | bytes 131104 | tf_op jit(solution)/shard_map/ppermute | solution.py:276
  36.6 1.9 %collective-permute-start.8 = (bf16[256,256]{1,0:T(8,128)(2,1)S(1)}, bf16[256,256]{1,0:T(8,128)(2,1)S(1)}, u32[]{:S(2)}, u32[]{:S(2)}) collective-permute-start(bf16[256,256]{1,0:T(8,128)(2,1)S(1)} %collective-permute-done.6.refs_3_), channel_id=1, source_target_pairs={{0,1},{1,0},{2,3},{3,2},{4,5},{5,4},{6,7},{7,6},{8,9},{9,8},{10,11... | collective-permute-start | bytes 393224 | tf_op jit(solution)/shard_map/ppermute | solution.py:288
  38.5 2.7 %collective-permute-start.1 = (bf16[272,256]{1,0:T(8,128)(2,1)S(1)}, bf16[272,256]{1,0:T(8,128)(2,1)S(1)}, u32[]{:S(2)}, u32[]{:S(2)}) collective-permute-start(bf16[272,256]{1,0:T(8,128)(2,1)S(1)} %collective-permute-done.refs_2_), channel_id=1, source_target_pairs={{0,2},{1,7},{2,4},{3,1},{4,6},{5,3},{6,0},{7,5},{8,10},{9,15},{10,... | collective-permute-start | bytes 417800 | tf_op jit(solution)/shard_map/ppermute | solution.py:276
  41.2 0.7 collective-permute-start.7
  42.0 1.3 %collective-permute-done.1.refs_0_ = bf16[272,256]{1,0:T(8,128)(2,1)S(1)} collective-permute-done((bf16[272,256]{1,0:T(8,128)(2,1)S(1)}, bf16[272,256]{1,0:T(8,128)(2,1)S(1)}, u32[]{:S(2)}, u32[]{:S(2)}) %collective-permute-start.1) | collective-permute-done | bytes 139296 | tf_op jit(solution)/shard_map/ppermute | solution.py:276
  43.2 3.0 %collective-permute-start.2 = (bf16[272,256]{1,0:T(8,128)(2,1)S(1)}, bf16[272,256]{1,0:T(8,128)(2,1)S(1)}, u32[]{:S(2)}, u32[]{:S(2)}) collective-permute-start(bf16[272,256]{1,0:T(8,128)(2,1)S(1)} %collective-permute-done.1.refs_0_), channel_id=1, source_target_pairs={{0,1},{1,0},{2,3},{3,2},{4,5},{5,4},{6,7},{7,6},{8,9},{9,8},{10,11... | collective-permute-start | bytes 417800 | tf_op jit(solution)/shard_map/ppermute | solution.py:288
  46.3 1.4 %collective-permute-start.11 = (bf16[256,256]{1,0:T(8,128)(2,1)S(1)}, bf16[256,256]{1,0:T(8,128)(2,1)S(1)}, u32[]{:S(2)}, u32[]{:S(2)}) collective-permute-start(bf16[256,256]{1,0:T(8,128)(2,1)S(1)} %collective-permute-done.10.refs_1_), channel_id=1, source_target_pairs={{0,1},{1,0},{2,3},{3,2},{4,5},{5,4},{6,7},{7,6},{8,9},{9,8},{10,11... | collective-permute-start | bytes 393224 | tf_op jit(solution)/shard_map/ppermute | solution.py:288
  47.7 1.3 %shard_map.82 = (bf16[192,512]{1,0:T(8,128)(2,1)S(1)}, f32[1,256]{1,0:T(1,128)S(1)}, bf16[2048,256]{1,0:T(8,128)(2,1)S(1)}) custom-call(s32[4,64]{1,0:T(4,128)} %bitcast.24, f32[4,64]{1,0:T(4,128)} %bitcast.25, f32[1,256]{1,0:T(1,128)} %bitcast.26, bf16[2048,256]{1,0:T(8,128)(2,1)} %bitcast.22), custom_call_target="tpu_custom_call" | custom-call | tf_op jit(solution)/shard_map/pallas_call | solution.py:246
  49.0 0.9 shard_map.85
  52.6 0.6 collective-permute-start.18
  53.2 0.6 shard_map.89
  54.9 1.8 %collective-permute-done.18 = bf16[256,256]{1,0:T(8,128)(2,1)S(1)} collective-permute-done((bf16[256,256]{1,0:T(8,128)(2,1)S(1)}, bf16[256,256]{1,0:T(8,128)(2,1)S(1)}, u32[]{:S(2)}, u32[]{:S(2)}) %collective-permute-start.18) | collective-permute-done | bytes 131104 | tf_op jit(solution)/shard_map/ppermute | solution.py:276
  56.7 1.6 %collective-permute-start.19 = (bf16[256,256]{1,0:T(8,128)(2,1)S(1)}, bf16[256,256]{1,0:T(8,128)(2,1)S(1)}, u32[]{:S(2)}, u32[]{:S(2)}) collective-permute-start(bf16[256,256]{1,0:T(8,128)(2,1)S(1)} %add_convert_fusion), channel_id=1, source_target_pairs={{0,2},{1,7},{2,4},{3,1},{4,6},{5,3},{6,0},{7,5},{8,10},{9,15},{10,... | collective-permute-start | bytes 393224 | tf_op jit(solution)/shard_map/ppermute | solution.py:276
  58.3 1.5 %collective-permute-done.14 = bf16[512,256]{1,0:T(8,128)(2,1)S(1)} collective-permute-done((bf16[512,256]{1,0:T(8,128)(2,1)S(1)}, bf16[512,256]{1,0:T(8,128)(2,1)S(1)}, u32[]{:S(2)}, u32[]{:S(2)}) %collective-permute-start.14) | collective-permute-done | bytes 262176 | tf_op jit(solution)/shard_map/ppermute | solution.py:276
  59.8 2.2 %collective-permute-start.15 = (bf16[512,256]{1,0:T(8,128)(2,1)S(1)}, bf16[512,256]{1,0:T(8,128)(2,1)S(1)}, u32[]{:S(2)}, u32[]{:S(2)}) collective-permute-start(bf16[512,256]{1,0:T(8,128)(2,1)S(1)} %collective-permute-done.14), channel_id=1, source_target_pairs={{0,1},{1,0},{2,3},{3,2},{4,5},{5,4},{6,7},{7,6},{8,9},{9,8},{10,11... | collective-permute-start | bytes 786440 | tf_op jit(solution)/shard_map/ppermute | solution.py:288
  62.1 1.1 %collective-permute-start.17 = (bf16[256,256]{1,0:T(8,128)(2,1)S(1)}, bf16[256,256]{1,0:T(8,128)(2,1)S(1)}, u32[]{:S(2)}, u32[]{:S(2)}) collective-permute-start(bf16[256,256]{1,0:T(8,128)(2,1)S(1)} %add_convert_fusion.1), channel_id=1, source_target_pairs={{0,2},{1,7},{2,4},{3,1},{4,6},{5,3},{6,0},{7,5},{8,10},{9,15},{10,... | collective-permute-start | bytes 393224 | tf_op jit(solution)/shard_map/ppermute | solution.py:276
  63.2 2.8 %collective-permute-done.17.near_a_ref = bf16[256,256]{1,0:T(8,128)(2,1)S(1)} collective-permute-done((bf16[256,256]{1,0:T(8,128)(2,1)S(1)}, bf16[256,256]{1,0:T(8,128)(2,1)S(1)}, u32[]{:S(2)}, u32[]{:S(2)}) %collective-permute-start.17) | collective-permute-done | bytes 131104 | tf_op jit(solution)/shard_map/ppermute | solution.py:276
  66.1 13.9 %all_to_all.10 = bf16[32,16,256]{2,1,0:T(8,128)(2,1)S(1)} all-to-all(bf16[32,16,256]{2,1,0:T(8,128)(2,1)S(1)} %bitcast.21), channel_id=1, replica_groups=mesh['ep'=32,'tp'=8] {'ep'}, dimensions={0} | all-to-all | bytes 524288 | tf_op jit(solution)/shard_map/all_to_all | solution.py:419
  80.4 5.1 %collective-permute-start.20 = (f32[8,128]{1,0:T(8,128)S(1)}, f32[8,128]{1,0:T(8,128)S(1)}, u32[]{:S(2)}, u32[]{:S(2)}) collective-permute-start(f32[8,128]{1,0:T(8,128)S(1)} %get-tuple-element.43), channel_id=1, source_target_pairs={{0,1},{1,0},{2,3},{3,2},{4,5},{5,4},{6,7},{7,6},{8,9},{9,8},{10,11... | collective-permute-start | bytes 12296 | tf_op jit(solution)/shard_map/ppermute | solution.py:288
  85.5 0.8 collective-permute-done.20
  86.3 0.7 collective-permute-start.21
  87.0 1.8 %collective-permute-done.21.refs_1_ = f32[8,128]{1,0:T(8,128)S(1)} collective-permute-done((f32[8,128]{1,0:T(8,128)S(1)}, f32[8,128]{1,0:T(8,128)S(1)}, u32[]{:S(2)}, u32[]{:S(2)}) %collective-permute-start.21) | collective-permute-done | bytes 4128 | tf_op jit(solution)/shard_map/ppermute | solution.py:276
  88.7 2.7 %collective-permute-start.22 = (f32[8,128]{1,0:T(8,128)S(1)}, f32[8,128]{1,0:T(8,128)S(1)}, u32[]{:S(2)}, u32[]{:S(2)}) collective-permute-start(f32[8,128]{1,0:T(8,128)S(1)} %collective-permute-done.21.refs_1_), channel_id=1, source_target_pairs={{0,1},{1,0},{2,3},{3,2},{4,5},{5,4},{6,7},{7,6},{8,9},{9,8},{10,11... | collective-permute-start | bytes 12296 | tf_op jit(solution)/shard_map/ppermute | solution.py:288
  91.5 0.8 collective-permute-done.22.refs_2_
  92.3 0.7 shard_map.94
  (39 shorter events, 5.3 us)
Async XLA Ops:
  0.0 49.0 %copy-start = (bf16[1,2048,256]{2,1,0:T(8,128)(2,1)S(1)}, bf16[1,2048,256]{2,1,0:T(8,128)(2,1)}, u32[]{:S(2)}) copy-start(bf16[1,2048,256]{2,1,0:T(8,128)(2,1)} %param.12) | copy-start | bytes 3145732
  1.9 23.2 %all-to-all-start = ((bf16[32,16,256]{2,1,0:T(8,128)(2,1)}), bf16[32,16,256]{2,1,0:T(8,128)(2,1)S(1)}, u32[]{:S(2)}, u32[]{:S(2)}) async-start(bf16[32,16,256]{2,1,0:T(8,128)(2,1)} %bitcast.5), calls=%async_computation | async-start | bytes 524288 | tf_op jit(solution)/shard_map/all_to_all | solution.py:305
  13.7 38.4 %collective-permute-start.13 = (bf16[256,2048]{1,0:T(8,128)(2,1)}, bf16[256,2048]{1,0:T(8,128)(2,1)S(1)}, u32[]{:S(2)}, u32[]{:S(2)}) collective-permute-start(bf16[256,2048]{1,0:T(8,128)(2,1)} %bitcast.15), channel_id=1, source_target_pairs={{0,1},{1,0},{2,3},{3,2},{4,5},{5,4},{6,7},{7,6},{8,9},{9,8},{10,11... | collective-permute-start | bytes 3145736 | tf_op jit(solution)/shard_map/ppermute | solution.py:288
  25.4 3.7 %collective-permute-start.3 = (bf16[528,256]{1,0:T(8,128)(2,1)S(1)}, bf16[528,256]{1,0:T(8,128)(2,1)S(1)}, u32[]{:S(2)}, u32[]{:S(2)}) collective-permute-start(bf16[528,256]{1,0:T(8,128)(2,1)S(1)} %get-tuple-element.30.refs_0_), channel_id=1, source_target_pairs={{0,1},{1,0},{2,3},{3,2},{4,5},{5,4},{6,7},{7,6},{8,9},{9,8},{10,11... | collective-permute-start | bytes 811016 | tf_op jit(solution)/shard_map/ppermute | solution.py:288
  29.1 9.5 %collective-permute-start.4 = (bf16[528,256]{1,0:T(8,128)(2,1)S(1)}, bf16[528,256]{1,0:T(8,128)(2,1)S(1)}, u32[]{:S(2)}, u32[]{:S(2)}) collective-permute-start(bf16[528,256]{1,0:T(8,128)(2,1)S(1)} %collective-permute-done.3.refs_1_), channel_id=1, source_target_pairs={{0,2},{1,7},{2,4},{3,1},{4,6},{5,3},{6,0},{7,5},{8,10},{9,15},{10,... | collective-permute-start | bytes 811016 | tf_op jit(solution)/shard_map/ppermute | solution.py:276
  31.8 4.8 %collective-permute-start.6 = (bf16[256,256]{1,0:T(8,128)(2,1)S(1)}, bf16[256,256]{1,0:T(8,128)(2,1)S(1)}, u32[]{:S(2)}, u32[]{:S(2)}) collective-permute-start(bf16[256,256]{1,0:T(8,128)(2,1)S(1)} %get-tuple-element.31), channel_id=1, source_target_pairs={{0,2},{1,7},{2,4},{3,1},{4,6},{5,3},{6,0},{7,5},{8,10},{9,15},{10,... | collective-permute-start | bytes 393224 | tf_op jit(solution)/shard_map/ppermute | solution.py:276
  32.3 6.3 %collective-permute-start = (bf16[272,256]{1,0:T(8,128)(2,1)S(1)}, bf16[272,256]{1,0:T(8,128)(2,1)S(1)}, u32[]{:S(2)}, u32[]{:S(2)}) collective-permute-start(bf16[272,256]{1,0:T(8,128)(2,1)S(1)} %get-tuple-element.28), channel_id=1, source_target_pairs={{0,2},{1,7},{2,4},{3,1},{4,6},{5,3},{6,0},{7,5},{8,10},{9,15},{10,... | collective-permute-start | bytes 417800 | tf_op jit(solution)/shard_map/ppermute | solution.py:276
  36.6 4.6 %collective-permute-start.8 = (bf16[256,256]{1,0:T(8,128)(2,1)S(1)}, bf16[256,256]{1,0:T(8,128)(2,1)S(1)}, u32[]{:S(2)}, u32[]{:S(2)}) collective-permute-start(bf16[256,256]{1,0:T(8,128)(2,1)S(1)} %collective-permute-done.6.refs_3_), channel_id=1, source_target_pairs={{0,1},{1,0},{2,3},{3,2},{4,5},{5,4},{6,7},{7,6},{8,9},{9,8},{10,11... | collective-permute-start | bytes 393224 | tf_op jit(solution)/shard_map/ppermute | solution.py:288
  38.5 11.4 %collective-permute-start.5 = (bf16[528,256]{1,0:T(8,128)(2,1)S(1)}, bf16[528,256]{1,0:T(8,128)(2,1)S(1)}, u32[]{:S(2)}, u32[]{:S(2)}) collective-permute-start(bf16[528,256]{1,0:T(8,128)(2,1)S(1)} %collective-permute-done.4.refs_0_), channel_id=1, source_target_pairs={{0,1},{1,0},{2,3},{3,2},{4,5},{5,4},{6,7},{7,6},{8,9},{9,8},{10,11... | collective-permute-start | bytes 811016 | tf_op jit(solution)/shard_map/ppermute | solution.py:288
  38.5 4.7 %collective-permute-start.1 = (bf16[272,256]{1,0:T(8,128)(2,1)S(1)}, bf16[272,256]{1,0:T(8,128)(2,1)S(1)}, u32[]{:S(2)}, u32[]{:S(2)}) collective-permute-start(bf16[272,256]{1,0:T(8,128)(2,1)S(1)} %collective-permute-done.refs_2_), channel_id=1, source_target_pairs={{0,2},{1,7},{2,4},{3,1},{4,6},{5,3},{6,0},{7,5},{8,10},{9,15},{10,... | collective-permute-start | bytes 417800 | tf_op jit(solution)/shard_map/ppermute | solution.py:276
  41.2 5.1 %collective-permute-start.10 = (bf16[256,256]{1,0:T(8,128)(2,1)S(1)}, bf16[256,256]{1,0:T(8,128)(2,1)S(1)}, u32[]{:S(2)}, u32[]{:S(2)}) collective-permute-start(bf16[256,256]{1,0:T(8,128)(2,1)S(1)} %collective-permute-done.6.refs_3_), channel_id=1, source_target_pairs={{0,2},{1,7},{2,4},{3,1},{4,6},{5,3},{6,0},{7,5},{8,10},{9,15},{10,... | collective-permute-start | bytes 393224 | tf_op jit(solution)/shard_map/ppermute | solution.py:276
  41.2 7.8 %collective-permute-start.7 = (bf16[272,256]{1,0:T(8,128)(2,1)S(1)}, bf16[272,256]{1,0:T(8,128)(2,1)S(1)}, u32[]{:S(2)}, u32[]{:S(2)}) collective-permute-start(bf16[272,256]{1,0:T(8,128)(2,1)S(1)} %collective-permute-done.refs_2_), channel_id=1, source_target_pairs={{0,1},{1,0},{2,3},{3,2},{4,5},{5,4},{6,7},{7,6},{8,9},{9,8},{10,11... | collective-permute-start | bytes 417800 | tf_op jit(solution)/shard_map/ppermute | solution.py:288
  43.2 7.2 %collective-permute-start.2 = (bf16[272,256]{1,0:T(8,128)(2,1)S(1)}, bf16[272,256]{1,0:T(8,128)(2,1)S(1)}, u32[]{:S(2)}, u32[]{:S(2)}) collective-permute-start(bf16[272,256]{1,0:T(8,128)(2,1)S(1)} %collective-permute-done.1.refs_0_), channel_id=1, source_target_pairs={{0,1},{1,0},{2,3},{3,2},{4,5},{5,4},{6,7},{7,6},{8,9},{9,8},{10,11... | collective-permute-start | bytes 417800 | tf_op jit(solution)/shard_map/ppermute | solution.py:288
  46.3 4.2 %collective-permute-start.11 = (bf16[256,256]{1,0:T(8,128)(2,1)S(1)}, bf16[256,256]{1,0:T(8,128)(2,1)S(1)}, u32[]{:S(2)}, u32[]{:S(2)}) collective-permute-start(bf16[256,256]{1,0:T(8,128)(2,1)S(1)} %collective-permute-done.10.refs_1_), channel_id=1, source_target_pairs={{0,1},{1,0},{2,3},{3,2},{4,5},{5,4},{6,7},{7,6},{8,9},{9,8},{10,11... | collective-permute-start | bytes 393224 | tf_op jit(solution)/shard_map/ppermute | solution.py:288
  50.9 1.4 %copy-start.1 = (bf16[1,256,2048]{2,1,0:T(8,128)(2,1)S(1)}, bf16[1,256,2048]{2,1,0:T(8,128)(2,1)}, u32[]{:S(2)}) copy-start(bf16[1,256,2048]{2,1,0:T(8,128)(2,1)} %param.14) | copy-start | bytes 3145732
  50.9 1.4 %collective-permute-start.12 = (bf16[256,256]{1,0:T(8,128)(2,1)S(1)}, bf16[256,256]{1,0:T(8,128)(2,1)S(1)}, u32[]{:S(2)}, u32[]{:S(2)}) collective-permute-start(bf16[256,256]{1,0:T(8,128)(2,1)S(1)} %shard_map.88.refs_2_.own_ref), channel_id=1, source_target_pairs={{0,1},{1,0},{2,3},{3,2},{4,5},{5,4},{6,7},{7,6},{8,9},{9,8},{10,11... | collective-permute-start | bytes 393224 | tf_op jit(solution)/shard_map/ppermute | solution.py:288
  51.5 1.7 %collective-permute-start.9 = (bf16[256,256]{1,0:T(8,128)(2,1)S(1)}, bf16[256,256]{1,0:T(8,128)(2,1)S(1)}, u32[]{:S(2)}, u32[]{:S(2)}) collective-permute-start(bf16[256,256]{1,0:T(8,128)(2,1)S(1)} %shard_map.87.refs_0_.own_ref), channel_id=1, source_target_pairs={{0,1},{1,0},{2,3},{3,2},{4,5},{5,4},{6,7},{7,6},{8,9},{9,8},{10,11... | collective-permute-start | bytes 393224 | tf_op jit(solution)/shard_map/ppermute | solution.py:288
  52.6 4.1 %collective-permute-start.18 = (bf16[256,256]{1,0:T(8,128)(2,1)S(1)}, bf16[256,256]{1,0:T(8,128)(2,1)S(1)}, u32[]{:S(2)}, u32[]{:S(2)}) collective-permute-start(bf16[256,256]{1,0:T(8,128)(2,1)S(1)} %shard_map.91), channel_id=1, source_target_pairs={{0,2},{1,7},{2,4},{3,1},{4,6},{5,3},{6,0},{7,5},{8,10},{9,15},{10,... | collective-permute-start | bytes 393224 | tf_op jit(solution)/shard_map/ppermute | solution.py:276
  53.8 6.0 %collective-permute-start.14 = (bf16[512,256]{1,0:T(8,128)(2,1)S(1)}, bf16[512,256]{1,0:T(8,128)(2,1)S(1)}, u32[]{:S(2)}, u32[]{:S(2)}) collective-permute-start(bf16[512,256]{1,0:T(8,128)(2,1)S(1)} %get-tuple-element.39), channel_id=1, source_target_pairs={{0,2},{1,7},{2,4},{3,1},{4,6},{5,3},{6,0},{7,5},{8,10},{9,15},{10,... | collective-permute-start | bytes 786440 | tf_op jit(solution)/shard_map/ppermute | solution.py:276
  54.6 7.5 %collective-permute-start.16 = (bf16[256,256]{1,0:T(8,128)(2,1)S(1)}, bf16[256,256]{1,0:T(8,128)(2,1)S(1)}, u32[]{:S(2)}, u32[]{:S(2)}) collective-permute-start(bf16[256,256]{1,0:T(8,128)(2,1)S(1)} %shard_map.90), channel_id=1, source_target_pairs={{0,2},{1,7},{2,4},{3,1},{4,6},{5,3},{6,0},{7,5},{8,10},{9,15},{10,... | collective-permute-start | bytes 393224 | tf_op jit(solution)/shard_map/ppermute | solution.py:276
  56.7 6.4 %collective-permute-start.19 = (bf16[256,256]{1,0:T(8,128)(2,1)S(1)}, bf16[256,256]{1,0:T(8,128)(2,1)S(1)}, u32[]{:S(2)}, u32[]{:S(2)}) collective-permute-start(bf16[256,256]{1,0:T(8,128)(2,1)S(1)} %add_convert_fusion), channel_id=1, source_target_pairs={{0,2},{1,7},{2,4},{3,1},{4,6},{5,3},{6,0},{7,5},{8,10},{9,15},{10,... | collective-permute-start | bytes 393224 | tf_op jit(solution)/shard_map/ppermute | solution.py:276
  59.8 6.2 %collective-permute-start.15 = (bf16[512,256]{1,0:T(8,128)(2,1)S(1)}, bf16[512,256]{1,0:T(8,128)(2,1)S(1)}, u32[]{:S(2)}, u32[]{:S(2)}) collective-permute-start(bf16[512,256]{1,0:T(8,128)(2,1)S(1)} %collective-permute-done.14), channel_id=1, source_target_pairs={{0,1},{1,0},{2,3},{3,2},{4,5},{5,4},{6,7},{7,6},{8,9},{9,8},{10,11... | collective-permute-start | bytes 786440 | tf_op jit(solution)/shard_map/ppermute | solution.py:288
  62.1 3.9 %collective-permute-start.17 = (bf16[256,256]{1,0:T(8,128)(2,1)S(1)}, bf16[256,256]{1,0:T(8,128)(2,1)S(1)}, u32[]{:S(2)}, u32[]{:S(2)}) collective-permute-start(bf16[256,256]{1,0:T(8,128)(2,1)S(1)} %add_convert_fusion.1), channel_id=1, source_target_pairs={{0,2},{1,7},{2,4},{3,1},{4,6},{5,3},{6,0},{7,5},{8,10},{9,15},{10,... | collective-permute-start | bytes 393224 | tf_op jit(solution)/shard_map/ppermute | solution.py:276
  80.4 5.9 %collective-permute-start.20 = (f32[8,128]{1,0:T(8,128)S(1)}, f32[8,128]{1,0:T(8,128)S(1)}, u32[]{:S(2)}, u32[]{:S(2)}) collective-permute-start(f32[8,128]{1,0:T(8,128)S(1)} %get-tuple-element.43), channel_id=1, source_target_pairs={{0,1},{1,0},{2,3},{3,2},{4,5},{5,4},{6,7},{7,6},{8,9},{9,8},{10,11... | collective-permute-start | bytes 12296 | tf_op jit(solution)/shard_map/ppermute | solution.py:288
  86.3 2.5 %collective-permute-start.21 = (f32[8,128]{1,0:T(8,128)S(1)}, f32[8,128]{1,0:T(8,128)S(1)}, u32[]{:S(2)}, u32[]{:S(2)}) collective-permute-start(f32[8,128]{1,0:T(8,128)S(1)} %add.11.refs_0_), channel_id=1, source_target_pairs={{0,2},{1,7},{2,4},{3,1},{4,6},{5,3},{6,0},{7,5},{8,10},{9,15},{10,... | collective-permute-start | bytes 12296 | tf_op jit(solution)/shard_map/ppermute | solution.py:276
  87.0 4.5 %collective-permute-start.23 = (f32[8,128]{1,0:T(8,128)S(1)}, f32[8,128]{1,0:T(8,128)S(1)}, u32[]{:S(2)}, u32[]{:S(2)}) collective-permute-start(f32[8,128]{1,0:T(8,128)S(1)} %add.11.refs_0_), channel_id=1, source_target_pairs={{0,4},{1,5},{2,6},{3,7},{4,0},{5,1},{6,2},{7,3},{8,12},{9,13},{10,... | collective-permute-start | bytes 12296 | tf_op jit(solution)/shard_map/ppermute | solution.py:284
  88.7 3.5 %collective-permute-start.22 = (f32[8,128]{1,0:T(8,128)S(1)}, f32[8,128]{1,0:T(8,128)S(1)}, u32[]{:S(2)}, u32[]{:S(2)}) collective-permute-start(f32[8,128]{1,0:T(8,128)S(1)} %collective-permute-done.21.refs_1_), channel_id=1, source_target_pairs={{0,1},{1,0},{2,3},{3,2},{4,5},{5,4},{6,7},{7,6},{8,9},{9,8},{10,11... | collective-permute-start | bytes 12296 | tf_op jit(solution)/shard_map/ppermute | solution.py:288

commit v6 on v5

--- a/solution.py
+++ b/solution.py
@@ -89,7 +89,7 @@
     )
     share = jnp.where(holds, spread(share), 0.0).T
     tokens = share.shape[0]
-    for i, part in enumerate(split3(share)):
+    for i, part in enumerate(split3(share)[:2]):
         share_ref[i * tokens : (i + 1) * tokens, :] = part
     for copy in copies[2:]:
         copy.wait()
@@ -218,10 +218,10 @@
 def combine_kernel(share_ref, rows_ref, mix_ref, squares_ref):
     tokens = mix_ref.shape[0]
     parts = jnp.dot(share_ref[...], rows_ref[...], preferred_element_type=jnp.float32)
-    mix = parts[:tokens] + parts[tokens : 2 * tokens] + parts[2 * tokens :]
+    mix = parts[:tokens] + parts[tokens:]
     mix_ref[...] = mix
     ones = jnp.ones((8, mix.shape[1]), jnp.bfloat16)
-    sums = functools.reduce(jnp.add, [dot_t(ones, part) for part in split3(mix * mix)])
+    sums = functools.reduce(jnp.add, [dot_t(ones, part) for part in split3(mix * mix)[:2]])
     sums = jnp.concatenate([sums, jnp.zeros_like(sums)], axis=1)
     squares_ref[...] = sums
 
@@ -324,7 +324,7 @@
     sources = (ids, route_weights.T, final_gain[None, :], up_proj[0])
     share, final_gain, up = call(
         functools.partial(load_kernel, experts, capacity),
-        [shape_of((3 * tok_rows, rows), jnp.bfloat16)]
+        [shape_of((2 * tok_rows, rows), jnp.bfloat16)]
         + [shape_of(source.shape, source.dtype) for source in sources[2:]],
         *sources,
         space=HBM,
@@ -424,7 +424,17 @@
         returned.reshape(rows, width),
     )
     squares += swap(squares)
-    around = onward(squares)
+
+    def beside(value, step):
+        pairs = [
+            (y * CORES + c, ((y + step) % chips) * CORES + c)
+            for y in range(chips)
+            for c in range(CORES)
+        ]
+        return lax.ppermute(value, "tp", pairs)
+
+    around = beside(squares, 1)
+    other_way = beside(squares, chips - 1)
     across = opposite(squares)
     return call(
         functools.partial(final_kernel, model_width),
@@ -432,7 +442,7 @@
         mixture,
         squares,
         around,
-        swap(around),
+        other_way,
         across,
         final_gain,
     )

time: 93.2 us -> 93.8 us (level)
  waiting for transfers between devices: 26.6 us -> 28 us
    ppermute x1, waiting for transfers between devices: 0.01 us -> 2.97 us  [opposite(): return lax.ppermute(value, 'tp', pairs)]
    ppermute x12 -> x11, starting transfers between devices: 21.3 us -> 18.6 us  [swap(): return lax.ppermute(value, 'tp', pairs)]
    ppermute x0 -> x2, starting transfers between devices: none -> 2.68 us  [beside(): return lax.ppermute(value, 'tp', pairs)]
    ppermute x11 -> x10, waiting for transfers between devices: 13.2 us -> 11.5 us  [onward(): return lax.ppermute(value, 'tp', pairs)]
    ppermute x0 -> x2, waiting for transfers between devices: none -> 0.99 us  [beside(): return lax.ppermute(value, 'tp', pairs)]
    ppermute x12 -> x11, waiting for transfers between devices: 3.12 us -> 2.3 us  [swap(): return lax.ppermute(value, 'tp', pairs)]
    ppermute x11 -> x10, starting transfers between devices: 11 us -> 10.3 us  [onward(): return lax.ppermute(value, 'tp', pairs)]
where the time goes in v6:
time: 93.8 us; the launch traced here: 93.6 us
  starting transfers between devices  43.4 us (46%)
  waiting for transfers between devices  28 us (30%)
  blocking collectives  13.9 us (15%)
  Pallas kernels  7.97 us (8%)
    ppermute x11, starting transfers between devices, swap(): return lax.ppermute(value, 'tp', pairs)  18.6 us
    all_to_all x1, blocking collectives, local(): lax.all_to_all(expert_out, 'ep', split_axis=0, concat_axis=0, tiled=True)  13.9 us
    all_to_all x1, starting transfers between devices, local(): lax.all_to_all(outbound.reshape(experts, capacity, width), 'ep', split_ax...  11.9 us
    ppermute x10, waiting for transfers between devices, onward(): return lax.ppermute(value, 'tp', pairs)  11.5 us
    all_to_all x1, waiting for transfers between devices, local(): lax.all_to_all(outbound.reshape(experts, capacity, width), 'ep', split_ax...  10.3 us
    ppermute x10, starting transfers between devices, onward(): return lax.ppermute(value, 'tp', pairs)  10.3 us
    pallas_call x13, Pallas kernels, call(): pl.pallas_call(kernel, out_shape=outs, in_specs=[space] * len(args), out_...  7.97 us
    ppermute x1, waiting for transfers between devices, opposite(): return lax.ppermute(value, 'tp', pairs)  2.97 us
  transfers between devices with their start and end apart: 25, of which 11 were waited for; matrix products, arithmetic and copies ran while one was open for 0% of the time, Pallas kernels for 5%

profile of v6, /device:TPU:1, one launch (start us, length us, event | category | flops | bytes accessed | tf_op | source)
XLA Modules:
  0.0 93.6 jit_solution(2222657858175427372)
XLA Ops:
  0.0 1.9 %shard_map.83 = (bf16[512,256]{1,0:T(8,128)(2,1)}, f32[1,256]{1,0:T(1,128)S(1)}) custom-call(s32[4,64]{1,0:T(4,128)} %bitcast.23, bf16[64,256]{1,0:T(8,128)(2,1)} %tokens_hbm.1, f32[1,256]{1,0:T(1,128)} %bitcast.27), custom_call_target="tpu_custom_call" | custom-call | tf_op jit(solution)/shard_map/pallas_call | solution.py:246
  1.9 11.9 %all-to-all-start = ((bf16[32,16,256]{2,1,0:T(8,128)(2,1)}), bf16[32,16,256]{2,1,0:T(8,128)(2,1)S(1)}, u32[]{:S(2)}, u32[]{:S(2)}) async-start(bf16[32,16,256]{2,1,0:T(8,128)(2,1)} %bitcast.5), calls=%async_computation | async-start | bytes 524288 | tf_op jit(solution)/shard_map/all_to_all | solution.py:305
  13.7 1.0 %collective-permute-start.13 = (bf16[256,2048]{1,0:T(8,128)(2,1)}, bf16[256,2048]{1,0:T(8,128)(2,1)S(1)}, u32[]{:S(2)}, u32[]{:S(2)}) collective-permute-start(bf16[256,2048]{1,0:T(8,128)(2,1)} %bitcast.15), channel_id=1, source_target_pairs={{0,1},{1,0},{2,3},{3,2},{4,5},{5,4},{6,7},{7,6},{8,9},{9,8},{10,11... | collective-permute-start | bytes 3145736 | tf_op jit(solution)/shard_map/ppermute | solution.py:288
  14.8 10.3 %all-to-all-done = bf16[32,16,256]{2,1,0:T(8,128)(2,1)S(1)} async-done(((bf16[32,16,256]{2,1,0:T(8,128)(2,1)}), bf16[32,16,256]{2,1,0:T(8,128)(2,1)S(1)}, u32[]{:S(2)}, u32[]{:S(2)}) %all-to-all-start) | async-done | bytes 262176 | tf_op jit(solution)/shard_map/all_to_all | solution.py:305
  25.4 2.5 %collective-permute-start.3 = (bf16[528,256]{1,0:T(8,128)(2,1)S(1)}, bf16[528,256]{1,0:T(8,128)(2,1)S(1)}, u32[]{:S(2)}, u32[]{:S(2)}) collective-permute-start(bf16[528,256]{1,0:T(8,128)(2,1)S(1)} %get-tuple-element.30.refs_0_), channel_id=1, source_target_pairs={{0,1},{1,0},{2,3},{3,2},{4,5},{5,4},{6,7},{7,6},{8,9},{9,8},{10,11... | collective-permute-start | bytes 811016 | tf_op jit(solution)/shard_map/ppermute | solution.py:288
  27.9 1.2 %collective-permute-done.3.refs_1_ = bf16[528,256]{1,0:T(8,128)(2,1)S(1)} collective-permute-done((bf16[528,256]{1,0:T(8,128)(2,1)S(1)}, bf16[528,256]{1,0:T(8,128)(2,1)S(1)}, u32[]{:S(2)}, u32[]{:S(2)}) %collective-permute-start.3) | collective-permute-done | bytes 270368 | tf_op jit(solution)/shard_map/ppermute | solution.py:288
  29.1 2.7 %collective-permute-start.4 = (bf16[528,256]{1,0:T(8,128)(2,1)S(1)}, bf16[528,256]{1,0:T(8,128)(2,1)S(1)}, u32[]{:S(2)}, u32[]{:S(2)}) collective-permute-start(bf16[528,256]{1,0:T(8,128)(2,1)S(1)} %collective-permute-done.3.refs_1_), channel_id=1, source_target_pairs={{0,2},{1,7},{2,4},{3,1},{4,6},{5,3},{6,0},{7,5},{8,10},{9,15},{10,... | collective-permute-start | bytes 811016 | tf_op jit(solution)/shard_map/ppermute | solution.py:276
  32.4 4.2 %collective-permute-done.6.refs_3_ = bf16[256,256]{1,0:T(8,128)(2,1)S(1)} collective-permute-done((bf16[256,256]{1,0:T(8,128)(2,1)S(1)}, bf16[256,256]{1,0:T(8,128)(2,1)S(1)}, u32[]{:S(2)}, u32[]{:S(2)}) %collective-permute-start.6) | collective-permute-done | bytes 131104 | tf_op jit(solution)/shard_map/ppermute | solution.py:276
  36.6 1.9 %collective-permute-start.8 = (bf16[256,256]{1,0:T(8,128)(2,1)S(1)}, bf16[256,256]{1,0:T(8,128)(2,1)S(1)}, u32[]{:S(2)}, u32[]{:S(2)}) collective-permute-start(bf16[256,256]{1,0:T(8,128)(2,1)S(1)} %collective-permute-done.6.refs_3_), channel_id=1, source_target_pairs={{0,1},{1,0},{2,3},{3,2},{4,5},{5,4},{6,7},{7,6},{8,9},{9,8},{10,11... | collective-permute-start | bytes 393224 | tf_op jit(solution)/shard_map/ppermute | solution.py:288
  38.5 2.7 %collective-permute-start.1 = (bf16[272,256]{1,0:T(8,128)(2,1)S(1)}, bf16[272,256]{1,0:T(8,128)(2,1)S(1)}, u32[]{:S(2)}, u32[]{:S(2)}) collective-permute-start(bf16[272,256]{1,0:T(8,128)(2,1)S(1)} %collective-permute-done.refs_2_), channel_id=1, source_target_pairs={{0,2},{1,7},{2,4},{3,1},{4,6},{5,3},{6,0},{7,5},{8,10},{9,15},{10,... | collective-permute-start | bytes 417800 | tf_op jit(solution)/shard_map/ppermute | solution.py:276
  41.2 0.7 collective-permute-start.7
  42.0 1.3 %collective-permute-done.1.refs_0_ = bf16[272,256]{1,0:T(8,128)(2,1)S(1)} collective-permute-done((bf16[272,256]{1,0:T(8,128)(2,1)S(1)}, bf16[272,256]{1,0:T(8,128)(2,1)S(1)}, u32[]{:S(2)}, u32[]{:S(2)}) %collective-permute-start.1) | collective-permute-done | bytes 139296 | tf_op jit(solution)/shard_map/ppermute | solution.py:276
  43.2 3.0 %collective-permute-start.2 = (bf16[272,256]{1,0:T(8,128)(2,1)S(1)}, bf16[272,256]{1,0:T(8,128)(2,1)S(1)}, u32[]{:S(2)}, u32[]{:S(2)}) collective-permute-start(bf16[272,256]{1,0:T(8,128)(2,1)S(1)} %collective-permute-done.1.refs_0_), channel_id=1, source_target_pairs={{0,1},{1,0},{2,3},{3,2},{4,5},{5,4},{6,7},{7,6},{8,9},{9,8},{10,11... | collective-permute-start | bytes 417800 | tf_op jit(solution)/shard_map/ppermute | solution.py:288
  46.3 1.4 %collective-permute-start.11 = (bf16[256,256]{1,0:T(8,128)(2,1)S(1)}, bf16[256,256]{1,0:T(8,128)(2,1)S(1)}, u32[]{:S(2)}, u32[]{:S(2)}) collective-permute-start(bf16[256,256]{1,0:T(8,128)(2,1)S(1)} %collective-permute-done.10.refs_1_), channel_id=1, source_target_pairs={{0,1},{1,0},{2,3},{3,2},{4,5},{5,4},{6,7},{7,6},{8,9},{9,8},{10,11... | collective-permute-start | bytes 393224 | tf_op jit(solution)/shard_map/ppermute | solution.py:288
  47.7 1.3 %shard_map.82 = (bf16[128,512]{1,0:T(8,128)(2,1)S(1)}, f32[1,256]{1,0:T(1,128)S(1)}, bf16[2048,256]{1,0:T(8,128)(2,1)S(1)}) custom-call(s32[4,64]{1,0:T(4,128)} %bitcast.24, f32[4,64]{1,0:T(4,128)} %bitcast.25, f32[1,256]{1,0:T(1,128)} %bitcast.26, bf16[2048,256]{1,0:T(8,128)(2,1)} %bitcast.22), custom_call_target="tpu_custom_call" | custom-call | tf_op jit(solution)/shard_map/pallas_call | solution.py:246
  49.0 0.9 shard_map.85
  51.5 0.6 collective-permute-start.9
  52.6 0.6 collective-permute-start.18
  53.2 0.6 shard_map.89
  54.9 1.8 %collective-permute-done.18 = bf16[256,256]{1,0:T(8,128)(2,1)S(1)} collective-permute-done((bf16[256,256]{1,0:T(8,128)(2,1)S(1)}, bf16[256,256]{1,0:T(8,128)(2,1)S(1)}, u32[]{:S(2)}, u32[]{:S(2)}) %collective-permute-start.18) | collective-permute-done | bytes 131104 | tf_op jit(solution)/shard_map/ppermute | solution.py:276
  56.7 1.6 %collective-permute-start.19 = (bf16[256,256]{1,0:T(8,128)(2,1)S(1)}, bf16[256,256]{1,0:T(8,128)(2,1)S(1)}, u32[]{:S(2)}, u32[]{:S(2)}) collective-permute-start(bf16[256,256]{1,0:T(8,128)(2,1)S(1)} %add_convert_fusion), channel_id=1, source_target_pairs={{0,2},{1,7},{2,4},{3,1},{4,6},{5,3},{6,0},{7,5},{8,10},{9,15},{10,... | collective-permute-start | bytes 393224 | tf_op jit(solution)/shard_map/ppermute | solution.py:276
  58.3 1.4 %collective-permute-done.14 = bf16[512,256]{1,0:T(8,128)(2,1)S(1)} collective-permute-done((bf16[512,256]{1,0:T(8,128)(2,1)S(1)}, bf16[512,256]{1,0:T(8,128)(2,1)S(1)}, u32[]{:S(2)}, u32[]{:S(2)}) %collective-permute-start.14) | collective-permute-done | bytes 262176 | tf_op jit(solution)/shard_map/ppermute | solution.py:276
  59.8 2.2 %collective-permute-start.15 = (bf16[512,256]{1,0:T(8,128)(2,1)S(1)}, bf16[512,256]{1,0:T(8,128)(2,1)S(1)}, u32[]{:S(2)}, u32[]{:S(2)}) collective-permute-start(bf16[512,256]{1,0:T(8,128)(2,1)S(1)} %collective-permute-done.14), channel_id=1, source_target_pairs={{0,1},{1,0},{2,3},{3,2},{4,5},{5,4},{6,7},{7,6},{8,9},{9,8},{10,11... | collective-permute-start | bytes 786440 | tf_op jit(solution)/shard_map/ppermute | solution.py:288
  62.1 1.1 %collective-permute-start.17 = (bf16[256,256]{1,0:T(8,128)(2,1)S(1)}, bf16[256,256]{1,0:T(8,128)(2,1)S(1)}, u32[]{:S(2)}, u32[]{:S(2)}) collective-permute-start(bf16[256,256]{1,0:T(8,128)(2,1)S(1)} %add_convert_fusion.1), channel_id=1, source_target_pairs={{0,2},{1,7},{2,4},{3,1},{4,6},{5,3},{6,0},{7,5},{8,10},{9,15},{10,... | collective-permute-start | bytes 393224 | tf_op jit(solution)/shard_map/ppermute | solution.py:276
  63.2 2.8 %collective-permute-done.17.near_a_ref = bf16[256,256]{1,0:T(8,128)(2,1)S(1)} collective-permute-done((bf16[256,256]{1,0:T(8,128)(2,1)S(1)}, bf16[256,256]{1,0:T(8,128)(2,1)S(1)}, u32[]{:S(2)}, u32[]{:S(2)}) %collective-permute-start.17) | collective-permute-done | bytes 131104 | tf_op jit(solution)/shard_map/ppermute | solution.py:276
  66.1 13.9 %all_to_all.10 = bf16[32,16,256]{2,1,0:T(8,128)(2,1)S(1)} all-to-all(bf16[32,16,256]{2,1,0:T(8,128)(2,1)S(1)} %bitcast.21), channel_id=1, replica_groups=mesh['ep'=32,'tp'=8] {'ep'}, dimensions={0} | all-to-all | bytes 524288 | tf_op jit(solution)/shard_map/all_to_all | solution.py:419
  80.3 5.1 %collective-permute-start.20 = (f32[8,128]{1,0:T(8,128)S(1)}, f32[8,128]{1,0:T(8,128)S(1)}, u32[]{:S(2)}, u32[]{:S(2)}) collective-permute-start(f32[8,128]{1,0:T(8,128)S(1)} %get-tuple-element.43), channel_id=1, source_target_pairs={{0,1},{1,0},{2,3},{3,2},{4,5},{5,4},{6,7},{7,6},{8,9},{9,8},{10,11... | collective-permute-start | bytes 12296 | tf_op jit(solution)/shard_map/ppermute | solution.py:288
  85.4 0.8 collective-permute-done.20
  86.2 2.7 %collective-permute-start.22 = (f32[8,128]{1,0:T(8,128)S(1)}, f32[8,128]{1,0:T(8,128)S(1)}, u32[]{:S(2)}, u32[]{:S(2)}) collective-permute-start(f32[8,128]{1,0:T(8,128)S(1)} %add.11.refs_0_), channel_id=1, source_target_pairs={{0,6},{1,7},{2,0},{3,1},{4,2},{5,3},{6,4},{7,5},{8,14},{9,15},{10,... | collective-permute-start | bytes 12296 | tf_op jit(solution)/shard_map/ppermute | solution.py:434
  88.9 1.0 %collective-permute-done.21.refs_1_ = f32[8,128]{1,0:T(8,128)S(1)} collective-permute-done((f32[8,128]{1,0:T(8,128)S(1)}, f32[8,128]{1,0:T(8,128)S(1)}, u32[]{:S(2)}, u32[]{:S(2)}) %collective-permute-start.21) | collective-permute-done | bytes 4128 | tf_op jit(solution)/shard_map/ppermute | solution.py:434
  89.9 3.0 %collective-permute-done.23.refs_3_ = f32[8,128]{1,0:T(8,128)S(1)} collective-permute-done((f32[8,128]{1,0:T(8,128)S(1)}, f32[8,128]{1,0:T(8,128)S(1)}, u32[]{:S(2)}, u32[]{:S(2)}) %collective-permute-start.23) | collective-permute-done | bytes 4128 | tf_op jit(solution)/shard_map/ppermute | solution.py:284
  92.9 0.7 shard_map.94
  (39 shorter events, 4.7 us)
Async XLA Ops:
  0.0 49.0 %copy-start = (bf16[1,2048,256]{2,1,0:T(8,128)(2,1)S(1)}, bf16[1,2048,256]{2,1,0:T(8,128)(2,1)}, u32[]{:S(2)}) copy-start(bf16[1,2048,256]{2,1,0:T(8,128)(2,1)} %param.12) | copy-start | bytes 3145732
  1.9 23.2 %all-to-all-start = ((bf16[32,16,256]{2,1,0:T(8,128)(2,1)}), bf16[32,16,256]{2,1,0:T(8,128)(2,1)S(1)}, u32[]{:S(2)}, u32[]{:S(2)}) async-start(bf16[32,16,256]{2,1,0:T(8,128)(2,1)} %bitcast.5), calls=%async_computation | async-start | bytes 524288 | tf_op jit(solution)/shard_map/all_to_all | solution.py:305
  13.7 38.4 %collective-permute-start.13 = (bf16[256,2048]{1,0:T(8,128)(2,1)}, bf16[256,2048]{1,0:T(8,128)(2,1)S(1)}, u32[]{:S(2)}, u32[]{:S(2)}) collective-permute-start(bf16[256,2048]{1,0:T(8,128)(2,1)} %bitcast.15), channel_id=1, source_target_pairs={{0,1},{1,0},{2,3},{3,2},{4,5},{5,4},{6,7},{7,6},{8,9},{9,8},{10,11... | collective-permute-start | bytes 3145736 | tf_op jit(solution)/shard_map/ppermute | solution.py:288
  25.4 3.7 %collective-permute-start.3 = (bf16[528,256]{1,0:T(8,128)(2,1)S(1)}, bf16[528,256]{1,0:T(8,128)(2,1)S(1)}, u32[]{:S(2)}, u32[]{:S(2)}) collective-permute-start(bf16[528,256]{1,0:T(8,128)(2,1)S(1)} %get-tuple-element.30.refs_0_), channel_id=1, source_target_pairs={{0,1},{1,0},{2,3},{3,2},{4,5},{5,4},{6,7},{7,6},{8,9},{9,8},{10,11... | collective-permute-start | bytes 811016 | tf_op jit(solution)/shard_map/ppermute | solution.py:288
  29.1 9.5 %collective-permute-start.4 = (bf16[528,256]{1,0:T(8,128)(2,1)S(1)}, bf16[528,256]{1,0:T(8,128)(2,1)S(1)}, u32[]{:S(2)}, u32[]{:S(2)}) collective-permute-start(bf16[528,256]{1,0:T(8,128)(2,1)S(1)} %collective-permute-done.3.refs_1_), channel_id=1, source_target_pairs={{0,2},{1,7},{2,4},{3,1},{4,6},{5,3},{6,0},{7,5},{8,10},{9,15},{10,... | collective-permute-start | bytes 811016 | tf_op jit(solution)/shard_map/ppermute | solution.py:276
  31.8 4.8 %collective-permute-start.6 = (bf16[256,256]{1,0:T(8,128)(2,1)S(1)}, bf16[256,256]{1,0:T(8,128)(2,1)S(1)}, u32[]{:S(2)}, u32[]{:S(2)}) collective-permute-start(bf16[256,256]{1,0:T(8,128)(2,1)S(1)} %get-tuple-element.31), channel_id=1, source_target_pairs={{0,2},{1,7},{2,4},{3,1},{4,6},{5,3},{6,0},{7,5},{8,10},{9,15},{10,... | collective-permute-start | bytes 393224 | tf_op jit(solution)/shard_map/ppermute | solution.py:276
  32.3 6.3 %collective-permute-start = (bf16[272,256]{1,0:T(8,128)(2,1)S(1)}, bf16[272,256]{1,0:T(8,128)(2,1)S(1)}, u32[]{:S(2)}, u32[]{:S(2)}) collective-permute-start(bf16[272,256]{1,0:T(8,128)(2,1)S(1)} %get-tuple-element.28), channel_id=1, source_target_pairs={{0,2},{1,7},{2,4},{3,1},{4,6},{5,3},{6,0},{7,5},{8,10},{9,15},{10,... | collective-permute-start | bytes 417800 | tf_op jit(solution)/shard_map/ppermute | solution.py:276
  36.6 4.6 %collective-permute-start.8 = (bf16[256,256]{1,0:T(8,128)(2,1)S(1)}, bf16[256,256]{1,0:T(8,128)(2,1)S(1)}, u32[]{:S(2)}, u32[]{:S(2)}) collective-permute-start(bf16[256,256]{1,0:T(8,128)(2,1)S(1)} %collective-permute-done.6.refs_3_), channel_id=1, source_target_pairs={{0,1},{1,0},{2,3},{3,2},{4,5},{5,4},{6,7},{7,6},{8,9},{9,8},{10,11... | collective-permute-start | bytes 393224 | tf_op jit(solution)/shard_map/ppermute | solution.py:288
  38.5 11.4 %collective-permute-start.5 = (bf16[528,256]{1,0:T(8,128)(2,1)S(1)}, bf16[528,256]{1,0:T(8,128)(2,1)S(1)}, u32[]{:S(2)}, u32[]{:S(2)}) collective-permute-start(bf16[528,256]{1,0:T(8,128)(2,1)S(1)} %collective-permute-done.4.refs_0_), channel_id=1, source_target_pairs={{0,1},{1,0},{2,3},{3,2},{4,5},{5,4},{6,7},{7,6},{8,9},{9,8},{10,11... | collective-permute-start | bytes 811016 | tf_op jit(solution)/shard_map/ppermute | solution.py:288
  38.5 4.7 %collective-permute-start.1 = (bf16[272,256]{1,0:T(8,128)(2,1)S(1)}, bf16[272,256]{1,0:T(8,128)(2,1)S(1)}, u32[]{:S(2)}, u32[]{:S(2)}) collective-permute-start(bf16[272,256]{1,0:T(8,128)(2,1)S(1)} %collective-permute-done.refs_2_), channel_id=1, source_target_pairs={{0,2},{1,7},{2,4},{3,1},{4,6},{5,3},{6,0},{7,5},{8,10},{9,15},{10,... | collective-permute-start | bytes 417800 | tf_op jit(solution)/shard_map/ppermute | solution.py:276
  41.2 5.1 %collective-permute-start.10 = (bf16[256,256]{1,0:T(8,128)(2,1)S(1)}, bf16[256,256]{1,0:T(8,128)(2,1)S(1)}, u32[]{:S(2)}, u32[]{:S(2)}) collective-permute-start(bf16[256,256]{1,0:T(8,128)(2,1)S(1)} %collective-permute-done.6.refs_3_), channel_id=1, source_target_pairs={{0,2},{1,7},{2,4},{3,1},{4,6},{5,3},{6,0},{7,5},{8,10},{9,15},{10,... | collective-permute-start | bytes 393224 | tf_op jit(solution)/shard_map/ppermute | solution.py:276
  41.2 7.8 %collective-permute-start.7 = (bf16[272,256]{1,0:T(8,128)(2,1)S(1)}, bf16[272,256]{1,0:T(8,128)(2,1)S(1)}, u32[]{:S(2)}, u32[]{:S(2)}) collective-permute-start(bf16[272,256]{1,0:T(8,128)(2,1)S(1)} %collective-permute-done.refs_2_), channel_id=1, source_target_pairs={{0,1},{1,0},{2,3},{3,2},{4,5},{5,4},{6,7},{7,6},{8,9},{9,8},{10,11... | collective-permute-start | bytes 417800 | tf_op jit(solution)/shard_map/ppermute | solution.py:288
  43.2 7.2 %collective-permute-start.2 = (bf16[272,256]{1,0:T(8,128)(2,1)S(1)}, bf16[272,256]{1,0:T(8,128)(2,1)S(1)}, u32[]{:S(2)}, u32[]{:S(2)}) collective-permute-start(bf16[272,256]{1,0:T(8,128)(2,1)S(1)} %collective-permute-done.1.refs_0_), channel_id=1, source_target_pairs={{0,1},{1,0},{2,3},{3,2},{4,5},{5,4},{6,7},{7,6},{8,9},{9,8},{10,11... | collective-permute-start | bytes 417800 | tf_op jit(solution)/shard_map/ppermute | solution.py:288
  46.3 4.2 %collective-permute-start.11 = (bf16[256,256]{1,0:T(8,128)(2,1)S(1)}, bf16[256,256]{1,0:T(8,128)(2,1)S(1)}, u32[]{:S(2)}, u32[]{:S(2)}) collective-permute-start(bf16[256,256]{1,0:T(8,128)(2,1)S(1)} %collective-permute-done.10.refs_1_), channel_id=1, source_target_pairs={{0,1},{1,0},{2,3},{3,2},{4,5},{5,4},{6,7},{7,6},{8,9},{9,8},{10,11... | collective-permute-start | bytes 393224 | tf_op jit(solution)/shard_map/ppermute | solution.py:288
  50.9 1.4 %copy-start.1 = (bf16[1,256,2048]{2,1,0:T(8,128)(2,1)S(1)}, bf16[1,256,2048]{2,1,0:T(8,128)(2,1)}, u32[]{:S(2)}) copy-start(bf16[1,256,2048]{2,1,0:T(8,128)(2,1)} %param.14) | copy-start | bytes 3145732
  50.9 1.4 %collective-permute-start.12 = (bf16[256,256]{1,0:T(8,128)(2,1)S(1)}, bf16[256,256]{1,0:T(8,128)(2,1)S(1)}, u32[]{:S(2)}, u32[]{:S(2)}) collective-permute-start(bf16[256,256]{1,0:T(8,128)(2,1)S(1)} %shard_map.88.refs_2_.own_ref), channel_id=1, source_target_pairs={{0,1},{1,0},{2,3},{3,2},{4,5},{5,4},{6,7},{7,6},{8,9},{9,8},{10,11... | collective-permute-start | bytes 393224 | tf_op jit(solution)/shard_map/ppermute | solution.py:288
  51.5 1.7 %collective-permute-start.9 = (bf16[256,256]{1,0:T(8,128)(2,1)S(1)}, bf16[256,256]{1,0:T(8,128)(2,1)S(1)}, u32[]{:S(2)}, u32[]{:S(2)}) collective-permute-start(bf16[256,256]{1,0:T(8,128)(2,1)S(1)} %shard_map.87.refs_0_.own_ref), channel_id=1, source_target_pairs={{0,1},{1,0},{2,3},{3,2},{4,5},{5,4},{6,7},{7,6},{8,9},{9,8},{10,11... | collective-permute-start | bytes 393224 | tf_op jit(solution)/shard_map/ppermute | solution.py:288
  52.6 4.1 %collective-permute-start.18 = (bf16[256,256]{1,0:T(8,128)(2,1)S(1)}, bf16[256,256]{1,0:T(8,128)(2,1)S(1)}, u32[]{:S(2)}, u32[]{:S(2)}) collective-permute-start(bf16[256,256]{1,0:T(8,128)(2,1)S(1)} %shard_map.91), channel_id=1, source_target_pairs={{0,2},{1,7},{2,4},{3,1},{4,6},{5,3},{6,0},{7,5},{8,10},{9,15},{10,... | collective-permute-start | bytes 393224 | tf_op jit(solution)/shard_map/ppermute | solution.py:276
  53.8 6.0 %collective-permute-start.14 = (bf16[512,256]{1,0:T(8,128)(2,1)S(1)}, bf16[512,256]{1,0:T(8,128)(2,1)S(1)}, u32[]{:S(2)}, u32[]{:S(2)}) collective-permute-start(bf16[512,256]{1,0:T(8,128)(2,1)S(1)} %get-tuple-element.39), channel_id=1, source_target_pairs={{0,2},{1,7},{2,4},{3,1},{4,6},{5,3},{6,0},{7,5},{8,10},{9,15},{10,... | collective-permute-start | bytes 786440 | tf_op jit(solution)/shard_map/ppermute | solution.py:276
  54.6 7.5 %collective-permute-start.16 = (bf16[256,256]{1,0:T(8,128)(2,1)S(1)}, bf16[256,256]{1,0:T(8,128)(2,1)S(1)}, u32[]{:S(2)}, u32[]{:S(2)}) collective-permute-start(bf16[256,256]{1,0:T(8,128)(2,1)S(1)} %shard_map.90), channel_id=1, source_target_pairs={{0,2},{1,7},{2,4},{3,1},{4,6},{5,3},{6,0},{7,5},{8,10},{9,15},{10,... | collective-permute-start | bytes 393224 | tf_op jit(solution)/shard_map/ppermute | solution.py:276
  56.7 6.4 %collective-permute-start.19 = (bf16[256,256]{1,0:T(8,128)(2,1)S(1)}, bf16[256,256]{1,0:T(8,128)(2,1)S(1)}, u32[]{:S(2)}, u32[]{:S(2)}) collective-permute-start(bf16[256,256]{1,0:T(8,128)(2,1)S(1)} %add_convert_fusion), channel_id=1, source_target_pairs={{0,2},{1,7},{2,4},{3,1},{4,6},{5,3},{6,0},{7,5},{8,10},{9,15},{10,... | collective-permute-start | bytes 393224 | tf_op jit(solution)/shard_map/ppermute | solution.py:276
  59.8 6.2 %collective-permute-start.15 = (bf16[512,256]{1,0:T(8,128)(2,1)S(1)}, bf16[512,256]{1,0:T(8,128)(2,1)S(1)}, u32[]{:S(2)}, u32[]{:S(2)}) collective-permute-start(bf16[512,256]{1,0:T(8,128)(2,1)S(1)} %collective-permute-done.14), channel_id=1, source_target_pairs={{0,1},{1,0},{2,3},{3,2},{4,5},{5,4},{6,7},{7,6},{8,9},{9,8},{10,11... | collective-permute-start | bytes 786440 | tf_op jit(solution)/shard_map/ppermute | solution.py:288
  62.1 3.9 %collective-permute-start.17 = (bf16[256,256]{1,0:T(8,128)(2,1)S(1)}, bf16[256,256]{1,0:T(8,128)(2,1)S(1)}, u32[]{:S(2)}, u32[]{:S(2)}) collective-permute-start(bf16[256,256]{1,0:T(8,128)(2,1)S(1)} %add_convert_fusion.1), channel_id=1, source_target_pairs={{0,2},{1,7},{2,4},{3,1},{4,6},{5,3},{6,0},{7,5},{8,10},{9,15},{10,... | collective-permute-start | bytes 393224 | tf_op jit(solution)/shard_map/ppermute | solution.py:276
  80.3 5.9 %collective-permute-start.20 = (f32[8,128]{1,0:T(8,128)S(1)}, f32[8,128]{1,0:T(8,128)S(1)}, u32[]{:S(2)}, u32[]{:S(2)}) collective-permute-start(f32[8,128]{1,0:T(8,128)S(1)} %get-tuple-element.43), channel_id=1, source_target_pairs={{0,1},{1,0},{2,3},{3,2},{4,5},{5,4},{6,7},{7,6},{8,9},{9,8},{10,11... | collective-permute-start | bytes 12296 | tf_op jit(solution)/shard_map/ppermute | solution.py:288
  86.2 3.7 %collective-permute-start.21 = (f32[8,128]{1,0:T(8,128)S(1)}, f32[8,128]{1,0:T(8,128)S(1)}, u32[]{:S(2)}, u32[]{:S(2)}) collective-permute-start(f32[8,128]{1,0:T(8,128)S(1)} %add.11.refs_0_), channel_id=1, source_target_pairs={{0,2},{1,3},{2,4},{3,5},{4,6},{5,7},{6,0},{7,1},{8,10},{9,11},{10,... | collective-permute-start | bytes 12296 | tf_op jit(solution)/shard_map/ppermute | solution.py:434
  86.2 3.7 %collective-permute-start.22 = (f32[8,128]{1,0:T(8,128)S(1)}, f32[8,128]{1,0:T(8,128)S(1)}, u32[]{:S(2)}, u32[]{:S(2)}) collective-permute-start(f32[8,128]{1,0:T(8,128)S(1)} %add.11.refs_0_), channel_id=1, source_target_pairs={{0,6},{1,7},{2,0},{3,1},{4,2},{5,3},{6,4},{7,5},{8,14},{9,15},{10,... | collective-permute-start | bytes 12296 | tf_op jit(solution)/shard_map/ppermute | solution.py:434
  88.9 4.0 %collective-permute-start.23 = (f32[8,128]{1,0:T(8,128)S(1)}, f32[8,128]{1,0:T(8,128)S(1)}, u32[]{:S(2)}, u32[]{:S(2)}) collective-permute-start(f32[8,128]{1,0:T(8,128)S(1)} %add.11.refs_0_), channel_id=1, source_target_pairs={{0,4},{1,5},{2,6},{3,7},{4,0},{5,1},{6,2},{7,3},{8,12},{9,13},{10,... | collective-permute-start | bytes 12296 | tf_op jit(solution)/shard_map/ppermute | solution.py:284

commit v7 on v6

--- a/solution.py
+++ b/solution.py
@@ -321,8 +321,8 @@
     second_other = swap(second)
     third_other_a = swap(third_a)
     third_other_b = swap(third_b)
-    sources = (ids, route_weights.T, final_gain[None, :], up_proj[0])
-    share, final_gain, up = call(
+    sources = (ids, route_weights.T, final_gain[None, :], up_proj[0], gate_proj[0])
+    share, final_gain, up, gate = call(
         functools.partial(load_kernel, experts, capacity),
         [shape_of((2 * tok_rows, rows), jnp.bfloat16)]
         + [shape_of(source.shape, source.dtype) for source in sources[2:]],
@@ -334,7 +334,7 @@
             pltpu.SemaphoreType.DMA((len(sources),)),
         ),
     )
-    gate, down = gate_proj[0], down_proj[0]
+    down = down_proj[0]
     down_other = swap(down)
     early = [
         ((0, 0, chips), (own,)),

time: 93.8 us -> 94.1 us (level)
  transfers between devices with their start and end apart: 25 -> 25, of which waited for: 11 -> 11; matrix products, arithmetic and copies ran while one was open for 0% -> 0% of each run, Pallas kernels for 5% -> 6%
where the time goes in v7:
time: 94.1 us; the launch traced here: 93.8 us
  starting transfers between devices  43.4 us (46%)
  waiting for transfers between devices  28 us (30%)
  blocking collectives  13.9 us (15%)
  Pallas kernels  8.21 us (9%)
    ppermute x11, starting transfers between devices, swap(): return lax.ppermute(value, 'tp', pairs)  18.6 us
    all_to_all x1, blocking collectives, local(): lax.all_to_all(expert_out, 'ep', split_axis=0, concat_axis=0, tiled=True)  13.9 us
    all_to_all x1, starting transfers between devices, local(): lax.all_to_all(outbound.reshape(experts, capacity, width), 'ep', split_ax...  11.9 us
    ppermute x10, waiting for transfers between devices, onward(): return lax.ppermute(value, 'tp', pairs)  11.5 us
    all_to_all x1, waiting for transfers between devices, local(): lax.all_to_all(outbound.reshape(experts, capacity, width), 'ep', split_ax...  10.3 us
    ppermute x10, starting transfers between devices, onward(): return lax.ppermute(value, 'tp', pairs)  10.2 us
    pallas_call x13, Pallas kernels, call(): pl.pallas_call(kernel, out_shape=outs, in_specs=[space] * len(args), out_...  8.21 us
    ppermute x1, waiting for transfers between devices, opposite(): return lax.ppermute(value, 'tp', pairs)  2.97 us
  transfers between devices with their start and end apart: 25, of which 11 were waited for; matrix products, arithmetic and copies ran while one was open for 0% of the time, Pallas kernels for 6%

profile of v7, /device:TPU:1, one launch (start us, length us, event | category | flops | bytes accessed | tf_op | source)
XLA Modules:
  0.0 93.8 jit_solution(3572053777046790626)
XLA Ops:
  0.0 1.8 %shard_map.83 = (bf16[512,256]{1,0:T(8,128)(2,1)}, f32[1,256]{1,0:T(1,128)S(1)}) custom-call(s32[4,64]{1,0:T(4,128)} %bitcast.20, bf16[64,256]{1,0:T(8,128)(2,1)} %tokens_hbm.1, f32[1,256]{1,0:T(1,128)} %bitcast.24), custom_call_target="tpu_custom_call" | custom-call | tf_op jit(solution)/shard_map/pallas_call | solution.py:246
  1.8 11.9 %all-to-all-start = ((bf16[32,16,256]{2,1,0:T(8,128)(2,1)}), bf16[32,16,256]{2,1,0:T(8,128)(2,1)S(1)}, u32[]{:S(2)}, u32[]{:S(2)}) async-start(bf16[32,16,256]{2,1,0:T(8,128)(2,1)} %bitcast.6), calls=%async_computation | async-start | bytes 524288 | tf_op jit(solution)/shard_map/all_to_all | solution.py:305
  13.6 1.0 %collective-permute-start.13 = (bf16[256,2048]{1,0:T(8,128)(2,1)}, bf16[256,2048]{1,0:T(8,128)(2,1)S(1)}, u32[]{:S(2)}, u32[]{:S(2)}) collective-permute-start(bf16[256,2048]{1,0:T(8,128)(2,1)} %bitcast.11), channel_id=1, source_target_pairs={{0,1},{1,0},{2,3},{3,2},{4,5},{5,4},{6,7},{7,6},{8,9},{9,8},{10,11... | collective-permute-start | bytes 3145736 | tf_op jit(solution)/shard_map/ppermute | solution.py:288
  14.7 10.3 %all-to-all-done = bf16[32,16,256]{2,1,0:T(8,128)(2,1)S(1)} async-done(((bf16[32,16,256]{2,1,0:T(8,128)(2,1)}), bf16[32,16,256]{2,1,0:T(8,128)(2,1)S(1)}, u32[]{:S(2)}, u32[]{:S(2)}) %all-to-all-start) | async-done | bytes 262176 | tf_op jit(solution)/shard_map/all_to_all | solution.py:305
  25.3 2.5 %collective-permute-start.3 = (bf16[528,256]{1,0:T(8,128)(2,1)S(1)}, bf16[528,256]{1,0:T(8,128)(2,1)S(1)}, u32[]{:S(2)}, u32[]{:S(2)}) collective-permute-start(bf16[528,256]{1,0:T(8,128)(2,1)S(1)} %get-tuple-element.32.refs_0_), channel_id=1, source_target_pairs={{0,1},{1,0},{2,3},{3,2},{4,5},{5,4},{6,7},{7,6},{8,9},{9,8},{10,11... | collective-permute-start | bytes 811016 | tf_op jit(solution)/shard_map/ppermute | solution.py:288
  27.8 1.2 %collective-permute-done.3.refs_1_ = bf16[528,256]{1,0:T(8,128)(2,1)S(1)} collective-permute-done((bf16[528,256]{1,0:T(8,128)(2,1)S(1)}, bf16[528,256]{1,0:T(8,128)(2,1)S(1)}, u32[]{:S(2)}, u32[]{:S(2)}) %collective-permute-start.3) | collective-permute-done | bytes 270368 | tf_op jit(solution)/shard_map/ppermute | solution.py:288
  29.0 2.7 %collective-permute-start.4 = (bf16[528,256]{1,0:T(8,128)(2,1)S(1)}, bf16[528,256]{1,0:T(8,128)(2,1)S(1)}, u32[]{:S(2)}, u32[]{:S(2)}) collective-permute-start(bf16[528,256]{1,0:T(8,128)(2,1)S(1)} %collective-permute-done.3.refs_1_), channel_id=1, source_target_pairs={{0,2},{1,7},{2,4},{3,1},{4,6},{5,3},{6,0},{7,5},{8,10},{9,15},{10,... | collective-permute-start | bytes 811016 | tf_op jit(solution)/shard_map/ppermute | solution.py:276
  32.4 4.2 %collective-permute-done.6.refs_3_ = bf16[256,256]{1,0:T(8,128)(2,1)S(1)} collective-permute-done((bf16[256,256]{1,0:T(8,128)(2,1)S(1)}, bf16[256,256]{1,0:T(8,128)(2,1)S(1)}, u32[]{:S(2)}, u32[]{:S(2)}) %collective-permute-start.6) | collective-permute-done | bytes 131104 | tf_op jit(solution)/shard_map/ppermute | solution.py:276
  36.5 1.9 %collective-permute-start.8 = (bf16[256,256]{1,0:T(8,128)(2,1)S(1)}, bf16[256,256]{1,0:T(8,128)(2,1)S(1)}, u32[]{:S(2)}, u32[]{:S(2)}) collective-permute-start(bf16[256,256]{1,0:T(8,128)(2,1)S(1)} %collective-permute-done.6.refs_3_), channel_id=1, source_target_pairs={{0,1},{1,0},{2,3},{3,2},{4,5},{5,4},{6,7},{7,6},{8,9},{9,8},{10,11... | collective-permute-start | bytes 393224 | tf_op jit(solution)/shard_map/ppermute | solution.py:288
  38.4 2.7 %collective-permute-start.1 = (bf16[272,256]{1,0:T(8,128)(2,1)S(1)}, bf16[272,256]{1,0:T(8,128)(2,1)S(1)}, u32[]{:S(2)}, u32[]{:S(2)}) collective-permute-start(bf16[272,256]{1,0:T(8,128)(2,1)S(1)} %collective-permute-done.refs_2_), channel_id=1, source_target_pairs={{0,2},{1,7},{2,4},{3,1},{4,6},{5,3},{6,0},{7,5},{8,10},{9,15},{10,... | collective-permute-start | bytes 417800 | tf_op jit(solution)/shard_map/ppermute | solution.py:276
  41.1 0.7 collective-permute-start.7
  41.9 1.3 %collective-permute-done.1.refs_0_ = bf16[272,256]{1,0:T(8,128)(2,1)S(1)} collective-permute-done((bf16[272,256]{1,0:T(8,128)(2,1)S(1)}, bf16[272,256]{1,0:T(8,128)(2,1)S(1)}, u32[]{:S(2)}, u32[]{:S(2)}) %collective-permute-start.1) | collective-permute-done | bytes 139296 | tf_op jit(solution)/shard_map/ppermute | solution.py:276
  43.1 3.0 %collective-permute-start.2 = (bf16[272,256]{1,0:T(8,128)(2,1)S(1)}, bf16[272,256]{1,0:T(8,128)(2,1)S(1)}, u32[]{:S(2)}, u32[]{:S(2)}) collective-permute-start(bf16[272,256]{1,0:T(8,128)(2,1)S(1)} %collective-permute-done.1.refs_0_), channel_id=1, source_target_pairs={{0,1},{1,0},{2,3},{3,2},{4,5},{5,4},{6,7},{7,6},{8,9},{9,8},{10,11... | collective-permute-start | bytes 417800 | tf_op jit(solution)/shard_map/ppermute | solution.py:288
  46.2 1.4 %collective-permute-start.11 = (bf16[256,256]{1,0:T(8,128)(2,1)S(1)}, bf16[256,256]{1,0:T(8,128)(2,1)S(1)}, u32[]{:S(2)}, u32[]{:S(2)}) collective-permute-start(bf16[256,256]{1,0:T(8,128)(2,1)S(1)} %collective-permute-done.10.refs_1_), channel_id=1, source_target_pairs={{0,1},{1,0},{2,3},{3,2},{4,5},{5,4},{6,7},{7,6},{8,9},{9,8},{10,11... | collective-permute-start | bytes 393224 | tf_op jit(solution)/shard_map/ppermute | solution.py:288
  47.6 1.6 %shard_map.82 = (bf16[128,512]{1,0:T(8,128)(2,1)S(1)}, f32[1,256]{1,0:T(1,128)S(1)}, bf16[2048,256]{1,0:T(8,128)(2,1)S(1)}, bf16[2048,256]{1,0:T(8,128)(2,1)S(1)}) custom-call(s32[4,64]{1,0:T(4,128)} %bitcast.21, f32[4,64]{1,0:T(4,128)} %bitcast.22, f32[1,256]{1,0:T(1,128)} %bitcast.23, bf16[2048,256]{1,0:T(8,128)(2,1)} %bitcast.18, bf16[2048,256]{1,0:T(8,128)(2,1)} %bitcast.19), custom_call_target="tpu_custom_call" | custom-call | tf_op jit(solution)/shard_map/pallas_call | solution.py:246
  49.2 0.9 shard_map.85
  51.7 0.6 collective-permute-start.9
  52.8 0.6 collective-permute-start.18
  53.4 0.6 shard_map.89
  55.2 1.8 %collective-permute-done.18 = bf16[256,256]{1,0:T(8,128)(2,1)S(1)} collective-permute-done((bf16[256,256]{1,0:T(8,128)(2,1)S(1)}, bf16[256,256]{1,0:T(8,128)(2,1)S(1)}, u32[]{:S(2)}, u32[]{:S(2)}) %collective-permute-start.18) | collective-permute-done | bytes 131104 | tf_op jit(solution)/shard_map/ppermute | solution.py:276
  57.0 1.6 %collective-permute-start.19 = (bf16[256,256]{1,0:T(8,128)(2,1)S(1)}, bf16[256,256]{1,0:T(8,128)(2,1)S(1)}, u32[]{:S(2)}, u32[]{:S(2)}) collective-permute-start(bf16[256,256]{1,0:T(8,128)(2,1)S(1)} %add_convert_fusion), channel_id=1, source_target_pairs={{0,2},{1,7},{2,4},{3,1},{4,6},{5,3},{6,0},{7,5},{8,10},{9,15},{10,... | collective-permute-start | bytes 393224 | tf_op jit(solution)/shard_map/ppermute | solution.py:276
  58.6 1.5 %collective-permute-done.14 = bf16[512,256]{1,0:T(8,128)(2,1)S(1)} collective-permute-done((bf16[512,256]{1,0:T(8,128)(2,1)S(1)}, bf16[512,256]{1,0:T(8,128)(2,1)S(1)}, u32[]{:S(2)}, u32[]{:S(2)}) %collective-permute-start.14) | collective-permute-done | bytes 262176 | tf_op jit(solution)/shard_map/ppermute | solution.py:276
  60.0 2.2 %collective-permute-start.15 = (bf16[512,256]{1,0:T(8,128)(2,1)S(1)}, bf16[512,256]{1,0:T(8,128)(2,1)S(1)}, u32[]{:S(2)}, u32[]{:S(2)}) collective-permute-start(bf16[512,256]{1,0:T(8,128)(2,1)S(1)} %collective-permute-done.14), channel_id=1, source_target_pairs={{0,1},{1,0},{2,3},{3,2},{4,5},{5,4},{6,7},{7,6},{8,9},{9,8},{10,11... | collective-permute-start | bytes 786440 | tf_op jit(solution)/shard_map/ppermute | solution.py:288
  62.3 1.1 %collective-permute-start.17 = (bf16[256,256]{1,0:T(8,128)(2,1)S(1)}, bf16[256,256]{1,0:T(8,128)(2,1)S(1)}, u32[]{:S(2)}, u32[]{:S(2)}) collective-permute-start(bf16[256,256]{1,0:T(8,128)(2,1)S(1)} %add_convert_fusion.1), channel_id=1, source_target_pairs={{0,2},{1,7},{2,4},{3,1},{4,6},{5,3},{6,0},{7,5},{8,10},{9,15},{10,... | collective-permute-start | bytes 393224 | tf_op jit(solution)/shard_map/ppermute | solution.py:276
  63.4 2.8 %collective-permute-done.17.near_a_ref = bf16[256,256]{1,0:T(8,128)(2,1)S(1)} collective-permute-done((bf16[256,256]{1,0:T(8,128)(2,1)S(1)}, bf16[256,256]{1,0:T(8,128)(2,1)S(1)}, u32[]{:S(2)}, u32[]{:S(2)}) %collective-permute-start.17) | collective-permute-done | bytes 131104 | tf_op jit(solution)/shard_map/ppermute | solution.py:276
  66.3 13.9 %all_to_all.10 = bf16[32,16,256]{2,1,0:T(8,128)(2,1)S(1)} all-to-all(bf16[32,16,256]{2,1,0:T(8,128)(2,1)S(1)} %bitcast.17), channel_id=1, replica_groups=mesh['ep'=32,'tp'=8] {'ep'}, dimensions={0} | all-to-all | bytes 524288 | tf_op jit(solution)/shard_map/all_to_all | solution.py:419
  80.5 5.1 %collective-permute-start.20 = (f32[8,128]{1,0:T(8,128)S(1)}, f32[8,128]{1,0:T(8,128)S(1)}, u32[]{:S(2)}, u32[]{:S(2)}) collective-permute-start(f32[8,128]{1,0:T(8,128)S(1)} %get-tuple-element.45), channel_id=1, source_target_pairs={{0,1},{1,0},{2,3},{3,2},{4,5},{5,4},{6,7},{7,6},{8,9},{9,8},{10,11... | collective-permute-start | bytes 12296 | tf_op jit(solution)/shard_map/ppermute | solution.py:288
  85.6 0.8 collective-permute-done.20
  86.5 2.7 %collective-permute-start.22 = (f32[8,128]{1,0:T(8,128)S(1)}, f32[8,128]{1,0:T(8,128)S(1)}, u32[]{:S(2)}, u32[]{:S(2)}) collective-permute-start(f32[8,128]{1,0:T(8,128)S(1)} %add.11.refs_0_), channel_id=1, source_target_pairs={{0,6},{1,7},{2,0},{3,1},{4,2},{5,3},{6,4},{7,5},{8,14},{9,15},{10,... | collective-permute-start | bytes 12296 | tf_op jit(solution)/shard_map/ppermute | solution.py:434
  89.1 1.0 %collective-permute-done.21.refs_1_ = f32[8,128]{1,0:T(8,128)S(1)} collective-permute-done((f32[8,128]{1,0:T(8,128)S(1)}, f32[8,128]{1,0:T(8,128)S(1)}, u32[]{:S(2)}, u32[]{:S(2)}) %collective-permute-start.21) | collective-permute-done | bytes 4128 | tf_op jit(solution)/shard_map/ppermute | solution.py:434
  90.1 3.0 %collective-permute-done.23.refs_3_ = f32[8,128]{1,0:T(8,128)S(1)} collective-permute-done((f32[8,128]{1,0:T(8,128)S(1)}, f32[8,128]{1,0:T(8,128)S(1)}, u32[]{:S(2)}, u32[]{:S(2)}) %collective-permute-start.23) | collective-permute-done | bytes 4128 | tf_op jit(solution)/shard_map/ppermute | solution.py:284
  93.1 0.7 shard_map.94
  (37 shorter events, 4.7 us)
Async XLA Ops:
  1.8 23.2 %all-to-all-start = ((bf16[32,16,256]{2,1,0:T(8,128)(2,1)}), bf16[32,16,256]{2,1,0:T(8,128)(2,1)S(1)}, u32[]{:S(2)}, u32[]{:S(2)}) async-start(bf16[32,16,256]{2,1,0:T(8,128)(2,1)} %bitcast.6), calls=%async_computation | async-start | bytes 524288 | tf_op jit(solution)/shard_map/all_to_all | solution.py:305
  13.6 38.7 %collective-permute-start.13 = (bf16[256,2048]{1,0:T(8,128)(2,1)}, bf16[256,2048]{1,0:T(8,128)(2,1)S(1)}, u32[]{:S(2)}, u32[]{:S(2)}) collective-permute-start(bf16[256,2048]{1,0:T(8,128)(2,1)} %bitcast.11), channel_id=1, source_target_pairs={{0,1},{1,0},{2,3},{3,2},{4,5},{5,4},{6,7},{7,6},{8,9},{9,8},{10,11... | collective-permute-start | bytes 3145736 | tf_op jit(solution)/shard_map/ppermute | solution.py:288
  25.3 3.7 %collective-permute-start.3 = (bf16[528,256]{1,0:T(8,128)(2,1)S(1)}, bf16[528,256]{1,0:T(8,128)(2,1)S(1)}, u32[]{:S(2)}, u32[]{:S(2)}) collective-permute-start(bf16[528,256]{1,0:T(8,128)(2,1)S(1)} %get-tuple-element.32.refs_0_), channel_id=1, source_target_pairs={{0,1},{1,0},{2,3},{3,2},{4,5},{5,4},{6,7},{7,6},{8,9},{9,8},{10,11... | collective-permute-start | bytes 811016 | tf_op jit(solution)/shard_map/ppermute | solution.py:288
  29.0 9.5 %collective-permute-start.4 = (bf16[528,256]{1,0:T(8,128)(2,1)S(1)}, bf16[528,256]{1,0:T(8,128)(2,1)S(1)}, u32[]{:S(2)}, u32[]{:S(2)}) collective-permute-start(bf16[528,256]{1,0:T(8,128)(2,1)S(1)} %collective-permute-done.3.refs_1_), channel_id=1, source_target_pairs={{0,2},{1,7},{2,4},{3,1},{4,6},{5,3},{6,0},{7,5},{8,10},{9,15},{10,... | collective-permute-start | bytes 811016 | tf_op jit(solution)/shard_map/ppermute | solution.py:276
  31.7 4.8 %collective-permute-start.6 = (bf16[256,256]{1,0:T(8,128)(2,1)S(1)}, bf16[256,256]{1,0:T(8,128)(2,1)S(1)}, u32[]{:S(2)}, u32[]{:S(2)}) collective-permute-start(bf16[256,256]{1,0:T(8,128)(2,1)S(1)} %get-tuple-element.33), channel_id=1, source_target_pairs={{0,2},{1,7},{2,4},{3,1},{4,6},{5,3},{6,0},{7,5},{8,10},{9,15},{10,... | collective-permute-start | bytes 393224 | tf_op jit(solution)/shard_map/ppermute | solution.py:276
  32.2 6.3 %collective-permute-start = (bf16[272,256]{1,0:T(8,128)(2,1)S(1)}, bf16[272,256]{1,0:T(8,128)(2,1)S(1)}, u32[]{:S(2)}, u32[]{:S(2)}) collective-permute-start(bf16[272,256]{1,0:T(8,128)(2,1)S(1)} %get-tuple-element.29), channel_id=1, source_target_pairs={{0,2},{1,7},{2,4},{3,1},{4,6},{5,3},{6,0},{7,5},{8,10},{9,15},{10,... | collective-permute-start | bytes 417800 | tf_op jit(solution)/shard_map/ppermute | solution.py:276
  36.5 4.6 %collective-permute-start.8 = (bf16[256,256]{1,0:T(8,128)(2,1)S(1)}, bf16[256,256]{1,0:T(8,128)(2,1)S(1)}, u32[]{:S(2)}, u32[]{:S(2)}) collective-permute-start(bf16[256,256]{1,0:T(8,128)(2,1)S(1)} %collective-permute-done.6.refs_3_), channel_id=1, source_target_pairs={{0,1},{1,0},{2,3},{3,2},{4,5},{5,4},{6,7},{7,6},{8,9},{9,8},{10,11... | collective-permute-start | bytes 393224 | tf_op jit(solution)/shard_map/ppermute | solution.py:288
  38.4 11.7 %collective-permute-start.5 = (bf16[528,256]{1,0:T(8,128)(2,1)S(1)}, bf16[528,256]{1,0:T(8,128)(2,1)S(1)}, u32[]{:S(2)}, u32[]{:S(2)}) collective-permute-start(bf16[528,256]{1,0:T(8,128)(2,1)S(1)} %collective-permute-done.4.refs_0_), channel_id=1, source_target_pairs={{0,1},{1,0},{2,3},{3,2},{4,5},{5,4},{6,7},{7,6},{8,9},{9,8},{10,11... | collective-permute-start | bytes 811016 | tf_op jit(solution)/shard_map/ppermute | solution.py:288
  38.4 4.7 %collective-permute-start.1 = (bf16[272,256]{1,0:T(8,128)(2,1)S(1)}, bf16[272,256]{1,0:T(8,128)(2,1)S(1)}, u32[]{:S(2)}, u32[]{:S(2)}) collective-permute-start(bf16[272,256]{1,0:T(8,128)(2,1)S(1)} %collective-permute-done.refs_2_), channel_id=1, source_target_pairs={{0,2},{1,7},{2,4},{3,1},{4,6},{5,3},{6,0},{7,5},{8,10},{9,15},{10,... | collective-permute-start | bytes 417800 | tf_op jit(solution)/shard_map/ppermute | solution.py:276
  41.1 5.1 %collective-permute-start.10 = (bf16[256,256]{1,0:T(8,128)(2,1)S(1)}, bf16[256,256]{1,0:T(8,128)(2,1)S(1)}, u32[]{:S(2)}, u32[]{:S(2)}) collective-permute-start(bf16[256,256]{1,0:T(8,128)(2,1)S(1)} %collective-permute-done.6.refs_3_), channel_id=1, source_target_pairs={{0,2},{1,7},{2,4},{3,1},{4,6},{5,3},{6,0},{7,5},{8,10},{9,15},{10,... | collective-permute-start | bytes 393224 | tf_op jit(solution)/shard_map/ppermute | solution.py:276
  41.1 8.1 %collective-permute-start.7 = (bf16[272,256]{1,0:T(8,128)(2,1)S(1)}, bf16[272,256]{1,0:T(8,128)(2,1)S(1)}, u32[]{:S(2)}, u32[]{:S(2)}) collective-permute-start(bf16[272,256]{1,0:T(8,128)(2,1)S(1)} %collective-permute-done.refs_2_), channel_id=1, source_target_pairs={{0,1},{1,0},{2,3},{3,2},{4,5},{5,4},{6,7},{7,6},{8,9},{9,8},{10,11... | collective-permute-start | bytes 417800 | tf_op jit(solution)/shard_map/ppermute | solution.py:288
  43.1 7.5 %collective-permute-start.2 = (bf16[272,256]{1,0:T(8,128)(2,1)S(1)}, bf16[272,256]{1,0:T(8,128)(2,1)S(1)}, u32[]{:S(2)}, u32[]{:S(2)}) collective-permute-start(bf16[272,256]{1,0:T(8,128)(2,1)S(1)} %collective-permute-done.1.refs_0_), channel_id=1, source_target_pairs={{0,1},{1,0},{2,3},{3,2},{4,5},{5,4},{6,7},{7,6},{8,9},{9,8},{10,11... | collective-permute-start | bytes 417800 | tf_op jit(solution)/shard_map/ppermute | solution.py:288
  46.2 4.5 %collective-permute-start.11 = (bf16[256,256]{1,0:T(8,128)(2,1)S(1)}, bf16[256,256]{1,0:T(8,128)(2,1)S(1)}, u32[]{:S(2)}, u32[]{:S(2)}) collective-permute-start(bf16[256,256]{1,0:T(8,128)(2,1)S(1)} %collective-permute-done.10.refs_1_), channel_id=1, source_target_pairs={{0,1},{1,0},{2,3},{3,2},{4,5},{5,4},{6,7},{7,6},{8,9},{9,8},{10,11... | collective-permute-start | bytes 393224 | tf_op jit(solution)/shard_map/ppermute | solution.py:288
  51.2 1.4 %copy-start = (bf16[1,256,2048]{2,1,0:T(8,128)(2,1)S(1)}, bf16[1,256,2048]{2,1,0:T(8,128)(2,1)}, u32[]{:S(2)}) copy-start(bf16[1,256,2048]{2,1,0:T(8,128)(2,1)} %param.14) | copy-start | bytes 3145732
  51.2 1.4 %collective-permute-start.12 = (bf16[256,256]{1,0:T(8,128)(2,1)S(1)}, bf16[256,256]{1,0:T(8,128)(2,1)S(1)}, u32[]{:S(2)}, u32[]{:S(2)}) collective-permute-start(bf16[256,256]{1,0:T(8,128)(2,1)S(1)} %shard_map.88.refs_2_.own_ref), channel_id=1, source_target_pairs={{0,1},{1,0},{2,3},{3,2},{4,5},{5,4},{6,7},{7,6},{8,9},{9,8},{10,11... | collective-permute-start | bytes 393224 | tf_op jit(solution)/shard_map/ppermute | solution.py:288
  51.7 1.7 %collective-permute-start.9 = (bf16[256,256]{1,0:T(8,128)(2,1)S(1)}, bf16[256,256]{1,0:T(8,128)(2,1)S(1)}, u32[]{:S(2)}, u32[]{:S(2)}) collective-permute-start(bf16[256,256]{1,0:T(8,128)(2,1)S(1)} %shard_map.87.refs_0_.own_ref), channel_id=1, source_target_pairs={{0,1},{1,0},{2,3},{3,2},{4,5},{5,4},{6,7},{7,6},{8,9},{9,8},{10,11... | collective-permute-start | bytes 393224 | tf_op jit(solution)/shard_map/ppermute | solution.py:288
  52.8 4.1 %collective-permute-start.18 = (bf16[256,256]{1,0:T(8,128)(2,1)S(1)}, bf16[256,256]{1,0:T(8,128)(2,1)S(1)}, u32[]{:S(2)}, u32[]{:S(2)}) collective-permute-start(bf16[256,256]{1,0:T(8,128)(2,1)S(1)} %shard_map.91), channel_id=1, source_target_pairs={{0,2},{1,7},{2,4},{3,1},{4,6},{5,3},{6,0},{7,5},{8,10},{9,15},{10,... | collective-permute-start | bytes 393224 | tf_op jit(solution)/shard_map/ppermute | solution.py:276
  54.0 6.0 %collective-permute-start.14 = (bf16[512,256]{1,0:T(8,128)(2,1)S(1)}, bf16[512,256]{1,0:T(8,128)(2,1)S(1)}, u32[]{:S(2)}, u32[]{:S(2)}) collective-permute-start(bf16[512,256]{1,0:T(8,128)(2,1)S(1)} %get-tuple-element.41), channel_id=1, source_target_pairs={{0,2},{1,7},{2,4},{3,1},{4,6},{5,3},{6,0},{7,5},{8,10},{9,15},{10,... | collective-permute-start | bytes 786440 | tf_op jit(solution)/shard_map/ppermute | solution.py:276
  54.8 7.5 %collective-permute-start.16 = (bf16[256,256]{1,0:T(8,128)(2,1)S(1)}, bf16[256,256]{1,0:T(8,128)(2,1)S(1)}, u32[]{:S(2)}, u32[]{:S(2)}) collective-permute-start(bf16[256,256]{1,0:T(8,128)(2,1)S(1)} %shard_map.90), channel_id=1, source_target_pairs={{0,2},{1,7},{2,4},{3,1},{4,6},{5,3},{6,0},{7,5},{8,10},{9,15},{10,... | collective-permute-start | bytes 393224 | tf_op jit(solution)/shard_map/ppermute | solution.py:276
  57.0 6.4 %collective-permute-start.19 = (bf16[256,256]{1,0:T(8,128)(2,1)S(1)}, bf16[256,256]{1,0:T(8,128)(2,1)S(1)}, u32[]{:S(2)}, u32[]{:S(2)}) collective-permute-start(bf16[256,256]{1,0:T(8,128)(2,1)S(1)} %add_convert_fusion), channel_id=1, source_target_pairs={{0,2},{1,7},{2,4},{3,1},{4,6},{5,3},{6,0},{7,5},{8,10},{9,15},{10,... | collective-permute-start | bytes 393224 | tf_op jit(solution)/shard_map/ppermute | solution.py:276
  60.0 6.2 %collective-permute-start.15 = (bf16[512,256]{1,0:T(8,128)(2,1)S(1)}, bf16[512,256]{1,0:T(8,128)(2,1)S(1)}, u32[]{:S(2)}, u32[]{:S(2)}) collective-permute-start(bf16[512,256]{1,0:T(8,128)(2,1)S(1)} %collective-permute-done.14), channel_id=1, source_target_pairs={{0,1},{1,0},{2,3},{3,2},{4,5},{5,4},{6,7},{7,6},{8,9},{9,8},{10,11... | collective-permute-start | bytes 786440 | tf_op jit(solution)/shard_map/ppermute | solution.py:288
  62.3 3.9 %collective-permute-start.17 = (bf16[256,256]{1,0:T(8,128)(2,1)S(1)}, bf16[256,256]{1,0:T(8,128)(2,1)S(1)}, u32[]{:S(2)}, u32[]{:S(2)}) collective-permute-start(bf16[256,256]{1,0:T(8,128)(2,1)S(1)} %add_convert_fusion.1), channel_id=1, source_target_pairs={{0,2},{1,7},{2,4},{3,1},{4,6},{5,3},{6,0},{7,5},{8,10},{9,15},{10,... | collective-permute-start | bytes 393224 | tf_op jit(solution)/shard_map/ppermute | solution.py:276
  80.5 5.9 %collective-permute-start.20 = (f32[8,128]{1,0:T(8,128)S(1)}, f32[8,128]{1,0:T(8,128)S(1)}, u32[]{:S(2)}, u32[]{:S(2)}) collective-permute-start(f32[8,128]{1,0:T(8,128)S(1)} %get-tuple-element.45), channel_id=1, source_target_pairs={{0,1},{1,0},{2,3},{3,2},{4,5},{5,4},{6,7},{7,6},{8,9},{9,8},{10,11... | collective-permute-start | bytes 12296 | tf_op jit(solution)/shard_map/ppermute | solution.py:288
  86.5 3.7 %collective-permute-start.21 = (f32[8,128]{1,0:T(8,128)S(1)}, f32[8,128]{1,0:T(8,128)S(1)}, u32[]{:S(2)}, u32[]{:S(2)}) collective-permute-start(f32[8,128]{1,0:T(8,128)S(1)} %add.11.refs_0_), channel_id=1, source_target_pairs={{0,2},{1,3},{2,4},{3,5},{4,6},{5,7},{6,0},{7,1},{8,10},{9,11},{10,... | collective-permute-start | bytes 12296 | tf_op jit(solution)/shard_map/ppermute | solution.py:434
  86.5 3.7 %collective-permute-start.22 = (f32[8,128]{1,0:T(8,128)S(1)}, f32[8,128]{1,0:T(8,128)S(1)}, u32[]{:S(2)}, u32[]{:S(2)}) collective-permute-start(f32[8,128]{1,0:T(8,128)S(1)} %add.11.refs_0_), channel_id=1, source_target_pairs={{0,6},{1,7},{2,0},{3,1},{4,2},{5,3},{6,4},{7,5},{8,14},{9,15},{10,... | collective-permute-start | bytes 12296 | tf_op jit(solution)/shard_map/ppermute | solution.py:434
  89.1 4.0 %collective-permute-start.23 = (f32[8,128]{1,0:T(8,128)S(1)}, f32[8,128]{1,0:T(8,128)S(1)}, u32[]{:S(2)}, u32[]{:S(2)}) collective-permute-start(f32[8,128]{1,0:T(8,128)S(1)} %add.11.refs_0_), channel_id=1, source_target_pairs={{0,4},{1,5},{2,6},{3,7},{4,0},{5,1},{6,2},{7,3},{8,12},{9,13},{10,... | collective-permute-start | bytes 12296 | tf_op jit(solution)/shard_map/ppermute | solution.py:284
